TPU v7x, 1024 devices: a whole 4x4x32 slice. The times are simulated.
1024 devices in a mesh: sp: 256 (over z, x, core), tp: 4 (over y).
Axes of the slice: x: 4, y: 4, z: 32, core: 2. Of those that a mesh axis runs over, the one named last changes fastest.
Arguments:
- proj_value: bfloat16 [98304, 1024], P('sp', 'tp'), may hold values from -6 to 6
- proj_gate: bfloat16 [98304, 1024], P('sp', 'tp'), may hold values from -8 to 8
- out_cotangent: bfloat16 [98304, 2048], P('sp'), may hold values from -24 to 24
- out_weight: bfloat16 [1024, 2048], P('tp'), may hold values from -0.1875 to 0.1875
- conv_taps: bfloat16 [31, 1024], P(None, 'tp'), may hold values from -1 to 1
- norm_gain: float32 [1024], P('tp'), may hold values from 0.1 to 1.9
- row_mean: float32 [98304], P('sp'), may hold values from -2 to 2
- row_scale: float32 [98304], P('sp'), may hold values from 0.7 to 3
Outputs:
- value_grad: bfloat16 [98304, 1024], P('sp', 'tp')
- gate_grad: bfloat16 [98304, 1024], P('sp', 'tp')
- out_weight_grad: float32 [2048, 1024], P('sp', 'tp')
- taps_grad: float32 [31, 1024], P(None, 'tp')
- gain_grad: float32 [1024], P('tp')
All inputs are finite; a program needn't handle non-finite values.
Results may differ from a plain program's by a relative error of at most 0.0047.
Values may be sent and summed in bfloat16 or wider, within the bound.
No kernel may reach another device: no remote copies, remote signals or barrier semaphores. Data moves between devices by JAX's collectives and lax.ppermute only.
A program may use at most 32 MiB of HBM per device.

v0:
```python
import jax
import jax.numpy as jnp
from jax import lax
from jax.sharding import Mesh
from jax.sharding import PartitionSpec as P

SP = ("sp_0", "sp_1", "sp_2")


def shifted(value, axis, steps):
    count = lax.axis_size(axis)
    first, last = (max(0, -steps), min(count, count - steps))
    return lax.ppermute(value, axis, [(source, source + steps) for source in range(first, last)])


def own_block(parts, axes, sequence):
    inside = parts.shape[1:]
    parts = parts.reshape(*(lax.axis_size(a) for a in axes), *inside)
    parts = jnp.moveaxis(parts, sequence, range(len(axes))).reshape(-1, *inside)
    for k in sequence:
        parts = lax.psum_scatter(parts, axes[k], scatter_dimension=0, tiled=True)
    return parts[0]


def in_blocks(array, dim, devices):
    lengths = array.shape
    parts = array.reshape(*lengths[:dim], devices, lengths[dim] // devices, *lengths[dim + 1 :])
    return jnp.moveaxis(parts, dim, 0)


def sum_by_axis(array, axes, sequence, dim):
    devices = lax.axis_size(axes)
    return own_block(in_blocks(array, dim, devices), axes, sequence)


def from_everyone(array, axis):
    devices = lax.axis_size(axis)
    return lax.all_to_all(
        jnp.broadcast_to(array[None], (devices, *array.shape)), axis, 0, 0, tiled=True
    )


def over_copies(array, axis):
    return from_everyone(array, axis).sum(axis=0)


def in_one(arrays, axis):
    ends = [0]
    for a in arrays:
        ends.append(ends[-1] + a.size)
    running = over_copies(jnp.concatenate([a.ravel() for a in arrays]), axis)
    return tuple((running[b:e].reshape(a.shape) for a, b, e in zip(arrays, ends, ends[1:])))


def over_axes(array, axes):
    for axis in axes:
        array = lax.psum(array, axis)
    return array


def shards(
    proj_value, proj_gate, out_cotangent, out_weight, conv_taps, norm_gain, row_mean, row_scale
):
    kernel = conv_taps.shape[0]
    margin = kernel - 1
    length = proj_value.shape[0]
    channels = proj_value.shape[1]
    gate_sig = jax.nn.sigmoid(proj_gate.astype(jnp.float32))
    gated = (proj_value.astype(jnp.float32) * gate_sig).astype(jnp.bfloat16)
    before = shifted(gated[length - margin :], SP, 1)
    padded = jnp.concatenate([before, gated], 0).astype(jnp.float32)
    taps_wide = conv_taps.astype(jnp.float32)
    conv = jnp.zeros((length, channels), jnp.float32)
    for offset in range(kernel):
        conv = conv + taps_wide[offset][None, :] * padded[offset : offset + length]
    normed = (conv - row_mean[:, None]) * row_scale[:, None]
    active = normed * norm_gain[None, :]
    sig_act = jax.nn.sigmoid(active)
    hidden = (active * sig_act).astype(jnp.bfloat16)
    upstream = lax.dot_general(
        out_cotangent, out_weight, (((1,), (1,)), ((), ())), preferred_element_type=jnp.float32
    )
    weight_grad = sum_by_axis(
        lax.dot_general(
            out_cotangent, hidden, (((0,), (0,)), ((), ())), preferred_element_type=jnp.float32
        ),
        SP,
        (2, 0, 1),
        0,
    )
    d_active = upstream * sig_act * (1.0 + active * (1.0 - sig_act))
    gain_local = jnp.sum(d_active * normed, 0)
    d_normed = d_active * norm_gain[None, :]
    sum_first, sum_second = in_one((jnp.sum(d_normed, 1), jnp.sum(d_normed * normed, 1)), "tp")
    total_channels = channels * lax.axis_size("tp")
    first = sum_first / total_channels
    second = sum_second / total_channels
    d_conv = row_scale[:, None] * (d_normed - first[:, None] - normed * second[:, None])
    taps_local = jnp.stack(
        [jnp.sum(d_conv * padded[offset : offset + length], 0) for offset in range(kernel)]
    )
    taps_grad, gain_grad = (over_axes(taps_local, SP), over_axes(gain_local, SP))
    spread = jnp.zeros((length + margin, channels), jnp.float32)
    for offset in range(kernel):
        placed = taps_wide[offset][None, :] * d_conv
        spread = spread + jnp.pad(placed, ((offset, margin - offset), (0, 0)))
    arrived = shifted(spread[:margin], SP, -1)
    tail_part = jnp.concatenate([jnp.zeros((length - margin, channels), jnp.float32), arrived], 0)
    d_gated = spread[margin:] + tail_part
    value_grad = (d_gated * gate_sig).astype(jnp.bfloat16)
    gate_grad = (d_gated * proj_value.astype(jnp.float32) * gate_sig * (1.0 - gate_sig)).astype(
        jnp.bfloat16
    )
    return (value_grad, gate_grad, weight_grad, taps_grad, gain_grad)


def solution(mesh):
    split = Mesh(mesh.devices.reshape(32, 4, 2, mesh.shape["tp"]), ("sp_0", "sp_1", "sp_2", "tp"))
    placed = (
        P(SP, "tp"),
        P(SP, "tp"),
        P(SP, None),
        P("tp", None),
        P(None, "tp"),
        P("tp"),
        P(SP),
        P(SP),
    )
    return jax.shard_map(
        shards,
        mesh=split,
        in_specs=placed,
        out_specs=(P(SP, "tp"), P(SP, "tp"), P(SP, "tp"), P(None, "tp"), P("tp")),
        check_vma=False,
    )
```

profile of v0, /device:TPU:7, one launch (start us, length us, event | category | flops | bytes accessed | tf_op | source)
XLA Modules:
  0.0 244.4 jit_solution(1409863044858874739)
XLA Ops:
  7.2 0.0 copy-start
  7.2 0.0 reduce-scatter.4.cloned.1.call-start
  7.2 1.2 fusion.1
  8.5 4.0 %collective-permute-start = (bf16[30,256]{1,0:T(8,128)(2,1)S(1)}, bf16[30,256]{1,0:T(8,128)(2,1)S(1)}, u32[]{:S(2)}, u32[]{:S(2)}) collective-permute-start(bf16[30,256]{1,0:T(8,128)(2,1)S(1)} %slice.331), channel_id=1, source_target_pairs={{0,4},{4,8},{8,12},{12,16},{16,20},{20,24},{24,28},{28,32},{32,36}... | collective-permute-start | bytes 46088 | tf_op jit(solution)/shard_map/ppermute | solution.py:13
  12.5 1.0 fusion.8
  13.5 1.0 fusion.9
  14.5 0.0 collective-permute-done
  14.6 0.0 copy-start.3
  14.6 1.8 subtract_multiply_fusion.1
  16.4 0.0 copy-done
  16.4 0.0 copy-done.3
  16.4 2.1 convolution_bitcast_fusion
  18.4 2.9 %copy.20 = f32[2048,256]{1,0:T(8,128)} copy(f32[2048,256]{0,1:T(8,128)} %convolution_bitcast_fusion) | data formatting | bytes 4194304 | tf_op jit(solution)/shard_map/dot_general | solution.py:84
  21.4 3.2 %copy.21 = f32[2,32,4,8,256]{4,3,2,1,0:T(8,128)} copy(f32[2,32,4,8,256]{4,3,0,2,1:T(8,128)} %bitcast.73) | data formatting | bytes 4194304 | tf_op jit(solution)/shard_map/transpose | solution.py:19
  24.6 0.0 reduce-scatter.4.cloned.1.call-update
  24.6 0.0 copy-start.4
  24.6 0.0 copy-start.5
  24.6 0.0 reduce-scatter.6.cloned.1.call-start
  24.7 2.0 multiply_reduce_fusion
  26.7 8.2 %all_to_all.6 = f32[4,1,768]{2,1,0:T(1,128)S(1)} all-to-all(f32[4,1,768]{2,1,0:T(1,128)S(1)} %broadcast_in_dim.2), channel_id=1, replica_groups=mesh['sp_0'=32,'sp_1'=4,'sp_2'=2,'tp'=4] {'tp'}, dimensions={0} | all-to-all | bytes 24576 | tf_op jit(solution)/shard_map/all_to_all | solution.py:38
  34.9 28.0 %reduce-scatter.4.cloned.1.call-done = f32[128,8,256]{2,1,0:T(8,128)} async-done(((f32[256,8,256]{2,1,0:T(8,128)}), f32[128,8,256]{2,1,0:T(8,128)}) %reduce-scatter.4.cloned.1.call-update) | async-done | bytes 1048592 | tf_op jit(solution)/shard_map/reduce_scatter | solution.py:21
  62.9 0.0 reduce-scatter.6.cloned.1.call-update
  63.0 0.0 reduce-scatter.8.cloned.1.call-start
  63.0 0.0 copy-done.4
  63.0 0.0 copy-done.5
  63.0 3.3 %multiply_reduce_fusion.1 = (f32[256]{0:T(256)S(1)}, f32[256]{0:T(256)S(1)}, f32[256]{0:T(256)S(1)}, f32[256]{0:T(256)S(1)}, f32[256]{0:T(256)S(1)}, /*index=5*/...) fusion(f32[414,256]{1,0:T(8,128)S(1)} %maximum_convert_fusion, ...), kind=kLoop, calls=%fused_computation.12 | loop fusion | flops 10219008 | bytes 13033472 | tf_op jit(solution)/shard_map/reduce_sum | solution.py:100
  66.4 0.3 broadcast_multiply_fusion.29
  66.7 0.6 multiply_reduce_fusion.19
  67.3 0.8 broadcast_multiply_fusion.30
  68.1 0.0 copy-start.1
  68.1 0.0 copy-start.2
  68.1 1.3 pad_add_fusion
  69.4 2.3 collective-permute-start.1
  71.7 0.1 stack.127
  71.8 87.2 %all-reduce.32 = (f32[31,256]{1,0:T(8,128)S(1)}, f32[256]{0:T(256)S(1)}) all-reduce(f32[31,256]{1,0:T(8,128)S(1)} %stack.127, f32[256]{0:T(256)S(1)} %get-tuple-element.36), channel_id=1, replica_groups=mesh['sp_0'=32,'sp_1'=4,'sp_2'=2,'tp'=4] {'sp_0'}, use_global_device_ids=true, to_apply=%region_37.0 | all-reduce | flops 8192 | bytes 65536 | tf_op jit(solution)/shard_map/psum | solution.py:57
  159.0 11.4 %all-reduce.33 = (f32[31,256]{1,0:T(8,128)S(1)}, f32[256]{0:T(256)S(1)}) all-reduce(f32[31,256]{1,0:T(8,128)S(1)} %get-tuple-element.39, f32[256]{0:T(256)S(1)} %get-tuple-element.40), channel_id=1, replica_groups=mesh['sp_0'=32,'sp_1'=4,'sp_2'=2,'tp'=4] {'sp_1'}, use_global_device_ids=true, to_apply=%region_38.0 | all-reduce | flops 8192 | bytes 65536 | tf_op jit(solution)/shard_map/psum | solution.py:57
  170.4 32.9 %all-reduce.34 = (f32[31,256]{1,0:T(8,128)}, f32[256]{0:T(256)}) all-reduce(f32[31,256]{1,0:T(8,128)S(1)} %get-tuple-element.41, f32[256]{0:T(256)S(1)} %get-tuple-element.42), channel_id=1, replica_groups=mesh['sp_0'=32,'sp_1'=4,'sp_2'=2,'tp'=4] {'sp_2'}, use_global_device_ids=true, to_apply=%region_39.0 | all-reduce | flops 8192 | bytes 65536 | tf_op jit(solution)/shard_map/psum | solution.py:57
  203.3 0.0 reduce-scatter.6.cloned.1.call-done
  203.3 0.0 reduce-scatter.8.cloned.1.call-update
  203.4 0.0 collective-permute-done.1
  203.4 0.0 copy-done.1
  203.4 0.0 copy-done.2
  203.4 0.9 fusion.4
  204.3 33.6 %reduce-scatter.8.cloned.1.call-done = f32[1,8,256]{2,1,0:T(8,128)} async-done(((f32[4,8,256]{2,1,0:T(8,128)}), f32[1,8,256]{2,1,0:T(8,128)}) %reduce-scatter.8.cloned.1.call-update) | async-done | bytes 8208 | tf_op jit(solution)/shard_map/reduce_scatter | solution.py:21
  (7 shorter events, 0.1 us)
Async XLA Ops:
  7.2 9.2 %copy-start = (bf16[384,2048]{1,0:T(8,128)(2,1)S(1)}, bf16[384,2048]{1,0:T(8,128)(2,1)}, u32[]{:S(2)}) copy-start(bf16[384,2048]{1,0:T(8,128)(2,1)} %param.10) | copy-start | bytes 4718596
  7.2 55.8 %reduce-scatter.4.cloned.1.call-start = ((), (), s32[]{:S(2)}) async-start(), calls=%async_computation.4 | async-start | bytes 3145728 | tf_op jit(solution)/shard_map/reduce_scatter | solution.py:21
  8.5 6.0 %collective-permute-start = (bf16[30,256]{1,0:T(8,128)(2,1)S(1)}, bf16[30,256]{1,0:T(8,128)(2,1)S(1)}, u32[]{:S(2)}, u32[]{:S(2)}) collective-permute-start(bf16[30,256]{1,0:T(8,128)(2,1)S(1)} %slice.331), channel_id=1, source_target_pairs={{0,4},{4,8},{8,12},{12,16},{16,20},{20,24},{24,28},{28,32},{32,36}... | collective-permute-start | bytes 46088 | tf_op jit(solution)/shard_map/ppermute | solution.py:13
  14.6 1.8 copy-start.3
  24.6 38.4 %copy-start.4 = (f32[384]{0:T(512)S(1)}, f32[384]{0:T(512)}, u32[]{:S(2)}) copy-start(f32[384]{0:T(512)} %param.14) | copy-start | bytes 4612
  24.6 38.4 %copy-start.5 = (f32[384]{0:T(512)S(1)}, f32[384]{0:T(512)}, u32[]{:S(2)}) copy-start(f32[384]{0:T(512)} %param.15) | copy-start | bytes 4612
  24.6 178.7 %reduce-scatter.6.cloned.1.call-start = ((), (), s32[]{:S(2)}) async-start(), calls=%async_computation.5 | async-start | bytes 1081344 | tf_op jit(solution)/shard_map/reduce_scatter | solution.py:21
  63.0 174.9 %reduce-scatter.8.cloned.1.call-start = ((), (), s32[]{:S(2)}) async-start(), calls=%async_computation.6 | async-start | bytes 40960 | tf_op jit(solution)/shard_map/reduce_scatter | solution.py:21
  68.1 135.3 %copy-start.1 = (bf16[384,256]{1,0:T(8,128)(2,1)S(1)}, bf16[384,256]{1,0:T(8,128)(2,1)}, u32[]{:S(2)}) copy-start(bf16[384,256]{1,0:T(8,128)(2,1)} %param.8) | copy-start | bytes 589828
  68.1 135.3 %copy-start.2 = (bf16[384,256]{1,0:T(8,128)(2,1)S(1)}, bf16[384,256]{1,0:T(8,128)(2,1)}, u32[]{:S(2)}) copy-start(bf16[384,256]{1,0:T(8,128)(2,1)} %param.9) | copy-start | bytes 589828
  69.4 134.0 %collective-permute-start.1 = (f32[30,256]{1,0:T(8,128)S(1)}, f32[30,256]{1,0:T(8,128)S(1)}, u32[]{:S(2)}, u32[]{:S(2)}) collective-permute-start(f32[30,256]{1,0:T(8,128)S(1)} %slice.394), channel_id=1, source_target_pairs={{4,0},{8,4},{12,8},{16,12},{20,16},{24,20},{28,24},{32,28},{36,32}... | collective-permute-start | bytes 92168 | tf_op jit(solution)/shard_map/ppermute | solution.py:13
Sparse Core Ops, SparseCore 0:
  24.7 38.1 reduce-scatter.3
  66.3 115.3 reduce-scatter.5
  203.5 34.3 reduce-scatter.7
where the time goes:
time: 249 us; the launch traced here: 244 us
  blocking collectives  140 us (56%)
  waiting for transfers between devices  61.7 us (25%)
  between operations  14 us (6%)
  other arithmetic  10.3 us (4%)
  local copies, waits for them, and re-layouts  8.29 us (3%)
  starting transfers between devices  6.39 us (3%)
  matrix products  4.08 us (2%)
    psum x3, blocking collectives, over_axes(): array = lax.psum(array, axis)  132 us
    reduce_scatter x3, waiting for transfers between devices, own_block(): parts = lax.psum_scatter(parts, axes[k], scatter_dimension=0, tiled=True)  61.6 us
    all_to_all x1, blocking collectives, from_everyone(): lax.all_to_all(jnp.broadcast_to(array[None], (devices, *array.shape)), ax...  8.18 us
    ppermute x2, starting transfers between devices, shifted(): lax.ppermute(value, axis, [(source, source + steps) for source in range(f...  6.28 us
  transfers between devices with their start and end apart: 5, of which 2 were waited for; matrix products, arithmetic and copies ran while one was open for 5% of the time, Pallas kernels for 0%

commit v1 on v0

v1 whole, which is shorter than its diff:
```python
import jax
import jax.numpy as jnp
from jax import lax
from jax.sharding import Mesh
from jax.sharding import PartitionSpec as P

SP = ("zh", "zl", "x", "c")
NEAR = ("zl", "x")
AXES = (("zh", 16), ("zl", 2), ("x", 4), ("c", 2))


def shifted(value, axis, steps):
    count = lax.axis_size(axis)
    first, last = (max(0, -steps), min(count, count - steps))
    return lax.ppermute(value, axis, [(source, source + steps) for source in range(first, last)])


def halves(value):
    high = lax.reduce_precision(value, 8, 7)
    return high.astype(jnp.bfloat16), (value - high).astype(jnp.bfloat16)


def exchange(pieces, axes):
    return lax.all_to_all(pieces, axes, 0, 0, tiled=True)


def shards(
    proj_value, proj_gate, out_cotangent, out_weight, conv_taps, norm_gain, row_mean, row_scale
):
    kernel = conv_taps.shape[0]
    margin = kernel - 1
    length = proj_value.shape[0]
    channels = proj_value.shape[1]
    near = lax.axis_size(NEAR)
    far = lax.axis_size("zh")
    wide = jnp.float32
    gate_sig = jax.nn.sigmoid(proj_gate.astype(wide))
    gated = (proj_value.astype(wide) * gate_sig).astype(jnp.bfloat16)
    before = shifted(gated[length - margin :], SP, 1)
    padded = jnp.concatenate([before, gated], 0).astype(wide)
    taps_wide = conv_taps.astype(wide)
    conv = jnp.zeros((length, channels), wide)
    for offset in range(kernel):
        conv = conv + taps_wide[offset][None, :] * padded[offset : offset + length]
    normed = (conv - row_mean[:, None]) * row_scale[:, None]
    active = normed * norm_gain[None, :]
    sig_act = jax.nn.sigmoid(active)
    hidden = (active * sig_act).astype(jnp.bfloat16)
    upstream = lax.dot_general(
        out_cotangent, out_weight, (((1,), (1,)), ((), ())), preferred_element_type=wide
    )
    d_active = upstream * sig_act * (1.0 + active * (1.0 - sig_act))
    gain_local = jnp.sum(d_active * normed, 0)
    d_normed = d_active * norm_gain[None, :]
    sums = jnp.stack([jnp.sum(d_normed, 1), jnp.sum(d_normed * normed, 1)])
    tp = lax.axis_size("tp")
    sums = exchange(jnp.broadcast_to(sums[None], (tp, *sums.shape)), "tp").sum(0)
    first, second = sums / (channels * tp)

    weight_part = lax.dot_general(
        out_cotangent, hidden, (((0,), (0,)), ((), ())), preferred_element_type=wide
    )
    model = weight_part.shape[0]
    own = model // (near * far * 2)
    core = lax.axis_index("c")
    by_core = weight_part.reshape(far * near, 2, own, channels)
    mine = lax.dynamic_index_in_dim(by_core, core, 1, keepdims=False)
    other = lax.dynamic_index_in_dim(by_core, 1 - core, 1, keepdims=False)
    other = lax.ppermute(other.astype(jnp.bfloat16), "c", [(0, 1), (1, 0)])
    chip = (mine + other.astype(wide)).astype(jnp.bfloat16)
    chip = chip.reshape(far, near, own, channels).transpose(1, 0, 2, 3)
    chip = chip.reshape(near, far * own, channels)

    d_conv = row_scale[:, None] * (d_normed - first[:, None] - normed * second[:, None])
    small = jnp.stack(
        [jnp.sum(d_conv * padded[offset : offset + length], 0) for offset in range(kernel)]
        + [gain_local]
    )
    rows = small.shape[0] // near
    small = small.reshape(near, rows, channels)
    arrived = exchange(jnp.concatenate([chip, *halves(small)], 1), NEAR).astype(wide).sum(0)
    chip, small = arrived[: far * own], arrived[far * own :]
    small = jnp.concatenate(halves(small[:rows] + small[rows:]), 0)
    pieces = jnp.concatenate(
        [
            chip.astype(jnp.bfloat16).reshape(far, own, channels),
            jnp.broadcast_to(small[None], (far, *small.shape)),
        ],
        1,
    )
    arrived = exchange(pieces, "zh").astype(wide).sum(0)
    weight_grad, small = arrived[:own], arrived[own:]
    small = small[:rows] + small[rows:]
    small = exchange(
        jnp.broadcast_to(small[None], (near * 2, *small.shape)), (*NEAR, "c")
    ).reshape(near, 2, rows, channels)
    small = small.sum(1).reshape(near * rows, channels)
    taps_grad, gain_grad = small[:kernel], small[kernel]

    spread = jnp.zeros((length + margin, channels), wide)
    for offset in range(kernel):
        placed = taps_wide[offset][None, :] * d_conv
        spread = spread + jnp.pad(placed, ((offset, margin - offset), (0, 0)))
    arrived = shifted(spread[:margin], SP, -1)
    tail_part = jnp.concatenate([jnp.zeros((length - margin, channels), wide), arrived], 0)
    d_gated = spread[margin:] + tail_part
    value_grad = (d_gated * gate_sig).astype(jnp.bfloat16)
    gate_grad = (d_gated * proj_value.astype(wide) * gate_sig * (1.0 - gate_sig)).astype(
        jnp.bfloat16
    )
    return (value_grad, gate_grad, weight_grad, taps_grad, gain_grad)


def solution(mesh):
    sizes = [size for _, size in AXES]
    split = Mesh(mesh.devices.reshape(*sizes, mesh.shape["tp"]), (*SP, "tp"))
    placed = (
        P(SP, "tp"),
        P(SP, "tp"),
        P(SP, None),
        P("tp", None),
        P(None, "tp"),
        P("tp"),
        P(SP),
        P(SP),
    )
    return jax.shard_map(
        shards,
        mesh=split,
        in_specs=placed,
        out_specs=(P(SP, "tp"), P(SP, "tp"), P(SP, "tp"), P(None, "tp"), P("tp")),
        check_vma=False,
    )
```

time: 249 us -> 126 us (0.51)
  blocking collectives: 140 us -> 20.8 us
  starting transfers between devices: 6.39 us -> 44.7 us
  waiting for transfers between devices: 61.7 us -> 24.8 us
  between operations: 14 us -> 0.99 us
  other arithmetic: 10.3 us -> 18 us
  local copies, waits for them, and re-layouts: 8.29 us -> 11.3 us
    psum x3 -> x0, blocking collectives: 132 us -> none  [over_axes(): array = lax.psum(array, axis)]
    reduce_scatter x3 -> x0, waiting for transfers between devices: 61.6 us -> none  [own_block(): parts = lax.psum_scatter(parts, axes[k], scatter_dimension=0, tiled=True)]
    all_to_all x0 -> x3, starting transfers between devices: none -> 36.5 us  [exchange(): return lax.all_to_all(pieces, axes, 0, 0, tiled=True)]
    all_to_all x0 -> x3, waiting for transfers between devices: none -> 19.8 us  [exchange(): return lax.all_to_all(pieces, axes, 0, 0, tiled=True)]
    all_to_all x1, blocking collectives: 8.18 us -> 20.8 us  [exchange(): return lax.all_to_all(pieces, axes, 0, 0, tiled=True)]
    ppermute x2, waiting for transfers between devices: 0.01 us -> 5.04 us  [shifted(): lax.ppermute(value, axis, [(source, source + steps) for source in range(f...]
    transpose x1 -> x0, local copies, waits for them, and re-layouts: 3.2 us -> none  [own_block(): parts = jnp.moveaxis(parts, sequence, range(len(axes))).reshape(-1, *inside)]
  transfers between devices with their start and end apart: 5 -> 6, of which waited for: 2 -> 2; matrix products, arithmetic and copies ran while one was open for 5% -> 16% of each run, Pallas kernels for 0% -> 0%
where the time goes in v1:
time: 126 us; the launch traced here: 123 us
  starting transfers between devices  44.7 us (35%)
  waiting for transfers between devices  24.8 us (20%)
  blocking collectives  20.8 us (17%)
  other arithmetic  18 us (14%)
  local copies, waits for them, and re-layouts  11.3 us (9%)
  matrix products  2.83 us (2%)
    all_to_all x3, starting transfers between devices, exchange(): return lax.all_to_all(pieces, axes, 0, 0, tiled=True)  36.5 us
    all_to_all x1, blocking collectives, exchange(): return lax.all_to_all(pieces, axes, 0, 0, tiled=True)  20.8 us
    all_to_all x3, waiting for transfers between devices, exchange(): return lax.all_to_all(pieces, axes, 0, 0, tiled=True)  19.8 us
    ppermute x2, starting transfers between devices, shifted(): lax.ppermute(value, axis, [(source, source + steps) for source in range(f...  6.32 us
    ppermute x2, waiting for transfers between devices, shifted(): lax.ppermute(value, axis, [(source, source + steps) for source in range(f...  5.04 us
    reduce_sum x2, other arithmetic, shards(): jnp.sum(d_conv * padded[offset:offset + length], 0)  4.77 us
    add x1, other arithmetic, shards(): spread = spread + jnp.pad(placed, ((offset, margin - offset), (0, 0)))  3.62 us
    mul x2, other arithmetic, shards(): placed = taps_wide[offset][None, :] * d_conv  3.2 us
  transfers between devices with their start and end apart: 6, of which 2 were waited for; matrix products, arithmetic and copies ran while one was open for 16% of the time, Pallas kernels for 0%

profile of v1, /device:TPU:7, one launch (start us, length us, event | category | flops | bytes accessed | tf_op | source)
XLA Modules:
  0.0 123.5 jit_solution(10410503341039358684)
XLA Ops:
  0.6 0.0 copy-start
  0.6 1.3 %fusion.3 = bf16[384,256]{1,0:T(8,128)(2,1)S(1)} fusion(bf16[384,256]{1,0:T(8,128)(2,1)} %param.8, bf16[384,256]{1,0:T(8,128)(2,1)} %param.9), kind=kLoop, calls=%fused_computation.13 | loop fusion | flops 688128 | bytes 589824 | tf_op jit(solution)/shard_map/convert_element_type | solution.py:38
  1.9 4.0 %collective-permute-start = (bf16[30,256]{1,0:T(8,128)(2,1)S(1)}, bf16[30,256]{1,0:T(8,128)(2,1)S(1)}, u32[]{:S(2)}, u32[]{:S(2)}) collective-permute-start(bf16[30,256]{1,0:T(8,128)(2,1)S(1)} %slice.362), channel_id=1, source_target_pairs={{0,4},{4,8},{8,12},{12,16},{16,20},{20,24},{24,28},{28,32},{32,36}... | collective-permute-start | bytes 46088 | tf_op jit(solution)/shard_map/ppermute | solution.py:15
  6.0 1.0 fusion.13
  7.0 1.0 fusion.14
  7.9 0.0 collective-permute-done
  8.0 0.0 copy-start.13
  8.0 1.8 %subtract_multiply_fusion.1 = f32[384,256]{1,0:T(8,128)S(1)} fusion(f32[414,256]{1,0:T(8,128)S(1)} %maximum_convert_fusion, f32[384]{0:T(512)} %param.14, f32[256]{0:T(256)S(1)} %bitcast.182, f32[256]{0:T(256)S(1)} %bitcast.179, f32[256]{0:T(256)S(1)} %bitcast.176, f32[256]{0:T(256)S(1)} %bitcast.173, f32[256]{0:T(256)S(1)} %bitcast.170, ...), kind=kLoop, calls=%fused_computation.55 | loop fusion | flops 6193152 | bytes 12617728 | tf_op jit(solution)/shard_map/mul | solution.py:45
  9.8 0.0 copy-done
  9.8 0.0 copy-done.13
  9.8 0.0 copy-start.16
  9.8 2.1 %convolution_bitcast_fusion = f32[2048,256]{0,1:T(8,128)} fusion(bf16[384,2048]{1,0:T(8,128)(2,1)S(1)} %copy-done, f32[384,256]{1,0:T(8,128)S(1)} %subtract_multiply_fusion.1, f32[256]{0:T(256)S(1)} %copy-done.13), kind=kOutput, calls=%fused_computation | convolution fusion | flops 403243008 | bytes 4064256 | tf_op jit(solution)/shard_map/dot_general | solution.py:60
  11.9 0.0 copy-done.16
  11.9 0.8 multiply_reduce_fusion
  12.7 0.6 broadcast_in_dim.6
  13.3 4.2 %all-to-all-start = ((f32[4,2,384]{2,1,0:T(2,128)}), f32[4,2,384]{2,1,0:T(2,128)S(1)}, u32[]{:S(2)}, u32[]{:S(2)}) async-start(f32[4,2,384]{2,1,0:T(2,128)} %broadcast_in_dim.6), calls=%async_computation | async-start | bytes 24576 | tf_op jit(solution)/shard_map/all_to_all | solution.py:24
  17.5 3.0 %copy.22 = f32[2048,256]{1,0:T(8,128)} copy(f32[2048,256]{0,1:T(8,128)} %convolution_bitcast_fusion) | data formatting | bytes 4194304 | tf_op jit(solution)/shard_map/dot_general | solution.py:60
  20.5 2.1 %fusion.2 = bf16[128,8,256]{2,1,0:T(8,128)(2,1)} fusion(f32[128,2,8,256]{3,2,1,0:T(8,128)} %bitcast.87, s32[]{:T(128)S(6)} %select_n.8), kind=kLoop, calls=%fused_computation.8 | loop fusion | bytes 1048580 | tf_op jit(solution)/shard_map/convert_element_type | solution.py:69
  22.5 1.9 %collective-permute-start.2 = (bf16[128,8,256]{2,1,0:T(8,128)(2,1)}, bf16[128,8,256]{2,1,0:T(8,128)(2,1)}, u32[]{:S(2)}, u32[]{:S(2)}) collective-permute-start(bf16[128,8,256]{2,1,0:T(8,128)(2,1)} %fusion.2), channel_id=1, source_target_pairs={{0,4},{4,0},{1,5},{5,1},{2,6},{6,2},{3,7},{7,3},{8,12},{12,8},{9,1... | collective-permute-start | bytes 1572872 | tf_op jit(solution)/shard_map/ppermute | solution.py:69
  24.5 0.0 all-to-all-done
  24.5 0.0 copy-done.14
  24.5 0.0 copy-done.15
  24.6 3.3 %multiply_reduce_fusion.1 = (f32[256]{0:T(256)S(1)}, f32[256]{0:T(256)S(1)}, f32[256]{0:T(256)S(1)}, f32[256]{0:T(256)S(1)}, f32[256]{0:T(256)S(1)}, /*index=5*/...) fusion(f32[414,256]{1,0:T(8,128)S(1)} %maximum_convert_fusion, ...), kind=kLoop, calls=%fused_computation.19 | loop fusion | flops 10219008 | bytes 13033472 | tf_op jit(solution)/shard_map/reduce_sum | solution.py:76
  27.8 1.5 %multiply_reduce_fusion.19 = (f32[256]{0:T(256)S(1)}, f32[256]{0:T(256)S(1)}, f32[256]{0:T(256)S(1)}, f32[256]{0:T(256)S(1)}, f32[256]{0:T(256)S(1)}, /*index=5*...) fusion(f32[384,256]{1,0:T(8,128)S(1)} %get-tuple-element.41, ...), kind=kLoop, calls=%fused_computation.37 | loop fusion | flops 3044096 | bytes 7489536 | tf_op jit(solution)/shard_map/reduce_sum | solution.py:76
  29.3 0.1 stack.143
  29.5 0.0 collective-permute-done.2
  29.5 1.5 %fusion.1 = bf16[128,8,256]{2,1,0:T(8,128)(2,1)S(1)} fusion(bf16[128,8,256]{2,1,0:T(8,128)(2,1)} %collective-permute-done.2, f32[128,2,8,256]{3,2,1,0:T(8,128)} %bitcast.88, s32[]{:T(128)S(6)} %select_n.7), kind=kLoop, calls=%fused_computation.5 | loop fusion | flops 786432 | bytes 2097156 | tf_op jit(solution)/shard_map/convert_element_type | solution.py:70
  31.1 20.8 %all_to_all.20 = bf16[8,136,256]{2,1,0:T(8,128)(2,1)S(1)} all-to-all(bf16[8,136,256]{2,1,0:T(8,128)(2,1)S(1)} %pad_maximum_fusion), channel_id=1, replica_groups=mesh['zh'=16,'zl'=2,'x'=4,'c'=2,'tp'=4] {'zl','x'}, dimensions={0} | all-to-all | bytes 1114112 | tf_op jit(solution)/shard_map/all_to_all | solution.py:24
  51.9 0.1 convert_reduce_fusion
  52.0 0.7 pad_maximum_fusion.1
  52.7 21.8 %all-to-all-start.2 = ((bf16[16,16,256]{2,1,0:T(8,128)(2,1)}), bf16[16,16,256]{2,1,0:T(8,128)(2,1)S(1)}, u32[]{:S(2)}, u32[]{:S(2)}) async-start(bf16[16,16,256]{2,1,0:T(8,128)(2,1)} %pad_maximum_fusion.1), calls=%async_computation.2 | async-start | bytes 262144 | tf_op jit(solution)/shard_map/all_to_all | solution.py:24
  74.5 2.9 %broadcast_multiply_fusion.30 = (f32[384,256]{1,0:T(8,128)}, f32[384,256]{1,0:T(8,128)}, f32[384,256]{1,0:T(8,128)}, f32[384,256]{1,0:T(8,128)}, f32[384,256]{1,...) fusion(f32[384,256]{1,0:T(8,128)S(1)} %get-tuple-element.41, ...), kind=kLoop, calls=%fused_computation.92 | loop fusion | flops 1769472 | bytes 7489536 | tf_op jit(solution)/shard_map/mul | solution.py:102
  77.4 19.8 %all-to-all-done.2 = bf16[16,16,256]{2,1,0:T(8,128)(2,1)S(1)} async-done(((bf16[16,16,256]{2,1,0:T(8,128)(2,1)}), bf16[16,16,256]{2,1,0:T(8,128)(2,1)S(1)}, u32[]{:S(2)}, u32[]{:S(2)}) %all-to-all-start.2) | async-done | bytes 131104 | tf_op jit(solution)/shard_map/all_to_all | solution.py:24
  97.3 0.6 broadcast_in_dim.8
  97.9 10.5 %all-to-all-start.3 = ((f32[16,4,256]{2,1,0:T(4,128)}), f32[16,4,256]{2,1,0:T(4,128)S(1)}, u32[]{:S(2)}, u32[]{:S(2)}) async-start(f32[16,4,256]{2,1,0:T(4,128)} %broadcast_in_dim.8), calls=%async_computation.3 | async-start | bytes 131072 | tf_op jit(solution)/shard_map/all_to_all | solution.py:24
  108.3 0.0 copy-start.2
  108.4 0.0 copy-start.3
  108.4 0.0 copy-start.4
  108.4 0.0 copy-start.5
  108.4 0.0 copy-start.6
  108.4 0.0 copy-start.7
  108.4 0.0 copy-start.8
  108.4 0.0 copy-start.9
  108.4 0.3 broadcast_multiply_fusion.29
  108.7 0.6 copy-done.1
  109.3 0.1 copy-done.2
  109.5 0.1 copy-done.3
  109.6 0.1 copy-done.4
  109.7 0.1 copy-done.5
  109.8 0.1 copy-done.6
  109.9 0.1 copy-done.7
  110.1 0.1 copy-done.8
  110.2 0.1 copy-done.9
  110.3 3.6 %pad_add_fusion = f32[414,256]{1,0:T(8,128)S(1)} fusion(f32[384,256]{1,0:T(8,128)S(1)} %get-tuple-element.44, f32[384,256]{1,0:T(8,128)S(1)} %get-tuple-element.45, f32[384,256]{1,0:T(8,128)S(1)} %copy-done.1, f32[384,256]{1,0:T(8,128)S(1)} %copy-done.2, f32[384,256]{1,0:T(8,128)S(1)} %copy-done.3, f32[384,256]{1,0:T(8,128)S(1)} %copy-done.5, ...), kind=kLoop, calls=%fused_computation.12 | loop fusion | flops 3179520 | bytes 12613632 | tf_op jit(solution)/shard_map/add | solution.py:103
  113.9 2.3 %collective-permute-start.1 = (f32[30,256]{1,0:T(8,128)S(1)}, f32[30,256]{1,0:T(8,128)S(1)}, u32[]{:S(2)}, u32[]{:S(2)}) collective-permute-start(f32[30,256]{1,0:T(8,128)S(1)} %slice.425), channel_id=1, source_target_pairs={{4,0},{8,4},{12,8},{16,12},{20,16},{24,20},{28,24},{32,28},{36,32}... | collective-permute-start | bytes 92168 | tf_op jit(solution)/shard_map/ppermute | solution.py:15
  116.2 5.0 %collective-permute-done.1 = f32[30,256]{1,0:T(8,128)S(1)} collective-permute-done((f32[30,256]{1,0:T(8,128)S(1)}, f32[30,256]{1,0:T(8,128)S(1)}, u32[]{:S(2)}, u32[]{:S(2)}) %collective-permute-start.1) | collective-permute-done | bytes 30752 | tf_op jit(solution)/shard_map/ppermute | solution.py:15
  121.3 0.0 copy-done.10
  121.3 0.0 copy-done.11
  121.3 0.9 fusion.6
  122.2 0.6 slice.429
  122.8 0.0 all-to-all-done.3
  122.9 0.0 copy-start.12
  122.9 0.6 slice.433
  123.5 0.0 copy-done.12
  (26 shorter events, 0.3 us)
Async XLA Ops:
  0.6 9.2 %copy-start = (bf16[384,2048]{1,0:T(8,128)(2,1)S(1)}, bf16[384,2048]{1,0:T(8,128)(2,1)}, u32[]{:S(2)}) copy-start(bf16[384,2048]{1,0:T(8,128)(2,1)} %param.10) | copy-start | bytes 4718596
  1.9 6.0 %collective-permute-start = (bf16[30,256]{1,0:T(8,128)(2,1)S(1)}, bf16[30,256]{1,0:T(8,128)(2,1)S(1)}, u32[]{:S(2)}, u32[]{:S(2)}) collective-permute-start(bf16[30,256]{1,0:T(8,128)(2,1)S(1)} %slice.362), channel_id=1, source_target_pairs={{0,4},{4,8},{8,12},{12,16},{16,20},{20,24},{24,28},{28,32},{32,36}... | collective-permute-start | bytes 46088 | tf_op jit(solution)/shard_map/ppermute | solution.py:15
  8.0 1.8 %copy-start.13 = (f32[256]{0:T(256)S(1)}, f32[256]{0:T(256)}, u32[]{:S(2)}) copy-start(f32[256]{0:T(256)} %param.13) | copy-start | bytes 3076
  9.8 2.1 %copy-start.16 = (bf16[256,2048]{1,0:T(8,128)(2,1)S(1)}, bf16[256,2048]{1,0:T(8,128)(2,1)}, u32[]{:S(2)}) copy-start(bf16[256,2048]{1,0:T(8,128)(2,1)} %param.11) | copy-start | bytes 3145732
  13.3 11.2 %all-to-all-start = ((f32[4,2,384]{2,1,0:T(2,128)}), f32[4,2,384]{2,1,0:T(2,128)S(1)}, u32[]{:S(2)}, u32[]{:S(2)}) async-start(f32[4,2,384]{2,1,0:T(2,128)} %broadcast_in_dim.6), calls=%async_computation | async-start | bytes 24576 | tf_op jit(solution)/shard_map/all_to_all | solution.py:24
  17.5 7.0 %copy-start.14 = (f32[384]{0:T(512)S(1)}, f32[384]{0:T(512)}, u32[]{:S(2)}) copy-start(f32[384]{0:T(512)} %param.14) | copy-start | bytes 4612
  17.5 7.1 %copy-start.15 = (f32[384]{0:T(512)S(1)}, f32[384]{0:T(512)}, u32[]{:S(2)}) copy-start(f32[384]{0:T(512)} %param.15) | copy-start | bytes 4612
  22.5 6.9 %collective-permute-start.2 = (bf16[128,8,256]{2,1,0:T(8,128)(2,1)}, bf16[128,8,256]{2,1,0:T(8,128)(2,1)}, u32[]{:S(2)}, u32[]{:S(2)}) collective-permute-start(bf16[128,8,256]{2,1,0:T(8,128)(2,1)} %fusion.2), channel_id=1, source_target_pairs={{0,4},{4,0},{1,5},{5,1},{2,6},{6,2},{3,7},{7,3},{8,12},{12,8},{9,1... | collective-permute-start | bytes 1572872 | tf_op jit(solution)/shard_map/ppermute | solution.py:69
  52.7 44.5 %all-to-all-start.2 = ((bf16[16,16,256]{2,1,0:T(8,128)(2,1)}), bf16[16,16,256]{2,1,0:T(8,128)(2,1)S(1)}, u32[]{:S(2)}, u32[]{:S(2)}) async-start(bf16[16,16,256]{2,1,0:T(8,128)(2,1)} %pad_maximum_fusion.1), calls=%async_computation.2 | async-start | bytes 262144 | tf_op jit(solution)/shard_map/all_to_all | solution.py:24
  97.9 24.9 %all-to-all-start.3 = ((f32[16,4,256]{2,1,0:T(4,128)}), f32[16,4,256]{2,1,0:T(4,128)S(1)}, u32[]{:S(2)}, u32[]{:S(2)}) async-start(f32[16,4,256]{2,1,0:T(4,128)} %broadcast_in_dim.8), calls=%async_computation.3 | async-start | bytes 131072 | tf_op jit(solution)/shard_map/all_to_all | solution.py:24
  108.3 1.0 copy-start.1
  108.3 1.1 copy-start.2
  108.4 1.2 copy-start.3
  108.4 1.3 %copy-start.4 = (f32[384,256]{1,0:T(8,128)S(1)}, f32[384,256]{1,0:T(8,128)}, u32[]{:S(2)}) copy-start(f32[384,256]{1,0:T(8,128)} %get-tuple-element.49) | copy-start | bytes 1179652
  108.4 1.4 %copy-start.5 = (f32[384,256]{1,0:T(8,128)S(1)}, f32[384,256]{1,0:T(8,128)}, u32[]{:S(2)}) copy-start(f32[384,256]{1,0:T(8,128)} %get-tuple-element.50) | copy-start | bytes 1179652
  108.4 1.6 %copy-start.6 = (f32[384,256]{1,0:T(8,128)S(1)}, f32[384,256]{1,0:T(8,128)}, u32[]{:S(2)}) copy-start(f32[384,256]{1,0:T(8,128)} %get-tuple-element.51) | copy-start | bytes 1179652
  108.4 1.7 %copy-start.7 = (f32[384,256]{1,0:T(8,128)S(1)}, f32[384,256]{1,0:T(8,128)}, u32[]{:S(2)}) copy-start(f32[384,256]{1,0:T(8,128)} %get-tuple-element.52) | copy-start | bytes 1179652
  108.4 1.8 %copy-start.8 = (f32[384,256]{1,0:T(8,128)S(1)}, f32[384,256]{1,0:T(8,128)}, u32[]{:S(2)}) copy-start(f32[384,256]{1,0:T(8,128)} %get-tuple-element.53) | copy-start | bytes 1179652
  108.4 1.9 %copy-start.9 = (f32[384,256]{1,0:T(8,128)S(1)}, f32[384,256]{1,0:T(8,128)}, u32[]{:S(2)}) copy-start(f32[384,256]{1,0:T(8,128)} %get-tuple-element.54) | copy-start | bytes 1179652
  110.3 11.0 %copy-start.10 = (bf16[384,256]{1,0:T(8,128)(2,1)S(1)}, bf16[384,256]{1,0:T(8,128)(2,1)}, u32[]{:S(2)}) copy-start(bf16[384,256]{1,0:T(8,128)(2,1)} %param.8) | copy-start | bytes 589828
  110.3 11.0 %copy-start.11 = (bf16[384,256]{1,0:T(8,128)(2,1)S(1)}, bf16[384,256]{1,0:T(8,128)(2,1)}, u32[]{:S(2)}) copy-start(bf16[384,256]{1,0:T(8,128)(2,1)} %param.9) | copy-start | bytes 589828
  113.9 7.3 %collective-permute-start.1 = (f32[30,256]{1,0:T(8,128)S(1)}, f32[30,256]{1,0:T(8,128)S(1)}, u32[]{:S(2)}, u32[]{:S(2)}) collective-permute-start(f32[30,256]{1,0:T(8,128)S(1)} %slice.425), channel_id=1, source_target_pairs={{4,0},{8,4},{12,8},{16,12},{20,16},{24,20},{28,24},{32,28},{36,32}... | collective-permute-start | bytes 92168 | tf_op jit(solution)/shard_map/ppermute | solution.py:15
  122.9 0.6 copy-start.12

commit v2 on v1

v2 whole, which is shorter than its diff:
```python
import functools

import jax
import jax.numpy as jnp
from jax import lax
from jax.experimental import pallas as pl
from jax.experimental.pallas import tpu as pltpu
from jax.sharding import Mesh
from jax.sharding import PartitionSpec as P

SP = ("zh", "zl", "x", "c")
NEAR = ("zl", "x")
FAR = 16
CLOSE = 8
AXES = (("zh", FAR), ("zl", 2), ("x", 4), ("c", 2))
TP = 4
TAPS = 31
ROWS = 384
EDGE = 32
LANES = 128
HALVES = 2
WIDTH = HALVES * LANES
MODEL = 2048
OWN = 8
CHUNK = 64
WIDE = jnp.float32
NARROW = jnp.bfloat16


def shifted(value, axis, steps):
    count = lax.axis_size(axis)
    first, last = (max(0, -steps), min(count, count - steps))
    return lax.ppermute(value, axis, [(source, source + steps) for source in range(first, last)])


def exchange(pieces, axes):
    return lax.all_to_all(pieces, axes, 0, 0, tiled=True)


def lanes(half):
    return slice(half * LANES, (half + 1) * LANES)


def column(row):
    return jnp.transpose(jnp.broadcast_to(row, (LANES, LANES)))


def call(body, outs, *args, flops=0, limit=24):
    shapes = [jax.ShapeDtypeStruct(shape, dtype) for shape, dtype in outs]
    size = sum(a.size * a.dtype.itemsize for a in (*args, *shapes))
    return pl.pallas_call(
        body,
        out_shape=shapes,
        compiler_params=pltpu.CompilerParams(vmem_limit_bytes=limit << 20),
        cost_estimate=pl.CostEstimate(flops=flops, bytes_accessed=size, transcendentals=0),
        name=body.__name__,
    )(*args)


def gate_and_upstream(value, gate, cotangent, weight, body, upstream):
    for start in range(0, ROWS, CHUNK):
        rows = slice(start, start + CHUNK)
        for half in range(HALVES):
            sig = jax.nn.sigmoid(gate[rows, lanes(half)].astype(WIDE))
            gated = (value[rows, lanes(half)].astype(WIDE) * sig).astype(NARROW)
            body[half, rows, :] = gated.astype(WIDE)
    product = lax.dot_general(
        cotangent[...], weight[...], (((1,), (1,)), ((), ())), preferred_element_type=WIDE
    )
    for half in range(HALVES):
        upstream[half] = product[:, lanes(half)]


def forward(
    halo, body, upstream, taps, gain, mean, scale,
    padded, scaled, spread, hidden, message, gain_part,
    taps_wide, mean_columns, scale_columns, sum_first, sum_second,
):
    taps_wide[0:TAPS] = taps[...].astype(WIDE)
    for block in range(ROWS // LANES):
        rows = slice(block * LANES, (block + 1) * LANES)
        mean_columns[rows] = column(mean[rows].reshape(1, LANES))
        scale_columns[rows] = column(scale[rows].reshape(1, LANES))
    for half in range(HALVES):
        padded[half, 0:EDGE] = halo[:, lanes(half)].astype(WIDE)
        padded[half, EDGE:] = body[half]
    for half in range(HALVES):
        gain_row = gain[0:1, lanes(half)]
        gain_sum = jnp.zeros((8, LANES), WIDE)
        for start in range(0, ROWS, CHUNK):
            rows = slice(start, start + CHUNK)
            conv = jnp.zeros((CHUNK, LANES), WIDE)
            for tap in range(TAPS):
                begin = start + tap + EDGE - TAPS + 1
                conv = conv + taps_wide[tap : tap + 1, lanes(half)] * padded[half, begin : begin + CHUNK]
            factor = scale_columns[rows]
            normed = (conv - mean_columns[rows]) * factor
            active = normed * gain_row
            sig = jax.nn.sigmoid(active)
            hidden[rows, lanes(half)] = (active * sig).astype(NARROW)
            d_active = upstream[half, rows] * sig * (1.0 + active * (1.0 - sig))
            gain_sum = gain_sum + jnp.sum((d_active * normed).reshape(CHUNK // 8, 8, LANES), 0)
            d_normed = d_active * gain_row
            scaled[half, rows] = factor * d_normed
            spread[half, rows] = factor * normed
            weighted = d_normed * normed
            if half == 0:
                sum_first[rows] = d_normed
                sum_second[rows] = weighted
            else:
                sum_first[rows] = sum_first[rows] + d_normed
                sum_second[rows] = sum_second[rows] + weighted
        gain_part[half] = gain_sum
    found = []
    for source in (sum_first, sum_second):
        for block in range(ROWS // LANES):
            turned = jnp.transpose(source[block * LANES : (block + 1) * LANES])
            found.append(jnp.sum(turned, 0, keepdims=True))
    found.append(jnp.zeros((2, LANES), WIDE))
    sums = jnp.concatenate(found, 0)
    for peer in range(TP):
        message[peer] = sums


def weight_product(core, cotangent, hidden, mine, other):
    first = core[0] == 0
    for far in range(FAR):
        part = lax.dot_general(
            cotangent[:, lanes(far)], hidden[...], (((0,), (0,)), ((), ())),
            preferred_element_type=WIDE,
        )
        part = part.reshape(CLOSE, 2, OWN, WIDTH)
        low, high = part[:, 0], part[:, 1]
        mine[:, far] = jnp.where(first, low, high)
        other[:, far] = jnp.where(first, high, low).astype(NARROW)


def halves(value):
    high = value.astype(NARROW)
    return high, (value - high.astype(WIDE)).astype(NARROW)


def backward(
    sums, scaled, spread, padded, scale, gain_part, mine, other,
    pieces, extended,
    small,
):
    total = sums[0]
    for peer in range(1, TP):
        total = total + sums[peer]
    total = total * (1.0 / (TP * WIDTH))
    blocks = ROWS // LANES
    for half in range(HALVES):
        extended[half, 0:EDGE] = jnp.zeros((EDGE, LANES), WIDE)
        extended[half, EDGE + ROWS :] = jnp.zeros((EDGE, LANES), WIDE)
    for block in range(blocks):
        rows = slice(block * LANES, (block + 1) * LANES)
        first = column(total[block : block + 1] * scale[rows].reshape(1, LANES))
        second = column(total[blocks + block : blocks + block + 1])
        for half in range(HALVES):
            d_conv = scaled[half, rows] - first - spread[half, rows] * second
            extended[half, EDGE + block * LANES : EDGE + (block + 1) * LANES] = d_conv
    for half in range(HALVES):
        for group in range(0, TAPS, 8):
            members = range(group, min(group + 8, TAPS))
            found = [jnp.zeros((8, LANES), WIDE) for _ in members]
            for start in range(0, ROWS, 8):
                d_conv = extended[half, EDGE + start : EDGE + start + 8]
                for i, tap in enumerate(members):
                    begin = start + tap + EDGE - TAPS + 1
                    found[i] = found[i] + d_conv * padded[half, begin : begin + 8]
            for i, tap in enumerate(members):
                small[tap : tap + 1, lanes(half)] = jnp.sum(found[i], 0, keepdims=True)
        small[TAPS : TAPS + 1, lanes(half)] = jnp.sum(gain_part[half], 0, keepdims=True)
    for near in range(CLOSE):
        chip = mine[near] + other[near].astype(WIDE)
        pieces[near, 0 : FAR * OWN] = chip.reshape(FAR * OWN, WIDTH).astype(NARROW)
        high, low = halves(small[near * 4 : near * 4 + 4])
        pieces[near, FAR * OWN :] = jnp.concatenate([high.astype(WIDE), low.astype(WIDE)], 0).astype(NARROW)


def gated_gradient(extended, taps, d_gated, margin, taps_wide):
    taps_wide[0:TAPS] = taps[...].astype(WIDE)
    for half in range(HALVES):
        for start in range(0, EDGE + ROWS, EDGE):
            found = jnp.zeros((EDGE, LANES), WIDE)
            for tap in range(TAPS):
                begin = start + TAPS - 1 - tap
                found = found + taps_wide[tap : tap + 1, lanes(half)] * extended[half, begin : begin + EDGE]
            if start == 0:
                margin[half] = found
            else:
                d_gated[half, start - EDGE : start] = found


def outputs(d_gated, arrived, value, gate, value_grad, gate_grad):
    for half in range(HALVES):
        for start in range(0, ROWS, EDGE):
            rows = slice(start, start + EDGE)
            grad = d_gated[half, rows]
            if start == ROWS - EDGE:
                grad = grad + arrived[half]
            sig = jax.nn.sigmoid(gate[rows, lanes(half)].astype(WIDE))
            wide = value[rows, lanes(half)].astype(WIDE)
            value_grad[rows, lanes(half)] = (grad * sig).astype(NARROW)
            gate_grad[rows, lanes(half)] = (grad * wide * sig * (1.0 - sig)).astype(NARROW)


def fold_near(arrived, pieces):
    for far in range(FAR):
        rows = slice(far * OWN, (far + 1) * OWN)
        total = arrived[0, rows].astype(WIDE)
        for near in range(1, CLOSE):
            total = total + arrived[near, rows].astype(WIDE)
        pieces[far, :, 0:WIDTH] = total.astype(NARROW)
    both = arrived[0, FAR * OWN :].astype(WIDE)
    for near in range(1, CLOSE):
        both = both + arrived[near, FAR * OWN :].astype(WIDE)
    small = both[0:4] + both[4:8]
    small = jnp.concatenate([small[:, lanes(0)], small[:, lanes(1)]], 0).astype(NARROW)
    for far in range(FAR):
        pieces[far, :, WIDTH:] = small


def fold_far(arrived, weight_grad, message):
    total = arrived[0].astype(WIDE)
    for far in range(1, FAR):
        total = total + arrived[far].astype(WIDE)
    weight_grad[...] = total[:, 0:WIDTH]
    for peer in range(CLOSE * 2):
        message[peer] = total[:, WIDTH:]


def finish(arrived, taps_grad, gain_grad):
    for near in range(CLOSE):
        total = arrived[2 * near] + arrived[2 * near + 1]
        total = jnp.concatenate([total[0:4], total[4:8]], 1)
        if near < CLOSE - 1:
            taps_grad[near * 4 : near * 4 + 4] = total
        else:
            taps_grad[near * 4 : near * 4 + 3] = total[0:3]
            gain_grad[...] = total[3:4]


def shards(
    proj_value, proj_gate, out_cotangent, out_weight, conv_taps, norm_gain, row_mean, row_scale
):
    end_gate = jax.nn.sigmoid(proj_gate[ROWS - EDGE :].astype(WIDE))
    end = (proj_value[ROWS - EDGE :].astype(WIDE) * end_gate).astype(NARROW)
    halo = shifted(end, SP, 1)
    split = (HALVES, ROWS, LANES)
    body, upstream = call(
        gate_and_upstream, [(split, WIDE), (split, WIDE)],
        proj_value, proj_gate, out_cotangent, out_weight, flops=2 * ROWS * WIDTH * MODEL,
    )
    column_scratch = [pltpu.VMEM((ROWS, LANES), WIDE)] * 4
    taps_scratch = pltpu.VMEM((TAPS + 1, WIDTH), WIDE)
    padded, scaled, spread, hidden, message, gain_part = call_with(
        forward,
        [
            ((HALVES, EDGE + ROWS, LANES), WIDE), (split, WIDE), (split, WIDE),
            ((ROWS, WIDTH), NARROW), ((TP, 8, LANES), WIDE), ((HALVES, 8, LANES), WIDE),
        ],
        [taps_scratch, *column_scratch],
        halo, body, upstream, conv_taps, norm_gain.reshape(1, WIDTH), row_mean, row_scale,
        flops=100 * ROWS * WIDTH,
    )
    sums = exchange(message, "tp")
    core = lax.axis_index("c").reshape(1)
    grouped = (CLOSE, FAR, OWN, WIDTH)
    mine, other = weight_call(core, out_cotangent, hidden, [(grouped, WIDE), (grouped, NARROW)])
    other = lax.ppermute(other, "c", [(0, 1), (1, 0)])
    pieces, extended = call_with(
        backward,
        [((CLOSE, FAR * OWN + 8, WIDTH), NARROW), ((HALVES, ROWS + 2 * EDGE, LANES), WIDE)],
        [pltpu.VMEM((TAPS + 1, WIDTH), WIDE)],
        sums, scaled, spread, padded, row_scale, gain_part, mine, other,
        flops=100 * ROWS * WIDTH,
    )
    (pieces,) = call(
        fold_near, [((FAR, OWN, WIDTH + LANES), NARROW)], exchange(pieces, NEAR), flops=1 << 20
    )
    arrived = exchange(pieces, "zh")
    d_gated, margin = call_with(
        gated_gradient, [(split, WIDE), ((HALVES, EDGE, LANES), WIDE)], [taps_scratch],
        extended, conv_taps, flops=100 * ROWS * WIDTH,
    )
    late = shifted(margin, SP, -1)
    value_grad, gate_grad = call(
        outputs, [((ROWS, WIDTH), NARROW), ((ROWS, WIDTH), NARROW)],
        d_gated, late, proj_value, proj_gate, flops=10 * ROWS * WIDTH,
    )
    weight_grad, message = call(
        fold_far, [((OWN, WIDTH), WIDE), ((CLOSE * 2, 8, LANES), WIDE)], arrived, flops=1 << 16
    )
    taps_grad, gain_grad = call(
        finish, [((TAPS, WIDTH), WIDE), ((1, WIDTH), WIDE)],
        exchange(message, (*NEAR, "c")), flops=1 << 16,
    )
    return (value_grad, gate_grad, weight_grad, taps_grad, gain_grad.reshape(WIDTH))


def call_with(body, outs, scratch, *args, flops=0, limit=24):
    shapes = [jax.ShapeDtypeStruct(shape, dtype) for shape, dtype in outs]
    size = sum(a.size * a.dtype.itemsize for a in (*args, *shapes))
    return pl.pallas_call(
        body,
        out_shape=shapes,
        scratch_shapes=scratch,
        compiler_params=pltpu.CompilerParams(vmem_limit_bytes=limit << 20),
        cost_estimate=pl.CostEstimate(flops=flops, bytes_accessed=size, transcendentals=0),
        name=body.__name__,
    )(*args)


def weight_call(core, cotangent, hidden, outs):
    whole = pl.BlockSpec(memory_space=pltpu.VMEM)
    return pl.pallas_call(
        weight_product,
        out_shape=[jax.ShapeDtypeStruct(shape, dtype) for shape, dtype in outs],
        in_specs=[pl.BlockSpec(memory_space=pltpu.SMEM), whole, whole],
        out_specs=[whole, whole],
        compiler_params=pltpu.CompilerParams(vmem_limit_bytes=24 << 20),
        cost_estimate=pl.CostEstimate(
            flops=2 * ROWS * WIDTH * MODEL, bytes_accessed=4 << 20, transcendentals=0
        ),
        name="weight_product",
    )(core, cotangent, hidden)


def solution(mesh):
    sizes = [size for _, size in AXES]
    split = Mesh(mesh.devices.reshape(*sizes, mesh.shape["tp"]), (*SP, "tp"))
    placed = (
        P(SP, "tp"),
        P(SP, "tp"),
        P(SP, None),
        P("tp", None),
        P(None, "tp"),
        P("tp"),
        P(SP),
        P(SP),
    )
    return jax.shard_map(
        shards,
        mesh=split,
        in_specs=placed,
        out_specs=(P(SP, "tp"), P(SP, "tp"), P(SP, "tp"), P(None, "tp"), P("tp")),
        check_vma=False,
    )
```

time: 126 us -> 106 us (0.84); the launches traced: 123 us -> 105 us
  blocking collectives: 20.8 us -> 68.7 us
  starting transfers between devices: 44.7 us -> 18 us
  waiting for transfers between devices: 24.8 us -> 5.05 us
  other arithmetic: 18 us -> 0.78 us
  Pallas kernels: 0 us -> 7.59 us
  local copies, waits for them, and re-layouts: 11.3 us -> 4.51 us
  matrix products: 2.83 us -> 0 us
    all_to_all x1 -> x3, blocking collectives: 20.8 us -> 68.7 us  [exchange(): return lax.all_to_all(pieces, axes, 0, 0, tiled=True)]
    all_to_all x3 -> x1, starting transfers between devices: 36.5 us -> 9.77 us  [exchange(): return lax.all_to_all(pieces, axes, 0, 0, tiled=True)]
    all_to_all x3 -> x1, waiting for transfers between devices: 19.8 us -> 0.01 us  [exchange(): return lax.all_to_all(pieces, axes, 0, 0, tiled=True)]
    pallas_call x0 -> x9, Pallas kernels: none -> 7.59 us  [the longest x3 3.9 us: call_with(): pl.pallas_call(body, out_shape=shapes, scratch_shapes=scratch, compiler_p...]
    mul x3 -> x0, other arithmetic: 4.98 us -> none  [the longest x2 3.2 us: shards(): placed = taps_wide[offset][None, :] * d_conv]
    reduce_sum x6 -> x0, other arithmetic: 4.9 us -> none  [the longest x2 4.77 us: shards(): jnp.sum(d_conv * padded[offset:offset + length], 0)]
    add x2 -> x0, other arithmetic: 3.63 us -> none  [the longest x1 3.62 us: shards(): spread = spread + jnp.pad(placed, ((offset, margin - offset), (0, 0)))]
    slice x6 -> x0, local copies, waits for them, and re-layouts: 3.16 us -> none  [the longest x1 1.01 us: shards(): placed = taps_wide[offset][None, :] * d_conv]
  transfers between devices with their start and end apart: 6 -> 4, of which waited for: 2 -> 1; matrix products, arithmetic and copies ran while one was open for 16% -> 0% of each run, Pallas kernels for 0% -> 2%
where the time goes in v2:
time: 106 us; the launch traced here: 105 us
  blocking collectives  68.7 us (65%)
  starting transfers between devices  18 us (17%)
  Pallas kernels  7.59 us (7%)
  waiting for transfers between devices  5.05 us (5%)
  local copies, waits for them, and re-layouts  4.51 us (4%)
    all_to_all x3, blocking collectives, exchange(): return lax.all_to_all(pieces, axes, 0, 0, tiled=True)  68.7 us
    all_to_all x1, starting transfers between devices, exchange(): return lax.all_to_all(pieces, axes, 0, 0, tiled=True)  9.77 us
    ppermute x2, starting transfers between devices, shifted(): lax.ppermute(value, axis, [(source, source + steps) for source in range(f...  6.32 us
    ppermute x2, waiting for transfers between devices, shifted(): lax.ppermute(value, axis, [(source, source + steps) for source in range(f...  5.04 us
    unnamed x22, local copies, waits for them, and re-layouts  4.51 us
    pallas_call x3, Pallas kernels, call_with(): pl.pallas_call(body, out_shape=shapes, scratch_shapes=scratch, compiler_p...  3.9 us
    pallas_call x5, Pallas kernels, call(): pl.pallas_call(body, out_shape=shapes, compiler_params=pltpu.CompilerPara...  2.91 us
  transfers between devices with their start and end apart: 4, of which 1 were waited for; matrix products, arithmetic and copies ran while one was open for 0% of the time, Pallas kernels for 2%

profile of v2, /device:TPU:7, one launch (start us, length us, event | category | flops | bytes accessed | tf_op | source)
XLA Modules:
  0.0 105.4 jit_solution(10397059300300486545)
XLA Ops:
  0.6 0.0 copy-start.8
  0.6 0.0 copy-start.7
  0.7 0.0 copy-start.9
  0.7 0.0 copy-start.10
  0.7 0.8 multiply_convert_fusion
  1.5 4.0 %collective-permute-start = (bf16[32,256]{1,0:T(8,128)(2,1)S(1)}, bf16[32,256]{1,0:T(8,128)(2,1)S(1)}, u32[]{:S(2)}, u32[]{:S(2)}) collective-permute-start(bf16[32,256]{1,0:T(8,128)(2,1)S(1)} %multiply_convert_fusion), channel_id=1, source_target_pairs={{0,4},{4,8},{8,12},{12,16},{16,20},{20,24},{24,28},{28,32},{32,36}... | collective-permute-start | bytes 49160 | tf_op jit(solution)/shard_map/ppermute | solution.py:33
  5.5 0.0 copy-start
  5.5 1.4 %copy-done = bf16[384,2048]{1,0:T(8,128)(2,1)S(1)} copy-done((bf16[384,2048]{1,0:T(8,128)(2,1)S(1)}, bf16[384,2048]{1,0:T(8,128)(2,1)}, u32[]{:S(2)}) %copy-start) | copy-done | bytes 1572888
  6.9 0.0 copy-start.2
  6.9 1.2 %copy-done.2 = bf16[256,2048]{1,0:T(8,128)(2,1)S(1)} copy-done((bf16[256,2048]{1,0:T(8,128)(2,1)S(1)}, bf16[256,2048]{1,0:T(8,128)(2,1)}, u32[]{:S(2)}) %copy-start.2) | copy-done | bytes 1048600
  8.1 0.0 copy-start.3
  8.1 0.9 copy-done.3
  9.0 0.0 copy-start.5
  9.0 0.9 copy-done.5
  10.0 0.0 copy-start.1
  10.0 0.7 gate_and_upstream.1
  10.7 0.0 collective-permute-done.halo
  10.7 0.0 copy-done.8
  10.7 0.0 copy-done.7
  10.7 0.0 copy-done.9
  10.7 0.0 copy-done.10
  10.7 1.3 %forward.1 = (f32[2,416,128]{2,1,0:T(8,128)S(1)}, f32[2,384,128]{2,1,0:T(8,128)S(1)}, f32[2,384,128]{2,1,0:T(8,128)S(1)}, bf16[384,256]{1,0:T(8,128)(2,1)S(1)}, ...) custom-call(bf16[32,256]{1,0:T(8,128)(2,1)S(1)} %collective-permute-done.halo, ...), custom_call_target="tpu_custom_call" | custom-call | flops 9830400 | bytes 2256384 | tf_op jit(solution)/shard_map/forward/pallas_call | solution.py:306
  12.0 0.0 copy-done.1
  12.1 0.8 weight_product.1
  12.8 1.9 %collective-permute-start.1 = (bf16[8,16,8,256]{3,2,1,0:T(8,128)(2,1)S(1)}, bf16[8,16,8,256]{3,2,1,0:T(8,128)(2,1)S(1)}, u32[]{:S(2)}, u32[]{:S(2)}) collective-permute-start(bf16[8,16,8,256]{3,2,1,0:T(8,128)(2,1)S(1)} %get-tuple-element.34), channel_id=1, source_target_pairs={{0,4},{4,0},{1,5},{5,1},{2,6},{6,2},{3,7},{7,3},{8,12},{12,8},{9,1... | collective-permute-start | bytes 1572872 | tf_op jit(solution)/shard_map/ppermute | solution.py:272
  14.8 8.2 %all_to_all.20.sums = f32[4,8,128]{2,1,0:T(8,128)S(1)} all-to-all(f32[4,8,128]{2,1,0:T(8,128)S(1)} %get-tuple-element.27), channel_id=1, replica_groups=mesh['zh'=16,'zl'=2,'x'=4,'c'=2,'tp'=4] {'tp'}, dimensions={0} | all-to-all | bytes 32768 | tf_op jit(solution)/shard_map/all_to_all | solution.py:37
  23.0 0.0 collective-permute-done.1.other
  23.0 1.7 %backward.1 = (bf16[8,136,256]{2,1,0:T(8,128)(2,1)S(1)}, f32[2,448,128]{2,1,0:T(8,128)S(1)}) custom-call(f32[4,8,128]{2,1,0:T(8,128)S(1)} %all_to_all.20.sums, f32[2,384,128]{2,1,0:T(8,128)S(1)} %get-tuple-element.28.scaled, f32[2,384,128]{2,1,0:T(8,128)S(1)} %get-tuple-element.29.spread, f32[2,416,128]{2,1,0:T(8,128)S(1)} %get-tuple-element.30.padded, ...), custom_call_target="tpu_custom_call" | custom-call | flops 9830400 | bytes 3827200 | tf_op jit(solution)/shard_map/backward/pallas_call | solution.py:306
  24.7 0.0 copy-start.4
  24.7 0.0 copy-start.6
  24.7 19.1 %all_to_all.21.arrived = bf16[8,136,256]{2,1,0:T(8,128)(2,1)S(1)} all-to-all(bf16[8,136,256]{2,1,0:T(8,128)(2,1)S(1)} %get-tuple-element.40), channel_id=1, replica_groups=mesh['zh'=16,'zl'=2,'x'=4,'c'=2,'tp'=4] {'zl','x'}, dimensions={0} | all-to-all | bytes 1114112 | tf_op jit(solution)/shard_map/all_to_all | solution.py:37
  43.9 0.1 fold_near.1
  43.9 41.3 %all_to_all.22.arrived = bf16[16,8,384]{2,1,0:T(8,128)(2,1)S(1)} all-to-all(bf16[16,8,384]{2,1,0:T(8,128)(2,1)S(1)} %fold_near.1), channel_id=1, replica_groups=mesh['zh'=16,'zl'=2,'x'=4,'c'=2,'tp'=4] {'zh'}, dimensions={0} | all-to-all | bytes 196608 | tf_op jit(solution)/shard_map/all_to_all | solution.py:37
  85.3 0.6 fold_far.1
  85.9 9.8 %all-to-all-start.3 = ((f32[16,8,128]{2,1,0:T(8,128)}), f32[16,8,128]{2,1,0:T(8,128)S(1)}, u32[]{:S(2)}, u32[]{:S(2)}) async-start(f32[16,8,128]{2,1,0:T(8,128)} %get-tuple-element.42), calls=%async_computation.3 | async-start | bytes 131072 | tf_op jit(solution)/shard_map/all_to_all | solution.py:37
  95.7 0.9 gated_gradient.1
  96.5 2.3 %collective-permute-start.2 = (f32[2,32,128]{2,1,0:T(8,128)S(1)}, f32[2,32,128]{2,1,0:T(8,128)S(1)}, u32[]{:S(2)}, u32[]{:S(2)}) collective-permute-start(f32[2,32,128]{2,1,0:T(8,128)S(1)} %get-tuple-element.37), channel_id=1, source_target_pairs={{4,0},{8,4},{12,8},{16,12},{20,16},{24,20},{28,24},{32,28},{36,32}... | collective-permute-start | bytes 98312 | tf_op jit(solution)/shard_map/ppermute | solution.py:33
  98.9 5.0 %collective-permute-done.2.arrived = f32[2,32,128]{2,1,0:T(8,128)S(1)} collective-permute-done((f32[2,32,128]{2,1,0:T(8,128)S(1)}, f32[2,32,128]{2,1,0:T(8,128)S(1)}, u32[]{:S(2)}, u32[]{:S(2)}) %collective-permute-start.2) | collective-permute-done | bytes 32800 | tf_op jit(solution)/shard_map/ppermute | solution.py:33
  103.9 0.0 copy-done.4
  103.9 0.0 copy-done.6
  103.9 0.9 outputs.1
  104.8 0.0 all-to-all-done.3.arrived
  104.8 0.6 finish.1
Async XLA Ops:
  0.6 10.0 %copy-start.8 = (f32[384]{0:T(512)S(1)}, f32[384]{0:T(512)}, u32[]{:S(2)}) copy-start(f32[384]{0:T(512)} %scale.3) | copy-start | bytes 4612
  0.6 10.0 %copy-start.7 = (bf16[31,256]{1,0:T(8,128)(2,1)S(1)}, bf16[31,256]{1,0:T(8,128)(2,1)}, u32[]{:S(2)}) copy-start(bf16[31,256]{1,0:T(8,128)(2,1)} %taps.3) | copy-start | bytes 47620
  0.7 10.0 %copy-start.9 = (f32[384]{0:T(512)S(1)}, f32[384]{0:T(512)}, u32[]{:S(2)}) copy-start(f32[384]{0:T(512)} %mean.1) | copy-start | bytes 4612
  0.7 10.0 %copy-start.10 = (f32[256]{0:T(256)S(1)}, f32[256]{0:T(256)}, u32[]{:S(2)}) copy-start(f32[256]{0:T(256)} %param.13) | copy-start | bytes 3076
  1.5 9.2 %collective-permute-start = (bf16[32,256]{1,0:T(8,128)(2,1)S(1)}, bf16[32,256]{1,0:T(8,128)(2,1)S(1)}, u32[]{:S(2)}, u32[]{:S(2)}) collective-permute-start(bf16[32,256]{1,0:T(8,128)(2,1)S(1)} %multiply_convert_fusion), channel_id=1, source_target_pairs={{0,4},{4,8},{8,12},{12,16},{16,20},{20,24},{24,28},{28,32},{32,36}... | collective-permute-start | bytes 49160 | tf_op jit(solution)/shard_map/ppermute | solution.py:33
  5.5 1.4 %copy-start = (bf16[384,2048]{1,0:T(8,128)(2,1)S(1)}, bf16[384,2048]{1,0:T(8,128)(2,1)}, u32[]{:S(2)}) copy-start(bf16[384,2048]{1,0:T(8,128)(2,1)} %cotangent.3) | copy-start | bytes 4718596
  6.9 1.2 %copy-start.2 = (bf16[256,2048]{1,0:T(8,128)(2,1)S(1)}, bf16[256,2048]{1,0:T(8,128)(2,1)}, u32[]{:S(2)}) copy-start(bf16[256,2048]{1,0:T(8,128)(2,1)} %weight.1) | copy-start | bytes 3145732
  8.1 0.9 copy-start.3
  9.0 0.9 copy-start.5
  10.0 2.1 %copy-start.1 = (bf16[384,2048]{1,0:T(8,128)(2,1)S(1)}, bf16[384,2048]{1,0:T(8,128)(2,1)}, u32[]{:S(2)}) copy-start(bf16[384,2048]{1,0:T(8,128)(2,1)} %cotangent.3) | copy-start | bytes 4718596
  12.8 10.1 %collective-permute-start.1 = (bf16[8,16,8,256]{3,2,1,0:T(8,128)(2,1)S(1)}, bf16[8,16,8,256]{3,2,1,0:T(8,128)(2,1)S(1)}, u32[]{:S(2)}, u32[]{:S(2)}) collective-permute-start(bf16[8,16,8,256]{3,2,1,0:T(8,128)(2,1)S(1)} %get-tuple-element.34), channel_id=1, source_target_pairs={{0,4},{4,0},{1,5},{5,1},{2,6},{6,2},{3,7},{7,3},{8,12},{12,8},{9,1... | collective-permute-start | bytes 1572872 | tf_op jit(solution)/shard_map/ppermute | solution.py:272
  24.7 79.2 %copy-start.4 = (bf16[384,256]{1,0:T(8,128)(2,1)S(1)}, bf16[384,256]{1,0:T(8,128)(2,1)}, u32[]{:S(2)}) copy-start(bf16[384,256]{1,0:T(8,128)(2,1)} %gate.3) | copy-start | bytes 589828
  24.7 79.2 %copy-start.6 = (bf16[384,256]{1,0:T(8,128)(2,1)S(1)}, bf16[384,256]{1,0:T(8,128)(2,1)}, u32[]{:S(2)}) copy-start(bf16[384,256]{1,0:T(8,128)(2,1)} %value.3) | copy-start | bytes 589828
  85.9 18.9 %all-to-all-start.3 = ((f32[16,8,128]{2,1,0:T(8,128)}), f32[16,8,128]{2,1,0:T(8,128)S(1)}, u32[]{:S(2)}, u32[]{:S(2)}) async-start(f32[16,8,128]{2,1,0:T(8,128)} %get-tuple-element.42), calls=%async_computation.3 | async-start | bytes 131072 | tf_op jit(solution)/shard_map/all_to_all | solution.py:37
  96.5 7.3 %collective-permute-start.2 = (f32[2,32,128]{2,1,0:T(8,128)S(1)}, f32[2,32,128]{2,1,0:T(8,128)S(1)}, u32[]{:S(2)}, u32[]{:S(2)}) collective-permute-start(f32[2,32,128]{2,1,0:T(8,128)S(1)} %get-tuple-element.37), channel_id=1, source_target_pairs={{4,0},{8,4},{12,8},{16,12},{20,16},{24,20},{28,24},{32,28},{36,32}... | collective-permute-start | bytes 98312 | tf_op jit(solution)/shard_map/ppermute | solution.py:33

commit v3 on v2

--- a/solution.py
+++ b/solution.py
@@ -1,5 +1,3 @@
-import functools
-
 import jax
 import jax.numpy as jnp
 from jax import lax
@@ -7,6 +5,7 @@
 from jax.experimental.pallas import tpu as pltpu
 from jax.sharding import Mesh
 from jax.sharding import PartitionSpec as P
+
 
 SP = ("zh", "zl", "x", "c")
 NEAR = ("zl", "x")
@@ -45,7 +44,7 @@
     return jnp.transpose(jnp.broadcast_to(row, (LANES, LANES)))
 
 
-def call(body, outs, *args, flops=0, limit=24):
+def call(body, outs, *args, flops=0, limit=6):
     shapes = [jax.ShapeDtypeStruct(shape, dtype) for shape, dtype in outs]
     size = sum(a.size * a.dtype.itemsize for a in (*args, *shapes))
     return pl.pallas_call(
@@ -53,22 +52,42 @@
         out_shape=shapes,
         compiler_params=pltpu.CompilerParams(vmem_limit_bytes=limit << 20),
         cost_estimate=pl.CostEstimate(flops=flops, bytes_accessed=size, transcendentals=0),
-        name=body.__name__,
     )(*args)
 
 
-def gate_and_upstream(value, gate, cotangent, weight, body, upstream):
+def gate_and_upstream(
+    value, gate, cotangent, weight, body, upstream, held, held_value, held_gate, held_weight, arrivals
+):
+    parts = ROWS // LANES
+    copies = [
+        pltpu.make_async_copy(value, held_value, arrivals.at[0]),
+        pltpu.make_async_copy(gate, held_gate, arrivals.at[1]),
+        pltpu.make_async_copy(weight, held_weight, arrivals.at[2]),
+    ]
+    for part in range(parts):
+        rows = pl.ds(part * LANES, LANES)
+        copies.append(
+            pltpu.make_async_copy(cotangent.at[rows], held.at[rows], arrivals.at[3 + part])
+        )
+    for copy in copies:
+        copy.start()
+    copies[0].wait()
+    copies[1].wait()
     for start in range(0, ROWS, CHUNK):
         rows = slice(start, start + CHUNK)
         for half in range(HALVES):
-            sig = jax.nn.sigmoid(gate[rows, lanes(half)].astype(WIDE))
-            gated = (value[rows, lanes(half)].astype(WIDE) * sig).astype(NARROW)
+            sig = jax.nn.sigmoid(held_gate[rows, lanes(half)].astype(WIDE))
+            gated = (held_value[rows, lanes(half)].astype(WIDE) * sig).astype(NARROW)
             body[half, rows, :] = gated.astype(WIDE)
-    product = lax.dot_general(
-        cotangent[...], weight[...], (((1,), (1,)), ((), ())), preferred_element_type=WIDE
-    )
-    for half in range(HALVES):
-        upstream[half] = product[:, lanes(half)]
+    copies[2].wait()
+    for part in range(parts):
+        rows = slice(part * LANES, (part + 1) * LANES)
+        copies[3 + part].wait()
+        product = lax.dot_general(
+            held[rows], held_weight[...], (((1,), (1,)), ((), ())), preferred_element_type=WIDE
+        )
+        for half in range(HALVES):
+            upstream[half, rows] = product[:, lanes(half)]
 
 
 def forward(
@@ -249,9 +268,9 @@
     end = (proj_value[ROWS - EDGE :].astype(WIDE) * end_gate).astype(NARROW)
     halo = shifted(end, SP, 1)
     split = (HALVES, ROWS, LANES)
-    body, upstream = call(
-        gate_and_upstream, [(split, WIDE), (split, WIDE)],
-        proj_value, proj_gate, out_cotangent, out_weight, flops=2 * ROWS * WIDTH * MODEL,
+    body, upstream, held = first_call(
+        [(split, WIDE), (split, WIDE), ((ROWS, MODEL), NARROW)],
+        proj_value, proj_gate, out_cotangent, out_weight,
     )
     column_scratch = [pltpu.VMEM((ROWS, LANES), WIDE)] * 4
     taps_scratch = pltpu.VMEM((TAPS + 1, WIDTH), WIDE)
@@ -268,7 +287,7 @@
     sums = exchange(message, "tp")
     core = lax.axis_index("c").reshape(1)
     grouped = (CLOSE, FAR, OWN, WIDTH)
-    mine, other = weight_call(core, out_cotangent, hidden, [(grouped, WIDE), (grouped, NARROW)])
+    mine, other = weight_call(core, held, hidden, [(grouped, WIDE), (grouped, NARROW)])
     other = lax.ppermute(other, "c", [(0, 1), (1, 0)])
     pieces, extended = call_with(
         backward,
@@ -300,7 +319,7 @@
     return (value_grad, gate_grad, weight_grad, taps_grad, gain_grad.reshape(WIDTH))
 
 
-def call_with(body, outs, scratch, *args, flops=0, limit=24):
+def call_with(body, outs, scratch, *args, flops=0, limit=6):
     shapes = [jax.ShapeDtypeStruct(shape, dtype) for shape, dtype in outs]
     size = sum(a.size * a.dtype.itemsize for a in (*args, *shapes))
     return pl.pallas_call(
@@ -309,8 +328,28 @@
         scratch_shapes=scratch,
         compiler_params=pltpu.CompilerParams(vmem_limit_bytes=limit << 20),
         cost_estimate=pl.CostEstimate(flops=flops, bytes_accessed=size, transcendentals=0),
-        name=body.__name__,
     )(*args)
+
+
+def first_call(outs, *args):
+    narrow = (ROWS, WIDTH)
+    return pl.pallas_call(
+        gate_and_upstream,
+        out_shape=[jax.ShapeDtypeStruct(shape, dtype) for shape, dtype in outs],
+        in_specs=[pl.BlockSpec(memory_space=pltpu.HBM)] * 4,
+        out_specs=[pl.BlockSpec(memory_space=pltpu.VMEM)] * 3,
+        scratch_shapes=[
+            pltpu.VMEM(narrow, NARROW),
+            pltpu.VMEM(narrow, NARROW),
+            pltpu.VMEM((WIDTH, MODEL), NARROW),
+            pltpu.SemaphoreType.DMA((3 + ROWS // LANES,)),
+        ],
+        compiler_params=pltpu.CompilerParams(vmem_limit_bytes=6 << 20),
+        cost_estimate=pl.CostEstimate(
+            flops=2 * ROWS * WIDTH * MODEL, bytes_accessed=4 << 20, transcendentals=0
+        ),
+        name="gate_and_upstream",
+    )(*(pltpu.with_memory_space_constraint(a, pltpu.HBM) for a in args))
 
 
 def weight_call(core, cotangent, hidden, outs):
@@ -320,7 +359,7 @@
         out_shape=[jax.ShapeDtypeStruct(shape, dtype) for shape, dtype in outs],
         in_specs=[pl.BlockSpec(memory_space=pltpu.SMEM), whole, whole],
         out_specs=[whole, whole],
-        compiler_params=pltpu.CompilerParams(vmem_limit_bytes=24 << 20),
+        compiler_params=pltpu.CompilerParams(vmem_limit_bytes=6 << 20),
         cost_estimate=pl.CostEstimate(
             flops=2 * ROWS * WIDTH * MODEL, bytes_accessed=4 << 20, transcendentals=0
         ),

time: 106 us -> 104 us (0.981)
  local copies, waits for them, and re-layouts: 4.51 us -> 0.03 us
  Pallas kernels: 7.59 us -> 10.4 us
    unnamed x22 -> x12, local copies, waits for them, and re-layouts: 4.51 us -> 0.03 us
    pallas_call x0 -> x1, Pallas kernels: none -> 3.51 us  [first_call(): pl.pallas_call(gate_and_upstream, out_shape=[jax.ShapeDtypeStruct(shape,...]
    pallas_call x5 -> x4, Pallas kernels: 2.91 us -> 2.25 us  [call(): pl.pallas_call(body, out_shape=shapes, compiler_params=pltpu.CompilerPara...]
  transfers between devices with their start and end apart: 4 -> 4, of which waited for: 1 -> 1; matrix products, arithmetic and copies ran while one was open for 0% -> 0% of each run, Pallas kernels for 2% -> 5%
where the time goes in v3:
time: 104 us
  blocking collectives  69.3 us (67%)
  starting transfers between devices  17.6 us (17%)
  Pallas kernels  10.4 us (10%)
  waiting for transfers between devices  5.04 us (5%)
    all_to_all x3, blocking collectives, exchange(): return lax.all_to_all(pieces, axes, 0, 0, tiled=True)  69.3 us
    all_to_all x1, starting transfers between devices, exchange(): return lax.all_to_all(pieces, axes, 0, 0, tiled=True)  9.38 us
    ppermute x2, starting transfers between devices, shifted(): lax.ppermute(value, axis, [(source, source + steps) for source in range(f...  6.32 us
    ppermute x2, waiting for transfers between devices, shifted(): lax.ppermute(value, axis, [(source, source + steps) for source in range(f...  5.04 us
    pallas_call x3, Pallas kernels, call_with(): pl.pallas_call(body, out_shape=shapes, scratch_shapes=scratch, compiler_p...  3.9 us
    pallas_call x1, Pallas kernels, first_call(): pl.pallas_call(gate_and_upstream, out_shape=[jax.ShapeDtypeStruct(shape,...  3.51 us
    pallas_call x4, Pallas kernels, call(): pl.pallas_call(body, out_shape=shapes, compiler_params=pltpu.CompilerPara...  2.25 us
  transfers between devices with their start and end apart: 4, of which 1 were waited for; matrix products, arithmetic and copies ran while one was open for 0% of the time, Pallas kernels for 5%

profile of v3, /device:TPU:7, one launch (start us, length us, event | category | flops | bytes accessed | tf_op | source)
XLA Modules:
  0.0 104.0 jit_solution(11384136609211829312)
XLA Ops:
  0.6 0.0 copy-start.2
  0.6 0.0 copy-start.5
  0.7 0.0 copy-start.4
  0.7 0.0 copy-start.3
  0.7 0.8 multiply_convert_fusion
  1.5 4.0 %collective-permute-start = (bf16[32,256]{1,0:T(8,128)(2,1)S(1)}, bf16[32,256]{1,0:T(8,128)(2,1)S(1)}, u32[]{:S(2)}, u32[]{:S(2)}) collective-permute-start(bf16[32,256]{1,0:T(8,128)(2,1)S(1)} %multiply_convert_fusion), channel_id=1, source_target_pairs={{0,4},{4,8},{8,12},{12,16},{16,20},{20,24},{24,28},{28,32},{32,36}... | collective-permute-start | bytes 49160 | tf_op jit(solution)/shard_map/ppermute | solution.py:32
  5.5 3.5 %gate_and_upstream.1 = (f32[2,384,128]{2,1,0:T(8,128)S(1)}, f32[2,384,128]{2,1,0:T(8,128)S(1)}, bf16[384,2048]{1,0:T(8,128)(2,1)S(1)}) custom-call(bf16[384,256]{1,0:T(8,128)(2,1)} %value.3, bf16[384,256]{1,0:T(8,128)(2,1)} %gate.3, bf16[384,2048]{1,0:T(8,128)(2,1)} %cotangent.1, bf16[256,2048]{1,0:T(8,128)(2,1)} %weight.1), custom_call_target="tpu_custom_call" | custom-call | flops 402653184 | bytes 4194304 | tf_op jit(solution)/shard_map/gate_and_upstream/pallas_call | solution.py:336
  9.0 0.0 collective-permute-done.halo
  9.0 0.0 copy-done.2
  9.0 0.0 copy-done.5
  9.0 0.0 copy-done.4
  9.0 0.0 copy-done.3
  9.1 1.3 %shard_map.119 = (f32[2,416,128]{2,1,0:T(8,128)S(1)}, f32[2,384,128]{2,1,0:T(8,128)S(1)}, f32[2,384,128]{2,1,0:T(8,128)S(1)}, bf16[384,256]{1,0:T(8,128)(2,1)S(1...) custom-call(bf16[32,256]{1,0:T(8,128)(2,1)S(1)} %collective-permute-done.halo, ...), custom_call_target="tpu_custom_call" | custom-call | flops 9830400 | bytes 2256384 | tf_op jit(solution)/shard_map/pallas_call | solution.py:325
  10.4 0.8 weight_product.1
  11.2 1.9 %collective-permute-start.1 = (bf16[8,16,8,256]{3,2,1,0:T(8,128)(2,1)S(1)}, bf16[8,16,8,256]{3,2,1,0:T(8,128)(2,1)S(1)}, u32[]{:S(2)}, u32[]{:S(2)}) collective-permute-start(bf16[8,16,8,256]{3,2,1,0:T(8,128)(2,1)S(1)} %get-tuple-element.36), channel_id=1, source_target_pairs={{0,4},{4,0},{1,5},{5,1},{2,6},{6,2},{3,7},{7,3},{8,12},{12,8},{9,1... | collective-permute-start | bytes 1572872 | tf_op jit(solution)/shard_map/ppermute | solution.py:291
  13.1 8.2 %all_to_all.20.sums = f32[4,8,128]{2,1,0:T(8,128)S(1)} all-to-all(f32[4,8,128]{2,1,0:T(8,128)S(1)} %get-tuple-element.28), channel_id=1, replica_groups=mesh['zh'=16,'zl'=2,'x'=4,'c'=2,'tp'=4] {'tp'}, dimensions={0} | all-to-all | bytes 32768 | tf_op jit(solution)/shard_map/all_to_all | solution.py:36
  21.3 0.0 collective-permute-done.1.other
  21.3 1.7 %shard_map.120 = (bf16[8,136,256]{2,1,0:T(8,128)(2,1)S(1)}, f32[2,448,128]{2,1,0:T(8,128)S(1)}) custom-call(f32[4,8,128]{2,1,0:T(8,128)S(1)} %all_to_all.20.sums, f32[2,384,128]{2,1,0:T(8,128)S(1)} %get-tuple-element.29.scaled, f32[2,384,128]{2,1,0:T(8,128)S(1)} %get-tuple-element.30.spread, f32[2,416,128]{2,1,0:T(8,128)S(1)} %get-tuple-element.31.padded, ...), custom_call_target="tpu_custom_call" | custom-call | flops 9830400 | bytes 3827200 | tf_op jit(solution)/shard_map/pallas_call | solution.py:325
  23.0 0.0 copy-start
  23.0 0.0 copy-start.1
  23.0 19.1 %all_to_all.21.arrived = bf16[8,136,256]{2,1,0:T(8,128)(2,1)S(1)} all-to-all(bf16[8,136,256]{2,1,0:T(8,128)(2,1)S(1)} %get-tuple-element.42), channel_id=1, replica_groups=mesh['zh'=16,'zl'=2,'x'=4,'c'=2,'tp'=4] {'zl','x'}, dimensions={0} | all-to-all | bytes 1114112 | tf_op jit(solution)/shard_map/all_to_all | solution.py:36
  42.2 0.1 shard_map.123
  42.3 41.9 %all_to_all.22.arrived = bf16[16,8,384]{2,1,0:T(8,128)(2,1)S(1)} all-to-all(bf16[16,8,384]{2,1,0:T(8,128)(2,1)S(1)} %shard_map.123), channel_id=1, replica_groups=mesh['zh'=16,'zl'=2,'x'=4,'c'=2,'tp'=4] {'zh'}, dimensions={0} | all-to-all | bytes 196608 | tf_op jit(solution)/shard_map/all_to_all | solution.py:36
  84.2 0.7 shard_map.124
  84.9 9.4 %all-to-all-start.3 = ((f32[16,8,128]{2,1,0:T(8,128)}), f32[16,8,128]{2,1,0:T(8,128)S(1)}, u32[]{:S(2)}, u32[]{:S(2)}) async-start(f32[16,8,128]{2,1,0:T(8,128)} %get-tuple-element.44), calls=%async_computation.3 | async-start | bytes 131072 | tf_op jit(solution)/shard_map/all_to_all | solution.py:36
  94.2 0.9 shard_map.121
  95.1 2.3 %collective-permute-start.2 = (f32[2,32,128]{2,1,0:T(8,128)S(1)}, f32[2,32,128]{2,1,0:T(8,128)S(1)}, u32[]{:S(2)}, u32[]{:S(2)}) collective-permute-start(f32[2,32,128]{2,1,0:T(8,128)S(1)} %get-tuple-element.39), channel_id=1, source_target_pairs={{4,0},{8,4},{12,8},{16,12},{20,16},{24,20},{28,24},{32,28},{36,32}... | collective-permute-start | bytes 98312 | tf_op jit(solution)/shard_map/ppermute | solution.py:32
  97.4 5.0 %collective-permute-done.2.arrived = f32[2,32,128]{2,1,0:T(8,128)S(1)} collective-permute-done((f32[2,32,128]{2,1,0:T(8,128)S(1)}, f32[2,32,128]{2,1,0:T(8,128)S(1)}, u32[]{:S(2)}, u32[]{:S(2)}) %collective-permute-start.2) | collective-permute-done | bytes 32800 | tf_op jit(solution)/shard_map/ppermute | solution.py:32
  102.4 0.0 copy-done
  102.4 0.0 copy-done.1
  102.5 0.9 shard_map.122
  103.3 0.0 all-to-all-done.3.arrived
  103.3 0.6 shard_map.125
Async XLA Ops:
  0.6 8.4 %copy-start.2 = (bf16[31,256]{1,0:T(8,128)(2,1)S(1)}, bf16[31,256]{1,0:T(8,128)(2,1)}, u32[]{:S(2)}) copy-start(bf16[31,256]{1,0:T(8,128)(2,1)} %taps.3) | copy-start | bytes 47620
  0.6 8.4 %copy-start.5 = (f32[256]{0:T(256)S(1)}, f32[256]{0:T(256)}, u32[]{:S(2)}) copy-start(f32[256]{0:T(256)} %param.13) | copy-start | bytes 3076
  0.7 8.4 %copy-start.4 = (f32[384]{0:T(512)S(1)}, f32[384]{0:T(512)}, u32[]{:S(2)}) copy-start(f32[384]{0:T(512)} %mean.1) | copy-start | bytes 4612
  0.7 8.4 %copy-start.3 = (f32[384]{0:T(512)S(1)}, f32[384]{0:T(512)}, u32[]{:S(2)}) copy-start(f32[384]{0:T(512)} %scale.3) | copy-start | bytes 4612
  1.5 7.5 %collective-permute-start = (bf16[32,256]{1,0:T(8,128)(2,1)S(1)}, bf16[32,256]{1,0:T(8,128)(2,1)S(1)}, u32[]{:S(2)}, u32[]{:S(2)}) collective-permute-start(bf16[32,256]{1,0:T(8,128)(2,1)S(1)} %multiply_convert_fusion), channel_id=1, source_target_pairs={{0,4},{4,8},{8,12},{12,16},{16,20},{20,24},{24,28},{28,32},{32,36}... | collective-permute-start | bytes 49160 | tf_op jit(solution)/shard_map/ppermute | solution.py:32
  11.2 10.1 %collective-permute-start.1 = (bf16[8,16,8,256]{3,2,1,0:T(8,128)(2,1)S(1)}, bf16[8,16,8,256]{3,2,1,0:T(8,128)(2,1)S(1)}, u32[]{:S(2)}, u32[]{:S(2)}) collective-permute-start(bf16[8,16,8,256]{3,2,1,0:T(8,128)(2,1)S(1)} %get-tuple-element.36), channel_id=1, source_target_pairs={{0,4},{4,0},{1,5},{5,1},{2,6},{6,2},{3,7},{7,3},{8,12},{12,8},{9,1... | collective-permute-start | bytes 1572872 | tf_op jit(solution)/shard_map/ppermute | solution.py:291
  23.0 79.4 %copy-start = (bf16[384,256]{1,0:T(8,128)(2,1)S(1)}, bf16[384,256]{1,0:T(8,128)(2,1)}, u32[]{:S(2)}) copy-start(bf16[384,256]{1,0:T(8,128)(2,1)} %gate.3) | copy-start | bytes 589828
  23.0 79.4 %copy-start.1 = (bf16[384,256]{1,0:T(8,128)(2,1)S(1)}, bf16[384,256]{1,0:T(8,128)(2,1)}, u32[]{:S(2)}) copy-start(bf16[384,256]{1,0:T(8,128)(2,1)} %value.3) | copy-start | bytes 589828
  84.9 18.5 %all-to-all-start.3 = ((f32[16,8,128]{2,1,0:T(8,128)}), f32[16,8,128]{2,1,0:T(8,128)S(1)}, u32[]{:S(2)}, u32[]{:S(2)}) async-start(f32[16,8,128]{2,1,0:T(8,128)} %get-tuple-element.44), calls=%async_computation.3 | async-start | bytes 131072 | tf_op jit(solution)/shard_map/all_to_all | solution.py:36
  95.1 7.3 %collective-permute-start.2 = (f32[2,32,128]{2,1,0:T(8,128)S(1)}, f32[2,32,128]{2,1,0:T(8,128)S(1)}, u32[]{:S(2)}, u32[]{:S(2)}) collective-permute-start(f32[2,32,128]{2,1,0:T(8,128)S(1)} %get-tuple-element.39), channel_id=1, source_target_pairs={{4,0},{8,4},{12,8},{16,12},{20,16},{24,20},{28,24},{32,28},{36,32}... | collective-permute-start | bytes 98312 | tf_op jit(solution)/shard_map/ppermute | solution.py:32

commit v4 on v2

--- a/solution.py
+++ b/solution.py
@@ -1,5 +1,3 @@
-import functools
-
 import jax
 import jax.numpy as jnp
 from jax import lax
@@ -8,11 +6,13 @@
 from jax.sharding import Mesh
 from jax.sharding import PartitionSpec as P
 
+
 SP = ("zh", "zl", "x", "c")
 NEAR = ("zl", "x")
 FAR = 16
 CLOSE = 8
 AXES = (("zh", FAR), ("zl", 2), ("x", 4), ("c", 2))
+FAR_ORDER = [(place + 10) % FAR for place in range(FAR)]
 TP = 4
 TAPS = 31
 ROWS = 384
@@ -33,8 +33,9 @@
     return lax.ppermute(value, axis, [(source, source + steps) for source in range(first, last)])
 
 
-def exchange(pieces, axes):
-    return lax.all_to_all(pieces, axes, 0, 0, tiled=True)
+def exchange(pieces, axes, order=None):
+    groups = order and [order]
+    return lax.all_to_all(pieces, axes, 0, 0, tiled=True, axis_index_groups=groups)
 
 
 def lanes(half):
@@ -45,7 +46,7 @@
     return jnp.transpose(jnp.broadcast_to(row, (LANES, LANES)))
 
 
-def call(body, outs, *args, flops=0, limit=24):
+def call(body, outs, *args, flops=0, limit=6):
     shapes = [jax.ShapeDtypeStruct(shape, dtype) for shape, dtype in outs]
     size = sum(a.size * a.dtype.itemsize for a in (*args, *shapes))
     return pl.pallas_call(
@@ -53,26 +54,11 @@
         out_shape=shapes,
         compiler_params=pltpu.CompilerParams(vmem_limit_bytes=limit << 20),
         cost_estimate=pl.CostEstimate(flops=flops, bytes_accessed=size, transcendentals=0),
-        name=body.__name__,
     )(*args)
 
 
-def gate_and_upstream(value, gate, cotangent, weight, body, upstream):
-    for start in range(0, ROWS, CHUNK):
-        rows = slice(start, start + CHUNK)
-        for half in range(HALVES):
-            sig = jax.nn.sigmoid(gate[rows, lanes(half)].astype(WIDE))
-            gated = (value[rows, lanes(half)].astype(WIDE) * sig).astype(NARROW)
-            body[half, rows, :] = gated.astype(WIDE)
-    product = lax.dot_general(
-        cotangent[...], weight[...], (((1,), (1,)), ((), ())), preferred_element_type=WIDE
-    )
-    for half in range(HALVES):
-        upstream[half] = product[:, lanes(half)]
-
-
 def forward(
-    halo, body, upstream, taps, gain, mean, scale,
+    halo, value, gate, upstream, taps, gain, mean, scale,
     padded, scaled, spread, hidden, message, gain_part,
     taps_wide, mean_columns, scale_columns, sum_first, sum_second,
 ):
@@ -83,7 +69,11 @@
         scale_columns[rows] = column(scale[rows].reshape(1, LANES))
     for half in range(HALVES):
         padded[half, 0:EDGE] = halo[:, lanes(half)].astype(WIDE)
-        padded[half, EDGE:] = body[half]
+        for start in range(0, ROWS, CHUNK):
+            rows = slice(start, start + CHUNK)
+            sig = jax.nn.sigmoid(gate[rows, lanes(half)].astype(WIDE))
+            gated = (value[rows, lanes(half)].astype(WIDE) * sig).astype(NARROW)
+            padded[half, EDGE + start : EDGE + start + CHUNK] = gated.astype(WIDE)
     for half in range(HALVES):
         gain_row = gain[0:1, lanes(half)]
         gain_sum = jnp.zeros((8, LANES), WIDE)
@@ -98,7 +88,7 @@
             active = normed * gain_row
             sig = jax.nn.sigmoid(active)
             hidden[rows, lanes(half)] = (active * sig).astype(NARROW)
-            d_active = upstream[half, rows] * sig * (1.0 + active * (1.0 - sig))
+            d_active = upstream[rows, lanes(half)] * sig * (1.0 + active * (1.0 - sig))
             gain_sum = gain_sum + jnp.sum((d_active * normed).reshape(CHUNK // 8, 8, LANES), 0)
             d_normed = d_active * gain_row
             scaled[half, rows] = factor * d_normed
@@ -212,7 +202,7 @@
         total = arrived[0, rows].astype(WIDE)
         for near in range(1, CLOSE):
             total = total + arrived[near, rows].astype(WIDE)
-        pieces[far, :, 0:WIDTH] = total.astype(NARROW)
+        pieces[FAR_ORDER.index(far), :, 0:WIDTH] = total.astype(NARROW)
     both = arrived[0, FAR * OWN :].astype(WIDE)
     for near in range(1, CLOSE):
         both = both + arrived[near, FAR * OWN :].astype(WIDE)
@@ -249,9 +239,8 @@
     end = (proj_value[ROWS - EDGE :].astype(WIDE) * end_gate).astype(NARROW)
     halo = shifted(end, SP, 1)
     split = (HALVES, ROWS, LANES)
-    body, upstream = call(
-        gate_and_upstream, [(split, WIDE), (split, WIDE)],
-        proj_value, proj_gate, out_cotangent, out_weight, flops=2 * ROWS * WIDTH * MODEL,
+    upstream = lax.dot_general(
+        out_cotangent, out_weight, (((1,), (1,)), ((), ())), preferred_element_type=WIDE
     )
     column_scratch = [pltpu.VMEM((ROWS, LANES), WIDE)] * 4
     taps_scratch = pltpu.VMEM((TAPS + 1, WIDTH), WIDE)
@@ -262,7 +251,7 @@
             ((ROWS, WIDTH), NARROW), ((TP, 8, LANES), WIDE), ((HALVES, 8, LANES), WIDE),
         ],
         [taps_scratch, *column_scratch],
-        halo, body, upstream, conv_taps, norm_gain.reshape(1, WIDTH), row_mean, row_scale,
+        halo, proj_value, proj_gate, upstream, conv_taps, norm_gain.reshape(1, WIDTH), row_mean, row_scale,
         flops=100 * ROWS * WIDTH,
     )
     sums = exchange(message, "tp")
@@ -280,7 +269,7 @@
     (pieces,) = call(
         fold_near, [((FAR, OWN, WIDTH + LANES), NARROW)], exchange(pieces, NEAR), flops=1 << 20
     )
-    arrived = exchange(pieces, "zh")
+    arrived = exchange(pieces, "zh", FAR_ORDER)
     d_gated, margin = call_with(
         gated_gradient, [(split, WIDE), ((HALVES, EDGE, LANES), WIDE)], [taps_scratch],
         extended, conv_taps, flops=100 * ROWS * WIDTH,
@@ -300,7 +289,7 @@
     return (value_grad, gate_grad, weight_grad, taps_grad, gain_grad.reshape(WIDTH))
 
 
-def call_with(body, outs, scratch, *args, flops=0, limit=24):
+def call_with(body, outs, scratch, *args, flops=0, limit=6):
     shapes = [jax.ShapeDtypeStruct(shape, dtype) for shape, dtype in outs]
     size = sum(a.size * a.dtype.itemsize for a in (*args, *shapes))
     return pl.pallas_call(
@@ -309,7 +298,6 @@
         scratch_shapes=scratch,
         compiler_params=pltpu.CompilerParams(vmem_limit_bytes=limit << 20),
         cost_estimate=pl.CostEstimate(flops=flops, bytes_accessed=size, transcendentals=0),
-        name=body.__name__,
     )(*args)
 
 
@@ -320,7 +308,7 @@
         out_shape=[jax.ShapeDtypeStruct(shape, dtype) for shape, dtype in outs],
         in_specs=[pl.BlockSpec(memory_space=pltpu.SMEM), whole, whole],
         out_specs=[whole, whole],
-        compiler_params=pltpu.CompilerParams(vmem_limit_bytes=24 << 20),
+        compiler_params=pltpu.CompilerParams(vmem_limit_bytes=6 << 20),
         cost_estimate=pl.CostEstimate(
             flops=2 * ROWS * WIDTH * MODEL, bytes_accessed=4 << 20, transcendentals=0
         ),

time: 106 us -> 94.3 us (0.89)
  blocking collectives: 68.7 us -> 61.3 us
  local copies, waits for them, and re-layouts: 4.51 us -> 0.04 us
  matrix products: 0 us -> 2.01 us
  starting transfers between devices: 18 us -> 16.7 us
    all_to_all x3, blocking collectives: 68.7 us -> 61.3 us  [exchange(): lax.all_to_all(pieces, axes, 0, 0, tiled=True, axis_index_groups=groups)]
    unnamed x22 -> x16, local copies, waits for them, and re-layouts: 4.51 us -> 0.04 us
    dot_general x0 -> x1, matrix products: none -> 2.01 us  [shards(): lax.dot_general(out_cotangent, out_weight, (((1,), (1,)), ((), ())), pref...]
    all_to_all x1, starting transfers between devices: 9.77 us -> 8.3 us  [exchange(): lax.all_to_all(pieces, axes, 0, 0, tiled=True, axis_index_groups=groups)]
    pallas_call x5 -> x4, Pallas kernels: 2.91 us -> 2.25 us  [call(): pl.pallas_call(body, out_shape=shapes, compiler_params=pltpu.CompilerPara...]
  transfers between devices with their start and end apart: 4 -> 4, of which waited for: 1 -> 1; matrix products, arithmetic and copies ran while one was open for 0% -> 2% of each run, Pallas kernels for 2% -> 2%
where the time goes in v4:
time: 94.3 us; the launch traced here: 93.8 us
  blocking collectives  61.3 us (65%)
  starting transfers between devices  16.7 us (18%)
  Pallas kernels  7.08 us (8%)
  waiting for transfers between devices  5.05 us (5%)
  matrix products  2.01 us (2%)
    all_to_all x3, blocking collectives, exchange(): lax.all_to_all(pieces, axes, 0, 0, tiled=True, axis_index_groups=groups)  61.3 us
    all_to_all x1, starting transfers between devices, exchange(): lax.all_to_all(pieces, axes, 0, 0, tiled=True, axis_index_groups=groups)  8.3 us
    ppermute x2, starting transfers between devices, shifted(): lax.ppermute(value, axis, [(source, source + steps) for source in range(f...  6.45 us
    ppermute x2, waiting for transfers between devices, shifted(): lax.ppermute(value, axis, [(source, source + steps) for source in range(f...  5.04 us
    pallas_call x3, Pallas kernels, call_with(): pl.pallas_call(body, out_shape=shapes, scratch_shapes=scratch, compiler_p...  4.06 us
    pallas_call x4, Pallas kernels, call(): pl.pallas_call(body, out_shape=shapes, compiler_params=pltpu.CompilerPara...  2.25 us
    dot_general x1, matrix products, shards(): lax.dot_general(out_cotangent, out_weight, (((1,), (1,)), ((), ())), pref...  2.01 us
    ppermute x1, starting transfers between devices, shards(): other = lax.ppermute(other, 'c', [(0, 1), (1, 0)])  1.92 us
  transfers between devices with their start and end apart: 4, of which 1 were waited for; matrix products, arithmetic and copies ran while one was open for 2% of the time, Pallas kernels for 2%

profile of v4, /device:TPU:7, one launch (start us, length us, event | category | flops | bytes accessed | tf_op | source)
XLA Modules:
  0.0 93.8 jit_solution(9310303805128117706)
XLA Ops:
  0.6 0.0 copy-start
  0.6 0.0 copy-start.2
  0.7 0.0 copy-start.3
  0.7 0.0 copy-start.5
  0.7 0.0 copy-start.4
  0.7 0.0 copy-start.6
  0.7 0.0 copy-start.7
  0.7 0.9 multiply_convert_fusion
  1.6 0.0 copy-start.1
  1.6 4.2 %collective-permute-start = (bf16[32,256]{1,0:T(8,128)(2,1)S(1)}, bf16[32,256]{1,0:T(8,128)(2,1)S(1)}, u32[]{:S(2)}, u32[]{:S(2)}) collective-permute-start(bf16[32,256]{1,0:T(8,128)(2,1)S(1)} %multiply_convert_fusion), channel_id=1, source_target_pairs={{0,4},{4,8},{8,12},{12,16},{16,20},{20,24},{24,28},{28,32},{32,36}... | collective-permute-start | bytes 49160 | tf_op jit(solution)/shard_map/ppermute | solution.py:33
  5.7 0.0 copy-done
  5.7 2.0 %fusion.upstream = f32[384,256]{1,0:T(8,128)S(1)} fusion(bf16[384,2048]{1,0:T(8,128)(2,1)} %cotangent.1, bf16[256,2048]{1,0:T(8,128)(2,1)S(1)} %copy-done), kind=kOutput, calls=%fused_computation.1 | convolution fusion | flops 402653184 | bytes 3014656 | tf_op jit(solution)/shard_map/dot_general | solution.py:242
  7.8 0.0 collective-permute-done.halo
  7.8 0.0 copy-done.2
  7.8 0.0 copy-done.3
  7.8 0.0 copy-done.5
  7.8 0.0 copy-done.4
  7.8 0.0 copy-done.6
  7.8 0.0 copy-done.7
  7.8 1.5 %shard_map.119 = (f32[2,416,128]{2,1,0:T(8,128)S(1)}, f32[2,384,128]{2,1,0:T(8,128)S(1)}, f32[2,384,128]{2,1,0:T(8,128)S(1)}, bf16[384,256]{1,0:T(8,128)(2,1)S(1...) custom-call(bf16[32,256]{1,0:T(8,128)(2,1)S(1)} %collective-permute-done.halo, bf16[384,256]{1,0:T(8,128)(2,1)S(1)} %copy-done.3, ...), custom_call_target="tpu_custom_call" | custom-call | flops 9830400 | bytes 2256384 | tf_op jit(solution)/shard_map/pallas_call | solution.py:295
  9.3 0.0 copy-done.1
  9.3 0.8 weight_product.1
  10.1 1.9 %collective-permute-start.1 = (bf16[8,16,8,256]{3,2,1,0:T(8,128)(2,1)S(1)}, bf16[8,16,8,256]{3,2,1,0:T(8,128)(2,1)S(1)}, u32[]{:S(2)}, u32[]{:S(2)}) collective-permute-start(bf16[8,16,8,256]{3,2,1,0:T(8,128)(2,1)S(1)} %get-tuple-element.30), channel_id=1, source_target_pairs={{0,4},{4,0},{1,5},{5,1},{2,6},{6,2},{3,7},{7,3},{8,12},{12,8},{9,1... | collective-permute-start | bytes 1572872 | tf_op jit(solution)/shard_map/ppermute | solution.py:261
  12.0 8.2 %all_to_all.20.sums = f32[4,8,128]{2,1,0:T(8,128)S(1)} all-to-all(f32[4,8,128]{2,1,0:T(8,128)S(1)} %get-tuple-element.23), channel_id=1, replica_groups=mesh['zh'=16,'zl'=2,'x'=4,'c'=2,'tp'=4] {'tp'}, dimensions={0} | all-to-all | bytes 32768 | tf_op jit(solution)/shard_map/all_to_all | solution.py:38
  20.2 0.0 collective-permute-done.1.other
  20.2 1.8 %shard_map.120 = (bf16[8,136,256]{2,1,0:T(8,128)(2,1)S(1)}, f32[2,448,128]{2,1,0:T(8,128)S(1)}) custom-call(f32[4,8,128]{2,1,0:T(8,128)S(1)} %all_to_all.20.sums, f32[2,384,128]{2,1,0:T(8,128)S(1)} %get-tuple-element.24.scaled, f32[2,384,128]{2,1,0:T(8,128)S(1)} %get-tuple-element.25.spread, f32[2,416,128]{2,1,0:T(8,128)S(1)} %get-tuple-element.26.padded, ...), custom_call_target="tpu_custom_call" | custom-call | flops 9830400 | bytes 3827200 | tf_op jit(solution)/shard_map/pallas_call | solution.py:295
  22.0 19.0 %all_to_all.21.arrived = bf16[8,136,256]{2,1,0:T(8,128)(2,1)S(1)} all-to-all(bf16[8,136,256]{2,1,0:T(8,128)(2,1)S(1)} %get-tuple-element.36), channel_id=1, replica_groups=mesh['zh'=16,'zl'=2,'x'=4,'c'=2,'tp'=4] {'zl','x'}, dimensions={0} | all-to-all | bytes 1114112 | tf_op jit(solution)/shard_map/all_to_all | solution.py:38
  41.0 0.1 shard_map.123
  41.1 34.1 %all_to_all.22.arrived = bf16[16,8,384]{2,1,0:T(8,128)(2,1)S(1)} all-to-all(bf16[16,8,384]{2,1,0:T(8,128)(2,1)S(1)} %shard_map.123), channel_id=1, replica_groups={{640,704,768,832,896,960,0,64,128,192,256,320,384,448,512,576},{641,705..., dimensions={0} | all-to-all | bytes 196608 | tf_op jit(solution)/shard_map/all_to_all | solution.py:38
  75.2 0.7 shard_map.124
  75.8 8.3 %all-to-all-start.3 = ((f32[16,8,128]{2,1,0:T(8,128)}), f32[16,8,128]{2,1,0:T(8,128)S(1)}, u32[]{:S(2)}, u32[]{:S(2)}) async-start(f32[16,8,128]{2,1,0:T(8,128)} %get-tuple-element.38), calls=%async_computation.3 | async-start | bytes 131072 | tf_op jit(solution)/shard_map/all_to_all | solution.py:38
  84.1 0.9 shard_map.121
  85.0 2.3 %collective-permute-start.2 = (f32[2,32,128]{2,1,0:T(8,128)S(1)}, f32[2,32,128]{2,1,0:T(8,128)S(1)}, u32[]{:S(2)}, u32[]{:S(2)}) collective-permute-start(f32[2,32,128]{2,1,0:T(8,128)S(1)} %get-tuple-element.33), channel_id=1, source_target_pairs={{4,0},{8,4},{12,8},{16,12},{20,16},{24,20},{28,24},{32,28},{36,32}... | collective-permute-start | bytes 98312 | tf_op jit(solution)/shard_map/ppermute | solution.py:33
  87.3 5.0 %collective-permute-done.2.arrived = f32[2,32,128]{2,1,0:T(8,128)S(1)} collective-permute-done((f32[2,32,128]{2,1,0:T(8,128)S(1)}, f32[2,32,128]{2,1,0:T(8,128)S(1)}, u32[]{:S(2)}, u32[]{:S(2)}) %collective-permute-start.2) | collective-permute-done | bytes 32800 | tf_op jit(solution)/shard_map/ppermute | solution.py:33
  92.3 0.9 shard_map.122
  93.2 0.0 all-to-all-done.3.arrived
  93.2 0.6 shard_map.125
Async XLA Ops:
  0.6 5.1 %copy-start = (bf16[256,2048]{1,0:T(8,128)(2,1)S(1)}, bf16[256,2048]{1,0:T(8,128)(2,1)}, u32[]{:S(2)}) copy-start(bf16[256,2048]{1,0:T(8,128)(2,1)} %param.11) | copy-start | bytes 3145732
  0.6 7.1 %copy-start.2 = (bf16[384,256]{1,0:T(8,128)(2,1)S(1)}, bf16[384,256]{1,0:T(8,128)(2,1)}, u32[]{:S(2)}) copy-start(bf16[384,256]{1,0:T(8,128)(2,1)} %gate.3) | copy-start | bytes 589828
  0.7 7.1 %copy-start.3 = (bf16[384,256]{1,0:T(8,128)(2,1)S(1)}, bf16[384,256]{1,0:T(8,128)(2,1)}, u32[]{:S(2)}) copy-start(bf16[384,256]{1,0:T(8,128)(2,1)} %value.3) | copy-start | bytes 589828
  0.7 7.1 %copy-start.5 = (f32[384]{0:T(512)S(1)}, f32[384]{0:T(512)}, u32[]{:S(2)}) copy-start(f32[384]{0:T(512)} %scale.3) | copy-start | bytes 4612
  0.7 7.1 %copy-start.4 = (bf16[31,256]{1,0:T(8,128)(2,1)S(1)}, bf16[31,256]{1,0:T(8,128)(2,1)}, u32[]{:S(2)}) copy-start(bf16[31,256]{1,0:T(8,128)(2,1)} %taps.3) | copy-start | bytes 47620
  0.7 7.1 %copy-start.6 = (f32[384]{0:T(512)S(1)}, f32[384]{0:T(512)}, u32[]{:S(2)}) copy-start(f32[384]{0:T(512)} %mean.1) | copy-start | bytes 4612
  0.7 7.1 %copy-start.7 = (f32[256]{0:T(256)S(1)}, f32[256]{0:T(256)}, u32[]{:S(2)}) copy-start(f32[256]{0:T(256)} %param.13) | copy-start | bytes 3076
  1.6 7.7 %copy-start.1 = (bf16[384,2048]{1,0:T(8,128)(2,1)S(1)}, bf16[384,2048]{1,0:T(8,128)(2,1)}, u32[]{:S(2)}) copy-start(bf16[384,2048]{1,0:T(8,128)(2,1)} %cotangent.1) | copy-start | bytes 4718596
  1.6 6.2 %collective-permute-start = (bf16[32,256]{1,0:T(8,128)(2,1)S(1)}, bf16[32,256]{1,0:T(8,128)(2,1)S(1)}, u32[]{:S(2)}, u32[]{:S(2)}) collective-permute-start(bf16[32,256]{1,0:T(8,128)(2,1)S(1)} %multiply_convert_fusion), channel_id=1, source_target_pairs={{0,4},{4,8},{8,12},{12,16},{16,20},{20,24},{24,28},{28,32},{32,36}... | collective-permute-start | bytes 49160 | tf_op jit(solution)/shard_map/ppermute | solution.py:33
  10.1 10.1 %collective-permute-start.1 = (bf16[8,16,8,256]{3,2,1,0:T(8,128)(2,1)S(1)}, bf16[8,16,8,256]{3,2,1,0:T(8,128)(2,1)S(1)}, u32[]{:S(2)}, u32[]{:S(2)}) collective-permute-start(bf16[8,16,8,256]{3,2,1,0:T(8,128)(2,1)S(1)} %get-tuple-element.30), channel_id=1, source_target_pairs={{0,4},{4,0},{1,5},{5,1},{2,6},{6,2},{3,7},{7,3},{8,12},{12,8},{9,1... | collective-permute-start | bytes 1572872 | tf_op jit(solution)/shard_map/ppermute | solution.py:261
  75.8 17.4 %all-to-all-start.3 = ((f32[16,8,128]{2,1,0:T(8,128)}), f32[16,8,128]{2,1,0:T(8,128)S(1)}, u32[]{:S(2)}, u32[]{:S(2)}) async-start(f32[16,8,128]{2,1,0:T(8,128)} %get-tuple-element.38), calls=%async_computation.3 | async-start | bytes 131072 | tf_op jit(solution)/shard_map/all_to_all | solution.py:38
  85.0 7.3 %collective-permute-start.2 = (f32[2,32,128]{2,1,0:T(8,128)S(1)}, f32[2,32,128]{2,1,0:T(8,128)S(1)}, u32[]{:S(2)}, u32[]{:S(2)}) collective-permute-start(f32[2,32,128]{2,1,0:T(8,128)S(1)} %get-tuple-element.33), channel_id=1, source_target_pairs={{4,0},{8,4},{12,8},{16,12},{20,16},{24,20},{28,24},{32,28},{36,32}... | collective-permute-start | bytes 98312 | tf_op jit(solution)/shard_map/ppermute | solution.py:33

commit v5 on v4

--- a/solution.py
+++ b/solution.py
@@ -13,6 +13,7 @@
 CLOSE = 8
 AXES = (("zh", FAR), ("zl", 2), ("x", 4), ("c", 2))
 FAR_ORDER = [(place + 10) % FAR for place in range(FAR)]
+GATHER_ORDER = [place ^ 1 for place in range(CLOSE * 2)]
 TP = 4
 TAPS = 31
 ROWS = 384
@@ -107,9 +108,7 @@
             turned = jnp.transpose(source[block * LANES : (block + 1) * LANES])
             found.append(jnp.sum(turned, 0, keepdims=True))
     found.append(jnp.zeros((2, LANES), WIDE))
-    sums = jnp.concatenate(found, 0)
-    for peer in range(TP):
-        message[peer] = sums
+    message[...] = jnp.concatenate(found, 0)
 
 
 def weight_product(core, cotangent, hidden, mine, other):
@@ -131,13 +130,11 @@
 
 
 def backward(
-    sums, scaled, spread, padded, scale, gain_part, mine, other,
+    sums_0, sums_1, sums_2, sums_3, scaled, spread, padded, scale, gain_part, mine, other,
     pieces, extended,
     small,
 ):
-    total = sums[0]
-    for peer in range(1, TP):
-        total = total + sums[peer]
+    total = (sums_0[...] + sums_1[...]) + (sums_2[...] + sums_3[...])
     total = total * (1.0 / (TP * WIDTH))
     blocks = ROWS // LANES
     for half in range(HALVES):
@@ -212,16 +209,19 @@
         pieces[far, :, WIDTH:] = small
 
 
-def fold_far(arrived, weight_grad, message):
-    total = arrived[0].astype(WIDE)
+def fold_far(arrived, message):
+    total = arrived[0, :, WIDTH:].astype(WIDE)
     for far in range(1, FAR):
-        total = total + arrived[far].astype(WIDE)
-    weight_grad[...] = total[:, 0:WIDTH]
+        total = total + arrived[far, :, WIDTH:].astype(WIDE)
     for peer in range(CLOSE * 2):
-        message[peer] = total[:, WIDTH:]
-
-
-def finish(arrived, taps_grad, gain_grad):
+        message[peer] = total
+
+
+def finish(arrived, weights, taps_grad, gain_grad, weight_grad):
+    total = weights[0, :, 0:WIDTH].astype(WIDE)
+    for far in range(1, FAR):
+        total = total + weights[far, :, 0:WIDTH].astype(WIDE)
+    weight_grad[...] = total
     for near in range(CLOSE):
         total = arrived[2 * near] + arrived[2 * near + 1]
         total = jnp.concatenate([total[0:4], total[4:8]], 1)
@@ -248,13 +248,16 @@
         forward,
         [
             ((HALVES, EDGE + ROWS, LANES), WIDE), (split, WIDE), (split, WIDE),
-            ((ROWS, WIDTH), NARROW), ((TP, 8, LANES), WIDE), ((HALVES, 8, LANES), WIDE),
+            ((ROWS, WIDTH), NARROW), ((8, LANES), WIDE), ((HALVES, 8, LANES), WIDE),
         ],
         [taps_scratch, *column_scratch],
         halo, proj_value, proj_gate, upstream, conv_taps, norm_gain.reshape(1, WIDTH), row_mean, row_scale,
         flops=100 * ROWS * WIDTH,
     )
-    sums = exchange(message, "tp")
+    sums = [message]
+    for step in range(1, TP):
+        pairs = [(place, (place + step) % TP) for place in range(TP)]
+        sums.append(lax.ppermute(message, "tp", pairs))
     core = lax.axis_index("c").reshape(1)
     grouped = (CLOSE, FAR, OWN, WIDTH)
     mine, other = weight_call(core, out_cotangent, hidden, [(grouped, WIDE), (grouped, NARROW)])
@@ -263,7 +266,7 @@
         backward,
         [((CLOSE, FAR * OWN + 8, WIDTH), NARROW), ((HALVES, ROWS + 2 * EDGE, LANES), WIDE)],
         [pltpu.VMEM((TAPS + 1, WIDTH), WIDE)],
-        sums, scaled, spread, padded, row_scale, gain_part, mine, other,
+        *sums, scaled, spread, padded, row_scale, gain_part, mine, other,
         flops=100 * ROWS * WIDTH,
     )
     (pieces,) = call(
@@ -279,12 +282,12 @@
         outputs, [((ROWS, WIDTH), NARROW), ((ROWS, WIDTH), NARROW)],
         d_gated, late, proj_value, proj_gate, flops=10 * ROWS * WIDTH,
     )
-    weight_grad, message = call(
-        fold_far, [((OWN, WIDTH), WIDE), ((CLOSE * 2, 8, LANES), WIDE)], arrived, flops=1 << 16
-    )
-    taps_grad, gain_grad = call(
-        finish, [((TAPS, WIDTH), WIDE), ((1, WIDTH), WIDE)],
-        exchange(message, (*NEAR, "c")), flops=1 << 16,
+    (message,) = call(
+        fold_far, [((CLOSE * 2, 8, LANES), WIDE)], arrived, flops=1 << 16
+    )
+    taps_grad, gain_grad, weight_grad = call(
+        finish, [((TAPS, WIDTH), WIDE), ((1, WIDTH), WIDE), ((OWN, WIDTH), WIDE)],
+        exchange(message, (*NEAR, "c"), GATHER_ORDER), arrived, flops=1 << 16,
     )
     return (value_grad, gate_grad, weight_grad, taps_grad, gain_grad.reshape(WIDTH))
 

time: 94.3 us -> 97.6 us (1.035)
  starting transfers between devices: 16.7 us -> 25.3 us
  blocking collectives: 61.3 us -> 53 us
  waiting for transfers between devices: 5.05 us -> 7.99 us
    ppermute x0 -> x3, starting transfers between devices: none -> 9.5 us  [shards(): sums.append(lax.ppermute(message, 'tp', pairs))]
    all_to_all x3 -> x2, blocking collectives: 61.3 us -> 53 us  [exchange(): lax.all_to_all(pieces, axes, 0, 0, tiled=True, axis_index_groups=groups)]
    ppermute x0 -> x3, waiting for transfers between devices: none -> 2.95 us  [shards(): sums.append(lax.ppermute(message, 'tp', pairs))]
  transfers between devices with their start and end apart: 4 -> 7, of which waited for: 1 -> 3; matrix products, arithmetic and copies ran while one was open for 2% -> 2% of each run, Pallas kernels for 2% -> 2%
where the time goes in v5:
time: 97.6 us; the launch traced here: 97.2 us
  blocking collectives  53 us (54%)
  starting transfers between devices  25.3 us (26%)
  waiting for transfers between devices  7.99 us (8%)
  Pallas kernels  7.06 us (7%)
  matrix products  2.01 us (2%)
    all_to_all x2, blocking collectives, exchange(): lax.all_to_all(pieces, axes, 0, 0, tiled=True, axis_index_groups=groups)  53 us
    ppermute x3, starting transfers between devices, shards(): sums.append(lax.ppermute(message, 'tp', pairs))  9.5 us
    all_to_all x1, starting transfers between devices, exchange(): lax.all_to_all(pieces, axes, 0, 0, tiled=True, axis_index_groups=groups)  7.46 us
    ppermute x2, starting transfers between devices, shifted(): lax.ppermute(value, axis, [(source, source + steps) for source in range(f...  6.46 us
    ppermute x2, waiting for transfers between devices, shifted(): lax.ppermute(value, axis, [(source, source + steps) for source in range(f...  5.03 us
    pallas_call x3, Pallas kernels, call_with(): pl.pallas_call(body, out_shape=shapes, scratch_shapes=scratch, compiler_p...  4.05 us
    ppermute x3, waiting for transfers between devices, shards(): sums.append(lax.ppermute(message, 'tp', pairs))  2.95 us
    pallas_call x4, Pallas kernels, call(): pl.pallas_call(body, out_shape=shapes, compiler_params=pltpu.CompilerPara...  2.24 us
  transfers between devices with their start and end apart: 7, of which 3 were waited for; matrix products, arithmetic and copies ran while one was open for 2% of the time, Pallas kernels for 2%

profile of v5, /device:TPU:7, one launch (start us, length us, event | category | flops | bytes accessed | tf_op | source)
XLA Modules:
  0.0 97.2 jit_solution(11623925501661796689)
XLA Ops:
  0.6 0.0 copy-start
  0.6 0.0 copy-start.2
  0.7 0.0 copy-start.3
  0.7 0.0 copy-start.5
  0.7 0.0 copy-start.4
  0.7 0.0 copy-start.6
  0.7 0.0 copy-start.7
  0.7 0.9 multiply_convert_fusion
  1.6 0.0 copy-start.1
  1.6 4.2 %collective-permute-start = (bf16[32,256]{1,0:T(8,128)(2,1)S(1)}, bf16[32,256]{1,0:T(8,128)(2,1)S(1)}, u32[]{:S(2)}, u32[]{:S(2)}) collective-permute-start(bf16[32,256]{1,0:T(8,128)(2,1)S(1)} %multiply_convert_fusion), channel_id=1, source_target_pairs={{0,4},{4,8},{8,12},{12,16},{16,20},{20,24},{24,28},{28,32},{32,36}... | collective-permute-start | bytes 49160 | tf_op jit(solution)/shard_map/ppermute | solution.py:34
  5.7 0.0 copy-done
  5.7 2.0 %fusion.upstream = f32[384,256]{1,0:T(8,128)S(1)} fusion(bf16[384,2048]{1,0:T(8,128)(2,1)} %cotangent.1, bf16[256,2048]{1,0:T(8,128)(2,1)S(1)} %copy-done), kind=kOutput, calls=%fused_computation.1 | convolution fusion | flops 402653184 | bytes 3014656 | tf_op jit(solution)/shard_map/dot_general | solution.py:242
  7.8 0.0 collective-permute-done.halo
  7.8 0.0 copy-done.2
  7.8 0.0 copy-done.3
  7.8 0.0 copy-done.5
  7.8 0.0 copy-done.4
  7.8 0.0 copy-done.6
  7.8 0.0 copy-done.7
  7.8 1.5 %shard_map.119 = (f32[2,416,128]{2,1,0:T(8,128)S(1)}, f32[2,384,128]{2,1,0:T(8,128)S(1)}, f32[2,384,128]{2,1,0:T(8,128)S(1)}, bf16[384,256]{1,0:T(8,128)(2,1)S(1...) custom-call(bf16[32,256]{1,0:T(8,128)(2,1)S(1)} %collective-permute-done.halo, bf16[384,256]{1,0:T(8,128)(2,1)S(1)} %copy-done.3, ...), custom_call_target="tpu_custom_call" | custom-call | flops 9830400 | bytes 2244096 | tf_op jit(solution)/shard_map/pallas_call | solution.py:298
  9.3 0.0 copy-done.1
  9.3 0.8 weight_product.1
  10.1 1.9 %collective-permute-start.4 = (bf16[8,16,8,256]{3,2,1,0:T(8,128)(2,1)S(1)}, bf16[8,16,8,256]{3,2,1,0:T(8,128)(2,1)S(1)}, u32[]{:S(2)}, u32[]{:S(2)}) collective-permute-start(bf16[8,16,8,256]{3,2,1,0:T(8,128)(2,1)S(1)} %get-tuple-element.29), channel_id=1, source_target_pairs={{0,4},{4,0},{1,5},{5,1},{2,6},{6,2},{3,7},{7,3},{8,12},{12,8},{9,1... | collective-permute-start | bytes 1572872 | tf_op jit(solution)/shard_map/ppermute | solution.py:264
  12.0 4.6 %collective-permute-start.3 = (f32[8,128]{1,0:T(8,128)S(1)}, f32[8,128]{1,0:T(8,128)S(1)}, u32[]{:S(2)}, u32[]{:S(2)}) collective-permute-start(f32[8,128]{1,0:T(8,128)S(1)} %get-tuple-element.22.sums_0), channel_id=1, source_target_pairs={{0,3},{1,0},{2,1},{3,2},{4,7},{5,4},{6,5},{7,6},{8,11},{9,8},{10,9... | collective-permute-start | bytes 12296 | tf_op jit(solution)/shard_map/ppermute | solution.py:260
  16.7 2.3 %collective-permute-start.2 = (f32[8,128]{1,0:T(8,128)S(1)}, f32[8,128]{1,0:T(8,128)S(1)}, u32[]{:S(2)}, u32[]{:S(2)}) collective-permute-start(f32[8,128]{1,0:T(8,128)S(1)} %get-tuple-element.22.sums_0), channel_id=1, source_target_pairs={{0,2},{1,3},{2,0},{3,1},{4,6},{5,7},{6,4},{7,5},{8,10},{9,11},{10,... | collective-permute-start | bytes 12296 | tf_op jit(solution)/shard_map/ppermute | solution.py:260
  18.9 2.6 %collective-permute-start.1 = (f32[8,128]{1,0:T(8,128)S(1)}, f32[8,128]{1,0:T(8,128)S(1)}, u32[]{:S(2)}, u32[]{:S(2)}) collective-permute-start(f32[8,128]{1,0:T(8,128)S(1)} %get-tuple-element.22.sums_0), channel_id=1, source_target_pairs={{0,1},{1,2},{2,3},{3,0},{4,5},{5,6},{6,7},{7,4},{8,9},{9,10},{10,1... | collective-permute-start | bytes 12296 | tf_op jit(solution)/shard_map/ppermute | solution.py:260
  21.5 0.0 collective-permute-done.3.sums_3
  21.6 1.0 %collective-permute-done.2.sums_2 = f32[8,128]{1,0:T(8,128)S(1)} collective-permute-done((f32[8,128]{1,0:T(8,128)S(1)}, f32[8,128]{1,0:T(8,128)S(1)}, u32[]{:S(2)}, u32[]{:S(2)}) %collective-permute-start.2) | collective-permute-done | bytes 4128 | tf_op jit(solution)/shard_map/ppermute | solution.py:260
  22.5 2.0 %collective-permute-done.1.sums_1 = f32[8,128]{1,0:T(8,128)S(1)} collective-permute-done((f32[8,128]{1,0:T(8,128)S(1)}, f32[8,128]{1,0:T(8,128)S(1)}, u32[]{:S(2)}, u32[]{:S(2)}) %collective-permute-start.1) | collective-permute-done | bytes 4128 | tf_op jit(solution)/shard_map/ppermute | solution.py:260
  24.5 0.0 collective-permute-done.4.other
  24.5 1.7 %shard_map.120 = (bf16[8,136,256]{2,1,0:T(8,128)(2,1)S(1)}, f32[2,448,128]{2,1,0:T(8,128)S(1)}) custom-call(f32[8,128]{1,0:T(8,128)S(1)} %get-tuple-element.22.sums_0, f32[8,128]{1,0:T(8,128)S(1)} %collective-permute-done.1.sums_1, f32[8,128]{1,0:T(8,128)S(1)} %collective-permute-done.2.sums_2, f32[8,128]{1,0:T(8,128)S(1)} %collective-permute-done.3.sums_3, ...), custom_call_target="tpu_custom_call" | custom-call | flops 9830400 | bytes 3827200 | tf_op jit(solution)/shard_map/pallas_call | solution.py:298
  26.3 18.4 %all_to_all.15.arrived = bf16[8,136,256]{2,1,0:T(8,128)(2,1)S(1)} all-to-all(bf16[8,136,256]{2,1,0:T(8,128)(2,1)S(1)} %get-tuple-element.35), channel_id=1, replica_groups=mesh['zh'=16,'zl'=2,'x'=4,'c'=2,'tp'=4] {'zl','x'}, dimensions={0} | all-to-all | bytes 1114112 | tf_op jit(solution)/shard_map/all_to_all | solution.py:39
  44.7 0.1 shard_map.123
  44.8 34.6 %all_to_all.16.arrived.weights = bf16[16,8,384]{2,1,0:T(8,128)(2,1)S(1)} all-to-all(bf16[16,8,384]{2,1,0:T(8,128)(2,1)S(1)} %shard_map.123), channel_id=1, replica_groups={{640,704,768,832,896,960,0,64,128,192,256,320,384,448,512,576},{641,705..., dimensions={0} | all-to-all | bytes 196608 | tf_op jit(solution)/shard_map/all_to_all | solution.py:39
  79.3 0.6 shard_map.124
  80.0 7.5 %all-to-all-start.2 = ((f32[16,8,128]{2,1,0:T(8,128)}), f32[16,8,128]{2,1,0:T(8,128)S(1)}, u32[]{:S(2)}, u32[]{:S(2)}) async-start(f32[16,8,128]{2,1,0:T(8,128)} %shard_map.124), calls=%async_computation.2 | async-start | bytes 131072 | tf_op jit(solution)/shard_map/all_to_all | solution.py:39
  87.4 0.9 shard_map.121
  88.3 2.3 %collective-permute-start.5 = (f32[2,32,128]{2,1,0:T(8,128)S(1)}, f32[2,32,128]{2,1,0:T(8,128)S(1)}, u32[]{:S(2)}, u32[]{:S(2)}) collective-permute-start(f32[2,32,128]{2,1,0:T(8,128)S(1)} %get-tuple-element.32), channel_id=1, source_target_pairs={{4,0},{8,4},{12,8},{16,12},{20,16},{24,20},{28,24},{32,28},{36,32}... | collective-permute-start | bytes 98312 | tf_op jit(solution)/shard_map/ppermute | solution.py:34
  90.6 5.0 %collective-permute-done.5.arrived = f32[2,32,128]{2,1,0:T(8,128)S(1)} collective-permute-done((f32[2,32,128]{2,1,0:T(8,128)S(1)}, f32[2,32,128]{2,1,0:T(8,128)S(1)}, u32[]{:S(2)}, u32[]{:S(2)}) %collective-permute-start.5) | collective-permute-done | bytes 32800 | tf_op jit(solution)/shard_map/ppermute | solution.py:34
  95.6 0.9 shard_map.122
  96.5 0.0 all-to-all-done.2.arrived
  96.5 0.6 shard_map.125
Async XLA Ops:
  0.6 5.1 %copy-start = (bf16[256,2048]{1,0:T(8,128)(2,1)S(1)}, bf16[256,2048]{1,0:T(8,128)(2,1)}, u32[]{:S(2)}) copy-start(bf16[256,2048]{1,0:T(8,128)(2,1)} %param.11) | copy-start | bytes 3145732
  0.6 7.1 %copy-start.2 = (bf16[384,256]{1,0:T(8,128)(2,1)S(1)}, bf16[384,256]{1,0:T(8,128)(2,1)}, u32[]{:S(2)}) copy-start(bf16[384,256]{1,0:T(8,128)(2,1)} %gate.3) | copy-start | bytes 589828
  0.7 7.1 %copy-start.3 = (bf16[384,256]{1,0:T(8,128)(2,1)S(1)}, bf16[384,256]{1,0:T(8,128)(2,1)}, u32[]{:S(2)}) copy-start(bf16[384,256]{1,0:T(8,128)(2,1)} %value.3) | copy-start | bytes 589828
  0.7 7.1 %copy-start.5 = (f32[384]{0:T(512)S(1)}, f32[384]{0:T(512)}, u32[]{:S(2)}) copy-start(f32[384]{0:T(512)} %scale.3) | copy-start | bytes 4612
  0.7 7.1 %copy-start.4 = (bf16[31,256]{1,0:T(8,128)(2,1)S(1)}, bf16[31,256]{1,0:T(8,128)(2,1)}, u32[]{:S(2)}) copy-start(bf16[31,256]{1,0:T(8,128)(2,1)} %taps.3) | copy-start | bytes 47620
  0.7 7.1 %copy-start.6 = (f32[384]{0:T(512)S(1)}, f32[384]{0:T(512)}, u32[]{:S(2)}) copy-start(f32[384]{0:T(512)} %mean.1) | copy-start | bytes 4612
  0.7 7.1 %copy-start.7 = (f32[256]{0:T(256)S(1)}, f32[256]{0:T(256)}, u32[]{:S(2)}) copy-start(f32[256]{0:T(256)} %param.13) | copy-start | bytes 3076
  1.6 7.7 %copy-start.1 = (bf16[384,2048]{1,0:T(8,128)(2,1)S(1)}, bf16[384,2048]{1,0:T(8,128)(2,1)}, u32[]{:S(2)}) copy-start(bf16[384,2048]{1,0:T(8,128)(2,1)} %cotangent.1) | copy-start | bytes 4718596
  1.6 6.2 %collective-permute-start = (bf16[32,256]{1,0:T(8,128)(2,1)S(1)}, bf16[32,256]{1,0:T(8,128)(2,1)S(1)}, u32[]{:S(2)}, u32[]{:S(2)}) collective-permute-start(bf16[32,256]{1,0:T(8,128)(2,1)S(1)} %multiply_convert_fusion), channel_id=1, source_target_pairs={{0,4},{4,8},{8,12},{12,16},{16,20},{20,24},{24,28},{28,32},{32,36}... | collective-permute-start | bytes 49160 | tf_op jit(solution)/shard_map/ppermute | solution.py:34
  10.1 14.4 %collective-permute-start.4 = (bf16[8,16,8,256]{3,2,1,0:T(8,128)(2,1)S(1)}, bf16[8,16,8,256]{3,2,1,0:T(8,128)(2,1)S(1)}, u32[]{:S(2)}, u32[]{:S(2)}) collective-permute-start(bf16[8,16,8,256]{3,2,1,0:T(8,128)(2,1)S(1)} %get-tuple-element.29), channel_id=1, source_target_pairs={{0,4},{4,0},{1,5},{5,1},{2,6},{6,2},{3,7},{7,3},{8,12},{12,8},{9,1... | collective-permute-start | bytes 1572872 | tf_op jit(solution)/shard_map/ppermute | solution.py:264
  12.0 9.5 %collective-permute-start.3 = (f32[8,128]{1,0:T(8,128)S(1)}, f32[8,128]{1,0:T(8,128)S(1)}, u32[]{:S(2)}, u32[]{:S(2)}) collective-permute-start(f32[8,128]{1,0:T(8,128)S(1)} %get-tuple-element.22.sums_0), channel_id=1, source_target_pairs={{0,3},{1,0},{2,1},{3,2},{4,7},{5,4},{6,5},{7,6},{8,11},{9,8},{10,9... | collective-permute-start | bytes 12296 | tf_op jit(solution)/shard_map/ppermute | solution.py:260
  16.7 5.9 %collective-permute-start.2 = (f32[8,128]{1,0:T(8,128)S(1)}, f32[8,128]{1,0:T(8,128)S(1)}, u32[]{:S(2)}, u32[]{:S(2)}) collective-permute-start(f32[8,128]{1,0:T(8,128)S(1)} %get-tuple-element.22.sums_0), channel_id=1, source_target_pairs={{0,2},{1,3},{2,0},{3,1},{4,6},{5,7},{6,4},{7,5},{8,10},{9,11},{10,... | collective-permute-start | bytes 12296 | tf_op jit(solution)/shard_map/ppermute | solution.py:260
  18.9 5.6 %collective-permute-start.1 = (f32[8,128]{1,0:T(8,128)S(1)}, f32[8,128]{1,0:T(8,128)S(1)}, u32[]{:S(2)}, u32[]{:S(2)}) collective-permute-start(f32[8,128]{1,0:T(8,128)S(1)} %get-tuple-element.22.sums_0), channel_id=1, source_target_pairs={{0,1},{1,2},{2,3},{3,0},{4,5},{5,6},{6,7},{7,4},{8,9},{9,10},{10,1... | collective-permute-start | bytes 12296 | tf_op jit(solution)/shard_map/ppermute | solution.py:260
  80.0 16.5 %all-to-all-start.2 = ((f32[16,8,128]{2,1,0:T(8,128)}), f32[16,8,128]{2,1,0:T(8,128)S(1)}, u32[]{:S(2)}, u32[]{:S(2)}) async-start(f32[16,8,128]{2,1,0:T(8,128)} %shard_map.124), calls=%async_computation.2 | async-start | bytes 131072 | tf_op jit(solution)/shard_map/all_to_all | solution.py:39
  88.3 7.3 %collective-permute-start.5 = (f32[2,32,128]{2,1,0:T(8,128)S(1)}, f32[2,32,128]{2,1,0:T(8,128)S(1)}, u32[]{:S(2)}, u32[]{:S(2)}) collective-permute-start(f32[2,32,128]{2,1,0:T(8,128)S(1)} %get-tuple-element.32), channel_id=1, source_target_pairs={{4,0},{8,4},{12,8},{16,12},{20,16},{24,20},{28,24},{32,28},{36,32}... | collective-permute-start | bytes 98312 | tf_op jit(solution)/shard_map/ppermute | solution.py:34

commit v6 on v5

--- a/solution.py
+++ b/solution.py
@@ -13,8 +13,8 @@
 CLOSE = 8
 AXES = (("zh", FAR), ("zl", 2), ("x", 4), ("c", 2))
 FAR_ORDER = [(place + 10) % FAR for place in range(FAR)]
-GATHER_ORDER = [place ^ 1 for place in range(CLOSE * 2)]
 TP = 4
+PARTS = 4
 TAPS = 31
 ROWS = 384
 EDGE = 32
@@ -58,10 +58,33 @@
     )(*args)
 
 
+def norm_backward(conv, mean, factor, gain_row, upstream):
+    normed = (conv - mean) * factor
+    active = normed * gain_row
+    sig = jax.nn.sigmoid(active)
+    hidden = (active * sig).astype(NARROW)
+    d_active = upstream * sig * (1.0 + active * (1.0 - sig))
+    d_normed = d_active * gain_row
+    gain_part = jnp.sum((d_active * normed).reshape(conv.shape[0] // 8, 8, LANES), 0)
+    return hidden, factor * d_normed, factor * normed, d_normed, d_normed * normed, gain_part
+
+
+def convolve(source, half, taps_wide, start, size):
+    conv = jnp.zeros((size, LANES), WIDE)
+    for tap in range(TAPS):
+        begin = start + tap + EDGE - TAPS + 1
+        conv = conv + taps_wide[tap : tap + 1, lanes(half)] * source[half, begin : begin + size]
+    return conv
+
+
+def column_sums(source):
+    return jnp.sum(jnp.transpose(source), 0, keepdims=True)
+
+
 def forward(
-    halo, value, gate, upstream, taps, gain, mean, scale,
-    padded, scaled, spread, hidden, message, gain_part,
-    taps_wide, mean_columns, scale_columns, sum_first, sum_second,
+    value, gate, upstream, taps, gain, mean, scale,
+    gated, scaled, spread, hidden, sums, gain_part,
+    padded, taps_wide, mean_columns, scale_columns, sum_first, sum_second,
 ):
     taps_wide[0:TAPS] = taps[...].astype(WIDE)
     for block in range(ROWS // LANES):
@@ -69,59 +92,105 @@
         mean_columns[rows] = column(mean[rows].reshape(1, LANES))
         scale_columns[rows] = column(scale[rows].reshape(1, LANES))
     for half in range(HALVES):
-        padded[half, 0:EDGE] = halo[:, lanes(half)].astype(WIDE)
         for start in range(0, ROWS, CHUNK):
             rows = slice(start, start + CHUNK)
             sig = jax.nn.sigmoid(gate[rows, lanes(half)].astype(WIDE))
-            gated = (value[rows, lanes(half)].astype(WIDE) * sig).astype(NARROW)
-            padded[half, EDGE + start : EDGE + start + CHUNK] = gated.astype(WIDE)
+            product = (value[rows, lanes(half)].astype(WIDE) * sig).astype(NARROW)
+            gated[rows, lanes(half)] = product
+            padded[half, EDGE + start : EDGE + start + CHUNK] = product.astype(WIDE)
+    sum_first[0:EDGE] = jnp.zeros((EDGE, LANES), WIDE)
+    sum_second[0:EDGE] = jnp.zeros((EDGE, LANES), WIDE)
     for half in range(HALVES):
         gain_row = gain[0:1, lanes(half)]
         gain_sum = jnp.zeros((8, LANES), WIDE)
-        for start in range(0, ROWS, CHUNK):
-            rows = slice(start, start + CHUNK)
-            conv = jnp.zeros((CHUNK, LANES), WIDE)
-            for tap in range(TAPS):
-                begin = start + tap + EDGE - TAPS + 1
-                conv = conv + taps_wide[tap : tap + 1, lanes(half)] * padded[half, begin : begin + CHUNK]
-            factor = scale_columns[rows]
-            normed = (conv - mean_columns[rows]) * factor
-            active = normed * gain_row
-            sig = jax.nn.sigmoid(active)
-            hidden[rows, lanes(half)] = (active * sig).astype(NARROW)
-            d_active = upstream[rows, lanes(half)] * sig * (1.0 + active * (1.0 - sig))
-            gain_sum = gain_sum + jnp.sum((d_active * normed).reshape(CHUNK // 8, 8, LANES), 0)
-            d_normed = d_active * gain_row
-            scaled[half, rows] = factor * d_normed
-            spread[half, rows] = factor * normed
-            weighted = d_normed * normed
+        for start in range(EDGE, ROWS, EDGE):
+            rows = slice(start, start + EDGE)
+            conv = convolve(padded, half, taps_wide, start, EDGE)
+            narrow, own_scaled, own_spread, first, second, part = norm_backward(
+                conv, mean_columns[rows], scale_columns[rows], gain_row, upstream[rows, lanes(half)]
+            )
+            hidden[start - EDGE : start, lanes(half)] = narrow
+            scaled[half, start - EDGE : start] = own_scaled
+            spread[half, start - EDGE : start] = own_spread
+            gain_sum = gain_sum + part
             if half == 0:
-                sum_first[rows] = d_normed
-                sum_second[rows] = weighted
+                sum_first[rows] = first
+                sum_second[rows] = second
             else:
-                sum_first[rows] = sum_first[rows] + d_normed
-                sum_second[rows] = sum_second[rows] + weighted
+                sum_first[rows] = sum_first[rows] + first
+                sum_second[rows] = sum_second[rows] + second
         gain_part[half] = gain_sum
-    found = []
-    for source in (sum_first, sum_second):
-        for block in range(ROWS // LANES):
-            turned = jnp.transpose(source[block * LANES : (block + 1) * LANES])
-            found.append(jnp.sum(turned, 0, keepdims=True))
-    found.append(jnp.zeros((2, LANES), WIDE))
-    message[...] = jnp.concatenate(found, 0)
-
-
-def weight_product(core, cotangent, hidden, mine, other):
+    found = [
+        column_sums(source[block * LANES : (block + 1) * LANES])
+        for source in (sum_first, sum_second)
+        for block in range(ROWS // LANES)
+    ]
+    sums[...] = jnp.concatenate([*found, jnp.zeros((2, LANES), WIDE)], 0)
+
+
+def head(
+    halo, gated, upstream, taps, gain, mean, scale, sums, gain_part,
+    scaled, spread, hidden, message, gain_total,
+    padded, taps_wide, turned,
+):
+    taps_wide[0:TAPS] = taps[...].astype(WIDE)
+    rows = slice(0, EDGE)
+    mean_columns = column(mean[0:LANES].reshape(1, LANES))[rows]
+    scale_columns = column(scale[0:LANES].reshape(1, LANES))[rows]
+    turned[...] = jnp.zeros((2, LANES, LANES), WIDE)
+    for half in range(HALVES):
+        padded[half, rows] = halo[:, lanes(half)].astype(WIDE)
+        padded[half, EDGE:] = gated[rows, lanes(half)].astype(WIDE)
+    for half in range(HALVES):
+        conv = convolve(padded, half, taps_wide, 0, EDGE)
+        narrow, own_scaled, own_spread, first, second, part = norm_backward(
+            conv, mean_columns, scale_columns, gain[0:1, lanes(half)], upstream[rows, lanes(half)]
+        )
+        hidden[:, lanes(half)] = narrow
+        scaled[half] = own_scaled
+        spread[half] = own_spread
+        gain_total[half] = gain_part[half] + part
+        turned[0, rows] = turned[0, rows] + first
+        turned[1, rows] = turned[1, rows] + second
+    blocks = ROWS // LANES
+    total = sums[...]
+    extra = [column_sums(turned[0]), column_sums(turned[1])]
+    none = jnp.zeros((blocks - 1, LANES), WIDE)
+    last = jnp.zeros((2, LANES), WIDE)
+    total = total + jnp.concatenate([extra[0], none, extra[1], none, last], 0)
+    for peer in range(TP):
+        message[peer] = total
+
+
+def weight_product(
+    core, cotangent, hidden, first_hidden, mine, other, held, whole, kept, arrivals, departure
+):
+    copies = []
+    for part in range(PARTS):
+        columns = pl.ds(part * (MODEL // PARTS), MODEL // PARTS)
+        copies.append(
+            pltpu.make_async_copy(
+                cotangent.at[:, columns], held.at[:, columns], arrivals.at[part]
+            )
+        )
+        copies[-1].start()
+    whole[0:EDGE] = first_hidden[...]
+    whole[EDGE:] = hidden[...]
     first = core[0] == 0
     for far in range(FAR):
+        if far % (FAR // PARTS) == 0:
+            copies[far // (FAR // PARTS)].wait()
         part = lax.dot_general(
-            cotangent[:, lanes(far)], hidden[...], (((0,), (0,)), ((), ())),
+            held[:, lanes(far)], whole[...], (((0,), (0,)), ((), ())),
             preferred_element_type=WIDE,
         )
         part = part.reshape(CLOSE, 2, OWN, WIDTH)
         low, high = part[:, 0], part[:, 1]
-        mine[:, far] = jnp.where(first, low, high)
+        kept[:, far] = jnp.where(first, low, high)
         other[:, far] = jnp.where(first, high, low).astype(NARROW)
+    leaving = pltpu.make_async_copy(kept, mine, departure)
+    leaving.start()
+    leaving.wait()
 
 
 def halves(value):
@@ -130,11 +199,20 @@
 
 
 def backward(
-    sums_0, sums_1, sums_2, sums_3, scaled, spread, padded, scale, gain_part, mine, other,
+    mine, other, sums, scaled, spread, first_scaled, first_spread, halo, gated, scale, gain_part,
     pieces, extended,
-    small,
+    small, padded, held_mine, held_other, arrivals,
 ):
-    total = (sums_0[...] + sums_1[...]) + (sums_2[...] + sums_3[...])
+    copies = [
+        pltpu.make_async_copy(mine, held_mine, arrivals.at[0]),
+        pltpu.make_async_copy(other, held_other, arrivals.at[1]),
+    ]
+    for copy in copies:
+        copy.start()
+    for half in range(HALVES):
+        padded[half, 0:EDGE] = halo[:, lanes(half)].astype(WIDE)
+        padded[half, EDGE:] = gated[:, lanes(half)].astype(WIDE)
+    total = (sums[0] + sums[1]) + (sums[2] + sums[3])
     total = total * (1.0 / (TP * WIDTH))
     blocks = ROWS // LANES
     for half in range(HALVES):
@@ -145,22 +223,39 @@
         first = column(total[block : block + 1] * scale[rows].reshape(1, LANES))
         second = column(total[blocks + block : blocks + block + 1])
         for half in range(HALVES):
-            d_conv = scaled[half, rows] - first - spread[half, rows] * second
-            extended[half, EDGE + block * LANES : EDGE + (block + 1) * LANES] = d_conv
-    for half in range(HALVES):
-        for group in range(0, TAPS, 8):
-            members = range(group, min(group + 8, TAPS))
-            found = [jnp.zeros((8, LANES), WIDE) for _ in members]
-            for start in range(0, ROWS, 8):
-                d_conv = extended[half, EDGE + start : EDGE + start + 8]
-                for i, tap in enumerate(members):
-                    begin = start + tap + EDGE - TAPS + 1
-                    found[i] = found[i] + d_conv * padded[half, begin : begin + 8]
-            for i, tap in enumerate(members):
-                small[tap : tap + 1, lanes(half)] = jnp.sum(found[i], 0, keepdims=True)
+            cut = 0
+            if block == 0:
+                cut = EDGE
+                d_conv = first_scaled[half] - first[0:cut] - first_spread[half] * second[0:cut]
+                extended[half, EDGE : EDGE + cut] = d_conv
+            rows = slice(block * LANES + cut - EDGE, (block + 1) * LANES - EDGE)
+            d_conv = scaled[half, rows] - first[cut:] - spread[half, rows] * second[cut:]
+            extended[half, EDGE + block * LANES + cut : EDGE + (block + 1) * LANES] = d_conv
+    lead = EDGE - TAPS + 1
+    groups = ROWS // 8
+    for offset in range(8):
+        steps = [q for q in range(5) if 0 <= 8 * q + offset - lead < TAPS]
+        found = {(half, q): jnp.zeros((8, LANES), WIDE) for half in range(HALVES) for q in steps}
+        loaded = {}
+        for m in range(groups + steps[-1]):
+            for half in range(HALVES):
+                if m < groups:
+                    begin = EDGE + 8 * m
+                    loaded[half, m] = extended[half, begin : begin + 8]
+                moved = padded[half, 8 * m + offset : 8 * m + offset + 8]
+                for q in steps:
+                    if 0 <= m - q < groups:
+                        found[half, q] = found[half, q] + loaded[half, m - q] * moved
+        for half in range(HALVES):
+            for q in steps:
+                tap = 8 * q + offset - lead
+                small[tap : tap + 1, lanes(half)] = jnp.sum(found[half, q], 0, keepdims=True)
+    for half in range(HALVES):
         small[TAPS : TAPS + 1, lanes(half)] = jnp.sum(gain_part[half], 0, keepdims=True)
+    for copy in copies:
+        copy.wait()
     for near in range(CLOSE):
-        chip = mine[near] + other[near].astype(WIDE)
+        chip = held_mine[near] + held_other[near].astype(WIDE)
         pieces[near, 0 : FAR * OWN] = chip.reshape(FAR * OWN, WIDTH).astype(NARROW)
         high, low = halves(small[near * 4 : near * 4 + 4])
         pieces[near, FAR * OWN :] = jnp.concatenate([high.astype(WIDE), low.astype(WIDE)], 0).astype(NARROW)
@@ -242,31 +337,50 @@
     upstream = lax.dot_general(
         out_cotangent, out_weight, (((1,), (1,)), ((), ())), preferred_element_type=WIDE
     )
-    column_scratch = [pltpu.VMEM((ROWS, LANES), WIDE)] * 4
+    rest = (HALVES, ROWS - EDGE, LANES)
+    row_gain = norm_gain.reshape(1, WIDTH)
+    sides = pltpu.VMEM((HALVES, EDGE + ROWS, LANES), WIDE)
     taps_scratch = pltpu.VMEM((TAPS + 1, WIDTH), WIDE)
-    padded, scaled, spread, hidden, message, gain_part = call_with(
+    gated, scaled, spread, hidden, sums, gain_part = call_with(
         forward,
         [
-            ((HALVES, EDGE + ROWS, LANES), WIDE), (split, WIDE), (split, WIDE),
-            ((ROWS, WIDTH), NARROW), ((8, LANES), WIDE), ((HALVES, 8, LANES), WIDE),
-        ],
-        [taps_scratch, *column_scratch],
-        halo, proj_value, proj_gate, upstream, conv_taps, norm_gain.reshape(1, WIDTH), row_mean, row_scale,
+            ((ROWS, WIDTH), NARROW), (rest, WIDE), (rest, WIDE),
+            ((ROWS - EDGE, WIDTH), NARROW), ((8, LANES), WIDE), ((HALVES, 8, LANES), WIDE),
+        ],
+        [sides, taps_scratch, *([pltpu.VMEM((ROWS, LANES), WIDE)] * 4)],
+        proj_value, proj_gate, upstream, conv_taps, row_gain, row_mean, row_scale,
         flops=100 * ROWS * WIDTH,
     )
-    sums = [message]
-    for step in range(1, TP):
-        pairs = [(place, (place + step) % TP) for place in range(TP)]
-        sums.append(lax.ppermute(message, "tp", pairs))
+    edge = (HALVES, EDGE, LANES)
+    first_scaled, first_spread, first_hidden, message, gain_part = call_with(
+        head,
+        [
+            (edge, WIDE), (edge, WIDE), ((EDGE, WIDTH), NARROW),
+            ((TP, 8, LANES), WIDE), ((HALVES, 8, LANES), WIDE),
+        ],
+        [
+            pltpu.VMEM((HALVES, 2 * EDGE, LANES), WIDE),
+            taps_scratch,
+            pltpu.VMEM((2, LANES, LANES), WIDE),
+        ],
+        halo, gated, upstream, conv_taps, row_gain, row_mean, row_scale, sums, gain_part,
+        flops=10 * ROWS * WIDTH,
+    )
+    sums = exchange(message, "tp")
     core = lax.axis_index("c").reshape(1)
     grouped = (CLOSE, FAR, OWN, WIDTH)
-    mine, other = weight_call(core, out_cotangent, hidden, [(grouped, WIDE), (grouped, NARROW)])
+    mine, other = weight_call(core, out_cotangent, hidden, first_hidden, [(grouped, WIDE), (grouped, NARROW)])
     other = lax.ppermute(other, "c", [(0, 1), (1, 0)])
     pieces, extended = call_with(
         backward,
         [((CLOSE, FAR * OWN + 8, WIDTH), NARROW), ((HALVES, ROWS + 2 * EDGE, LANES), WIDE)],
-        [pltpu.VMEM((TAPS + 1, WIDTH), WIDE)],
-        *sums, scaled, spread, padded, row_scale, gain_part, mine, other,
+        [
+            taps_scratch, sides, pltpu.VMEM(grouped, WIDE), pltpu.VMEM(grouped, NARROW),
+            pltpu.SemaphoreType.DMA((2,)),
+        ],
+        mine, other,
+        sums, scaled, spread, first_scaled, first_spread, halo, gated, row_scale, gain_part,
+        in_hbm=2,
         flops=100 * ROWS * WIDTH,
     )
     (pieces,) = call(
@@ -287,36 +401,53 @@
     )
     taps_grad, gain_grad, weight_grad = call(
         finish, [((TAPS, WIDTH), WIDE), ((1, WIDTH), WIDE), ((OWN, WIDTH), WIDE)],
-        exchange(message, (*NEAR, "c"), GATHER_ORDER), arrived, flops=1 << 16,
+        exchange(message, (*NEAR, "c")), arrived, flops=1 << 16,
     )
     return (value_grad, gate_grad, weight_grad, taps_grad, gain_grad.reshape(WIDTH))
 
 
-def call_with(body, outs, scratch, *args, flops=0, limit=6):
+def call_with(body, outs, scratch, *args, flops=0, limit=6, in_hbm=0):
     shapes = [jax.ShapeDtypeStruct(shape, dtype) for shape, dtype in outs]
     size = sum(a.size * a.dtype.itemsize for a in (*args, *shapes))
+    far = [pltpu.with_memory_space_constraint(a, pltpu.HBM) for a in args[:in_hbm]]
+    specs = [pl.BlockSpec(memory_space=pltpu.HBM)] * in_hbm
+    specs += [pl.BlockSpec(memory_space=pltpu.VMEM)] * (len(args) - in_hbm)
     return pl.pallas_call(
         body,
         out_shape=shapes,
+        in_specs=specs,
         scratch_shapes=scratch,
         compiler_params=pltpu.CompilerParams(vmem_limit_bytes=limit << 20),
         cost_estimate=pl.CostEstimate(flops=flops, bytes_accessed=size, transcendentals=0),
-    )(*args)
-
-
-def weight_call(core, cotangent, hidden, outs):
+    )(*far, *args[in_hbm:])
+
+
+def weight_call(core, cotangent, hidden, first_hidden, outs):
     whole = pl.BlockSpec(memory_space=pltpu.VMEM)
+    cotangent = pltpu.with_memory_space_constraint(cotangent, pltpu.HBM)
     return pl.pallas_call(
         weight_product,
-        out_shape=[jax.ShapeDtypeStruct(shape, dtype) for shape, dtype in outs],
-        in_specs=[pl.BlockSpec(memory_space=pltpu.SMEM), whole, whole],
-        out_specs=[whole, whole],
+        out_shape=[pltpu.HBM(*outs[0]), jax.ShapeDtypeStruct(*outs[1])],
+        in_specs=[
+            pl.BlockSpec(memory_space=pltpu.SMEM),
+            pl.BlockSpec(memory_space=pltpu.HBM),
+            whole,
+            whole,
+        ],
+        out_specs=[pl.BlockSpec(memory_space=pltpu.HBM), whole],
+        scratch_shapes=[
+            pltpu.VMEM((ROWS, MODEL), NARROW),
+            pltpu.VMEM((ROWS, WIDTH), NARROW),
+            pltpu.VMEM(*outs[0]),
+            pltpu.SemaphoreType.DMA((PARTS,)),
+            pltpu.SemaphoreType.DMA,
+        ],
         compiler_params=pltpu.CompilerParams(vmem_limit_bytes=6 << 20),
         cost_estimate=pl.CostEstimate(
             flops=2 * ROWS * WIDTH * MODEL, bytes_accessed=4 << 20, transcendentals=0
         ),
         name="weight_product",
-    )(core, cotangent, hidden)
+    )(core, cotangent, hidden, first_hidden)
 
 
 def solution(mesh):

time: 97.6 us -> 95.7 us (0.981)
  starting transfers between devices: 25.3 us -> 17.5 us
  blocking collectives: 53 us -> 58.7 us
  waiting for transfers between devices: 7.99 us -> 5.05 us
  Pallas kernels: 7.06 us -> 9.46 us
    ppermute x3 -> x0, starting transfers between devices: 9.5 us -> none  [shards(): sums.append(lax.ppermute(message, 'tp', pairs))]
    all_to_all x2 -> x3, blocking collectives: 53 us -> 58.7 us  [exchange(): lax.all_to_all(pieces, axes, 0, 0, tiled=True, axis_index_groups=groups)]
    ppermute x3 -> x0, waiting for transfers between devices: 2.95 us -> none  [shards(): sums.append(lax.ppermute(message, 'tp', pairs))]
    pallas_call x4 -> x5, Pallas kernels: 4.82 us -> 7.22 us  [the longest x4 3.81 us: call_with(): pl.pallas_call(body, out_shape=shapes, in_specs=specs, scratch_shapes=scr...]
    all_to_all x1, starting transfers between devices: 7.46 us -> 9.25 us  [exchange(): lax.all_to_all(pieces, axes, 0, 0, tiled=True, axis_index_groups=groups)]
  transfers between devices with their start and end apart: 7 -> 4, of which waited for: 3 -> 1; matrix products, arithmetic and copies ran while one was open for 2% -> 2% of each run, Pallas kernels for 2% -> 3%
where the time goes in v6:
time: 95.7 us; the launch traced here: 95.3 us
  blocking collectives  58.7 us (61%)
  starting transfers between devices  17.5 us (18%)
  Pallas kernels  9.46 us (10%)
  waiting for transfers between devices  5.05 us (5%)
  matrix products  2.01 us (2%)
    all_to_all x3, blocking collectives, exchange(): lax.all_to_all(pieces, axes, 0, 0, tiled=True, axis_index_groups=groups)  58.7 us
    all_to_all x1, starting transfers between devices, exchange(): lax.all_to_all(pieces, axes, 0, 0, tiled=True, axis_index_groups=groups)  9.25 us
    ppermute x2, starting transfers between devices, shifted(): lax.ppermute(value, axis, [(source, source + steps) for source in range(f...  6.32 us
    ppermute x2, waiting for transfers between devices, shifted(): lax.ppermute(value, axis, [(source, source + steps) for source in range(f...  5.04 us
    pallas_call x4, Pallas kernels, call_with(): pl.pallas_call(body, out_shape=shapes, in_specs=specs, scratch_shapes=scr...  3.81 us
    pallas_call x1, Pallas kernels, weight_call(): pl.pallas_call(weight_product, out_shape=[pltpu.HBM(*outs[0]), jax.ShapeD...  3.41 us
    pallas_call x4, Pallas kernels, call(): pl.pallas_call(body, out_shape=shapes, compiler_params=pltpu.CompilerPara...  2.24 us
    dot_general x1, matrix products, shards(): lax.dot_general(out_cotangent, out_weight, (((1,), (1,)), ((), ())), pref...  2.01 us
  transfers between devices with their start and end apart: 4, of which 1 were waited for; matrix products, arithmetic and copies ran while one was open for 2% of the time, Pallas kernels for 3%

profile of v6, /device:TPU:7, one launch (start us, length us, event | category | flops | bytes accessed | tf_op | source)
XLA Modules:
  0.0 95.3 jit_solution(5511620024809099144)
XLA Ops:
  0.6 0.0 copy-start
  0.6 0.0 copy-start.2
  0.7 0.0 copy-start.1
  0.7 0.0 copy-start.4
  0.7 0.0 copy-start.3
  0.7 0.0 copy-start.5
  0.7 0.0 copy-start.6
  0.7 0.9 multiply_convert_fusion
  1.6 4.0 %collective-permute-start = (bf16[32,256]{1,0:T(8,128)(2,1)S(1)}, bf16[32,256]{1,0:T(8,128)(2,1)S(1)}, u32[]{:S(2)}, u32[]{:S(2)}) collective-permute-start(bf16[32,256]{1,0:T(8,128)(2,1)S(1)} %multiply_convert_fusion), channel_id=1, source_target_pairs={{0,4},{4,8},{8,12},{12,16},{16,20},{20,24},{24,28},{28,32},{32,36}... | collective-permute-start | bytes 49160 | tf_op jit(solution)/shard_map/ppermute | solution.py:34
  5.6 0.0 copy-done
  5.6 2.0 %fusion.upstream = f32[384,256]{1,0:T(8,128)S(1)} fusion(bf16[384,2048]{1,0:T(8,128)(2,1)} %cotangent.1, bf16[256,2048]{1,0:T(8,128)(2,1)S(1)} %copy-done), kind=kOutput, calls=%fused_computation.1 | convolution fusion | flops 402653184 | bytes 3014656 | tf_op jit(solution)/shard_map/dot_general | solution.py:337
  7.6 0.0 copy-done.2
  7.6 0.0 copy-done.1
  7.7 0.0 copy-done.4
  7.7 0.0 copy-done.3
  7.7 0.0 copy-done.5
  7.7 0.0 copy-done.6
  7.7 1.3 %shard_map.119 = (bf16[384,256]{1,0:T(8,128)(2,1)S(1)}, f32[2,352,128]{2,1,0:T(8,128)S(1)}, f32[2,352,128]{2,1,0:T(8,128)S(1)}, bf16[352,256]{1,0:T(8,128)(2,1)S...) custom-call(bf16[384,256]{1,0:T(8,128)(2,1)S(1)} %copy-done.1, bf16[384,256]{1,0:T(8,128)(2,1)S(1)} %copy-done.2, ...), custom_call_target="tpu_custom_call" | custom-call | flops 9830400 | bytes 1916416 | tf_op jit(solution)/shard_map/pallas_call | solution.py:415
  9.0 0.0 collective-permute-done.halo
  9.0 0.2 shard_map.120
  9.2 3.4 %weight_product.1 = (f32[8,16,8,256]{3,2,1,0:T(8,128)}, bf16[8,16,8,256]{3,2,1,0:T(8,128)(2,1)S(1)}) custom-call(s32[1]{0:T(128)} %bitcast.core, bf16[384,2048]{1,0:T(8,128)(2,1)} %cotangent.1, bf16[352,256]{1,0:T(8,128)(2,1)S(1)} %get-tuple-element.27.hidden, bf16[32,256]{1,0:T(8,128)(2,1)S(1)} %get-tuple-element.31.first_hidden), custom_call_target="tpu_custom_call" | custom-call | flops 402653184 | bytes 4194304 | tf_op jit(solution)/shard_map/weight_product/pallas_call | solution.py:428
  12.6 1.9 %collective-permute-start.1 = (bf16[8,16,8,256]{3,2,1,0:T(8,128)(2,1)S(1)}, bf16[8,16,8,256]{3,2,1,0:T(8,128)(2,1)S(1)}, u32[]{:S(2)}, u32[]{:S(2)}) collective-permute-start(bf16[8,16,8,256]{3,2,1,0:T(8,128)(2,1)S(1)} %get-tuple-element.33), channel_id=1, source_target_pairs={{0,4},{4,0},{1,5},{5,1},{2,6},{6,2},{3,7},{7,3},{8,12},{12,8},{9,1... | collective-permute-start | bytes 1572872 | tf_op jit(solution)/shard_map/ppermute | solution.py:373
  14.5 8.2 %all_to_all.20.sums = f32[4,8,128]{2,1,0:T(8,128)S(1)} all-to-all(f32[4,8,128]{2,1,0:T(8,128)S(1)} %get-tuple-element.34), channel_id=1, replica_groups=mesh['zh'=16,'zl'=2,'x'=4,'c'=2,'tp'=4] {'tp'}, dimensions={0} | all-to-all | bytes 32768 | tf_op jit(solution)/shard_map/all_to_all | solution.py:39
  22.7 0.0 collective-permute-done.1.other
  22.7 0.0 copy-start.7
  22.7 0.8 copy-done.7
  23.6 1.5 %shard_map.121 = (bf16[8,136,256]{2,1,0:T(8,128)(2,1)S(1)}, f32[2,448,128]{2,1,0:T(8,128)S(1)}) custom-call(f32[8,16,8,256]{3,2,1,0:T(8,128)} %get-tuple-element.32.mine, bf16[8,16,8,256]{3,2,1,0:T(8,128)(2,1)} %copy-done.7, f32[4,8,128]{2,1,0:T(8,128)S(1)} %all_to_all.20.sums, f32[2,352,128]{2,1,0:T(8,128)S(1)} %get-tuple-element.35.scaled, ...), custom_call_target="tpu_custom_call" | custom-call | flops 9830400 | bytes 3614208 | tf_op jit(solution)/shard_map/pallas_call | solution.py:415
  25.0 19.0 %all_to_all.21.arrived = bf16[8,136,256]{2,1,0:T(8,128)(2,1)S(1)} all-to-all(bf16[8,136,256]{2,1,0:T(8,128)(2,1)S(1)} %get-tuple-element.45), channel_id=1, replica_groups=mesh['zh'=16,'zl'=2,'x'=4,'c'=2,'tp'=4] {'zl','x'}, dimensions={0} | all-to-all | bytes 1114112 | tf_op jit(solution)/shard_map/all_to_all | solution.py:39
  44.0 0.1 shard_map.124
  44.1 31.5 %all_to_all.22.arrived.weights = bf16[16,8,384]{2,1,0:T(8,128)(2,1)S(1)} all-to-all(bf16[16,8,384]{2,1,0:T(8,128)(2,1)S(1)} %shard_map.124), channel_id=1, replica_groups={{640,704,768,832,896,960,0,64,128,192,256,320,384,448,512,576},{641,705..., dimensions={0} | all-to-all | bytes 196608 | tf_op jit(solution)/shard_map/all_to_all | solution.py:39
  75.6 0.6 shard_map.125
  76.3 9.2 %all-to-all-start.3 = ((f32[16,8,128]{2,1,0:T(8,128)}), f32[16,8,128]{2,1,0:T(8,128)S(1)}, u32[]{:S(2)}, u32[]{:S(2)}) async-start(f32[16,8,128]{2,1,0:T(8,128)} %shard_map.125), calls=%async_computation.3 | async-start | bytes 131072 | tf_op jit(solution)/shard_map/all_to_all | solution.py:39
  85.5 0.9 shard_map.122
  86.4 2.3 %collective-permute-start.2 = (f32[2,32,128]{2,1,0:T(8,128)S(1)}, f32[2,32,128]{2,1,0:T(8,128)S(1)}, u32[]{:S(2)}, u32[]{:S(2)}) collective-permute-start(f32[2,32,128]{2,1,0:T(8,128)S(1)} %get-tuple-element.42), channel_id=1, source_target_pairs={{4,0},{8,4},{12,8},{16,12},{20,16},{24,20},{28,24},{32,28},{36,32}... | collective-permute-start | bytes 98312 | tf_op jit(solution)/shard_map/ppermute | solution.py:34
  88.7 5.0 %collective-permute-done.2.arrived = f32[2,32,128]{2,1,0:T(8,128)S(1)} collective-permute-done((f32[2,32,128]{2,1,0:T(8,128)S(1)}, f32[2,32,128]{2,1,0:T(8,128)S(1)}, u32[]{:S(2)}, u32[]{:S(2)}) %collective-permute-start.2) | collective-permute-done | bytes 32800 | tf_op jit(solution)/shard_map/ppermute | solution.py:34
  93.7 0.9 shard_map.123
  94.6 0.0 all-to-all-done.3.arrived
  94.6 0.6 shard_map.126
Async XLA Ops:
  0.6 5.0 %copy-start = (bf16[256,2048]{1,0:T(8,128)(2,1)S(1)}, bf16[256,2048]{1,0:T(8,128)(2,1)}, u32[]{:S(2)}) copy-start(bf16[256,2048]{1,0:T(8,128)(2,1)} %param.11) | copy-start | bytes 3145732
  0.6 7.0 %copy-start.2 = (bf16[384,256]{1,0:T(8,128)(2,1)S(1)}, bf16[384,256]{1,0:T(8,128)(2,1)}, u32[]{:S(2)}) copy-start(bf16[384,256]{1,0:T(8,128)(2,1)} %gate.3) | copy-start | bytes 589828
  0.7 7.0 %copy-start.1 = (bf16[384,256]{1,0:T(8,128)(2,1)S(1)}, bf16[384,256]{1,0:T(8,128)(2,1)}, u32[]{:S(2)}) copy-start(bf16[384,256]{1,0:T(8,128)(2,1)} %value.3) | copy-start | bytes 589828
  0.7 7.0 %copy-start.4 = (f32[384]{0:T(512)S(1)}, f32[384]{0:T(512)}, u32[]{:S(2)}) copy-start(f32[384]{0:T(512)} %scale.5) | copy-start | bytes 4612
  0.7 7.0 %copy-start.3 = (bf16[31,256]{1,0:T(8,128)(2,1)S(1)}, bf16[31,256]{1,0:T(8,128)(2,1)}, u32[]{:S(2)}) copy-start(bf16[31,256]{1,0:T(8,128)(2,1)} %taps.5) | copy-start | bytes 47620
  0.7 7.0 %copy-start.5 = (f32[384]{0:T(512)S(1)}, f32[384]{0:T(512)}, u32[]{:S(2)}) copy-start(f32[384]{0:T(512)} %mean.3) | copy-start | bytes 4612
  0.7 7.0 %copy-start.6 = (f32[256]{0:T(256)S(1)}, f32[256]{0:T(256)}, u32[]{:S(2)}) copy-start(f32[256]{0:T(256)} %param.13) | copy-start | bytes 3076
  1.6 7.4 %collective-permute-start = (bf16[32,256]{1,0:T(8,128)(2,1)S(1)}, bf16[32,256]{1,0:T(8,128)(2,1)S(1)}, u32[]{:S(2)}, u32[]{:S(2)}) collective-permute-start(bf16[32,256]{1,0:T(8,128)(2,1)S(1)} %multiply_convert_fusion), channel_id=1, source_target_pairs={{0,4},{4,8},{8,12},{12,16},{16,20},{20,24},{24,28},{28,32},{32,36}... | collective-permute-start | bytes 49160 | tf_op jit(solution)/shard_map/ppermute | solution.py:34
  12.6 10.1 %collective-permute-start.1 = (bf16[8,16,8,256]{3,2,1,0:T(8,128)(2,1)S(1)}, bf16[8,16,8,256]{3,2,1,0:T(8,128)(2,1)S(1)}, u32[]{:S(2)}, u32[]{:S(2)}) collective-permute-start(bf16[8,16,8,256]{3,2,1,0:T(8,128)(2,1)S(1)} %get-tuple-element.33), channel_id=1, source_target_pairs={{0,4},{4,0},{1,5},{5,1},{2,6},{6,2},{3,7},{7,3},{8,12},{12,8},{9,1... | collective-permute-start | bytes 1572872 | tf_op jit(solution)/shard_map/ppermute | solution.py:373
  22.7 0.8 copy-start.7
  76.3 18.3 %all-to-all-start.3 = ((f32[16,8,128]{2,1,0:T(8,128)}), f32[16,8,128]{2,1,0:T(8,128)S(1)}, u32[]{:S(2)}, u32[]{:S(2)}) async-start(f32[16,8,128]{2,1,0:T(8,128)} %shard_map.125), calls=%async_computation.3 | async-start | bytes 131072 | tf_op jit(solution)/shard_map/all_to_all | solution.py:39
  86.4 7.3 %collective-permute-start.2 = (f32[2,32,128]{2,1,0:T(8,128)S(1)}, f32[2,32,128]{2,1,0:T(8,128)S(1)}, u32[]{:S(2)}, u32[]{:S(2)}) collective-permute-start(f32[2,32,128]{2,1,0:T(8,128)S(1)} %get-tuple-element.42), channel_id=1, source_target_pairs={{4,0},{8,4},{12,8},{16,12},{20,16},{24,20},{28,24},{32,28},{36,32}... | collective-permute-start | bytes 98312 | tf_op jit(solution)/shard_map/ppermute | solution.py:34

commit v7 on v6

--- a/solution.py
+++ b/solution.py
@@ -14,7 +14,6 @@
 AXES = (("zh", FAR), ("zl", 2), ("x", 4), ("c", 2))
 FAR_ORDER = [(place + 10) % FAR for place in range(FAR)]
 TP = 4
-PARTS = 4
 TAPS = 31
 ROWS = 384
 EDGE = 32
@@ -162,35 +161,19 @@
         message[peer] = total
 
 
-def weight_product(
-    core, cotangent, hidden, first_hidden, mine, other, held, whole, kept, arrivals, departure
-):
-    copies = []
-    for part in range(PARTS):
-        columns = pl.ds(part * (MODEL // PARTS), MODEL // PARTS)
-        copies.append(
-            pltpu.make_async_copy(
-                cotangent.at[:, columns], held.at[:, columns], arrivals.at[part]
-            )
-        )
-        copies[-1].start()
+def weight_product(core, cotangent, hidden, first_hidden, mine, other, whole):
     whole[0:EDGE] = first_hidden[...]
     whole[EDGE:] = hidden[...]
     first = core[0] == 0
     for far in range(FAR):
-        if far % (FAR // PARTS) == 0:
-            copies[far // (FAR // PARTS)].wait()
         part = lax.dot_general(
-            held[:, lanes(far)], whole[...], (((0,), (0,)), ((), ())),
+            cotangent[:, lanes(far)], whole[...], (((0,), (0,)), ((), ())),
             preferred_element_type=WIDE,
         )
         part = part.reshape(CLOSE, 2, OWN, WIDTH)
         low, high = part[:, 0], part[:, 1]
-        kept[:, far] = jnp.where(first, low, high)
+        mine[:, far] = jnp.where(first, low, high)
         other[:, far] = jnp.where(first, high, low).astype(NARROW)
-    leaving = pltpu.make_async_copy(kept, mine, departure)
-    leaving.start()
-    leaving.wait()
 
 
 def halves(value):
@@ -199,16 +182,10 @@
 
 
 def backward(
-    mine, other, sums, scaled, spread, first_scaled, first_spread, halo, gated, scale, gain_part,
+    sums, scaled, spread, first_scaled, first_spread, halo, gated, scale, gain_part, mine, other,
     pieces, extended,
-    small, padded, held_mine, held_other, arrivals,
+    small, padded,
 ):
-    copies = [
-        pltpu.make_async_copy(mine, held_mine, arrivals.at[0]),
-        pltpu.make_async_copy(other, held_other, arrivals.at[1]),
-    ]
-    for copy in copies:
-        copy.start()
     for half in range(HALVES):
         padded[half, 0:EDGE] = halo[:, lanes(half)].astype(WIDE)
         padded[half, EDGE:] = gated[:, lanes(half)].astype(WIDE)
@@ -252,10 +229,8 @@
                 small[tap : tap + 1, lanes(half)] = jnp.sum(found[half, q], 0, keepdims=True)
     for half in range(HALVES):
         small[TAPS : TAPS + 1, lanes(half)] = jnp.sum(gain_part[half], 0, keepdims=True)
-    for copy in copies:
-        copy.wait()
     for near in range(CLOSE):
-        chip = held_mine[near] + held_other[near].astype(WIDE)
+        chip = mine[near] + other[near].astype(WIDE)
         pieces[near, 0 : FAR * OWN] = chip.reshape(FAR * OWN, WIDTH).astype(NARROW)
         high, low = halves(small[near * 4 : near * 4 + 4])
         pieces[near, FAR * OWN :] = jnp.concatenate([high.astype(WIDE), low.astype(WIDE)], 0).astype(NARROW)
@@ -374,13 +349,9 @@
     pieces, extended = call_with(
         backward,
         [((CLOSE, FAR * OWN + 8, WIDTH), NARROW), ((HALVES, ROWS + 2 * EDGE, LANES), WIDE)],
-        [
-            taps_scratch, sides, pltpu.VMEM(grouped, WIDE), pltpu.VMEM(grouped, NARROW),
-            pltpu.SemaphoreType.DMA((2,)),
-        ],
+        [taps_scratch, sides],
+        sums, scaled, spread, first_scaled, first_spread, halo, gated, row_scale, gain_part,
         mine, other,
-        sums, scaled, spread, first_scaled, first_spread, halo, gated, row_scale, gain_part,
-        in_hbm=2,
         flops=100 * ROWS * WIDTH,
     )
     (pieces,) = call(
@@ -406,42 +377,26 @@
     return (value_grad, gate_grad, weight_grad, taps_grad, gain_grad.reshape(WIDTH))
 
 
-def call_with(body, outs, scratch, *args, flops=0, limit=6, in_hbm=0):
+def call_with(body, outs, scratch, *args, flops=0, limit=6):
     shapes = [jax.ShapeDtypeStruct(shape, dtype) for shape, dtype in outs]
     size = sum(a.size * a.dtype.itemsize for a in (*args, *shapes))
-    far = [pltpu.with_memory_space_constraint(a, pltpu.HBM) for a in args[:in_hbm]]
-    specs = [pl.BlockSpec(memory_space=pltpu.HBM)] * in_hbm
-    specs += [pl.BlockSpec(memory_space=pltpu.VMEM)] * (len(args) - in_hbm)
     return pl.pallas_call(
         body,
         out_shape=shapes,
-        in_specs=specs,
         scratch_shapes=scratch,
         compiler_params=pltpu.CompilerParams(vmem_limit_bytes=limit << 20),
         cost_estimate=pl.CostEstimate(flops=flops, bytes_accessed=size, transcendentals=0),
-    )(*far, *args[in_hbm:])
+    )(*args)
 
 
 def weight_call(core, cotangent, hidden, first_hidden, outs):
     whole = pl.BlockSpec(memory_space=pltpu.VMEM)
-    cotangent = pltpu.with_memory_space_constraint(cotangent, pltpu.HBM)
     return pl.pallas_call(
         weight_product,
-        out_shape=[pltpu.HBM(*outs[0]), jax.ShapeDtypeStruct(*outs[1])],
-        in_specs=[
-            pl.BlockSpec(memory_space=pltpu.SMEM),
-            pl.BlockSpec(memory_space=pltpu.HBM),
-            whole,
-            whole,
-        ],
-        out_specs=[pl.BlockSpec(memory_space=pltpu.HBM), whole],
-        scratch_shapes=[
-            pltpu.VMEM((ROWS, MODEL), NARROW),
-            pltpu.VMEM((ROWS, WIDTH), NARROW),
-            pltpu.VMEM(*outs[0]),
-            pltpu.SemaphoreType.DMA((PARTS,)),
-            pltpu.SemaphoreType.DMA,
-        ],
+        out_shape=[jax.ShapeDtypeStruct(shape, dtype) for shape, dtype in outs],
+        in_specs=[pl.BlockSpec(memory_space=pltpu.SMEM), whole, whole, whole],
+        out_specs=[whole, whole],
+        scratch_shapes=[pltpu.VMEM((ROWS, WIDTH), NARROW)],
         compiler_params=pltpu.CompilerParams(vmem_limit_bytes=6 << 20),
         cost_estimate=pl.CostEstimate(
             flops=2 * ROWS * WIDTH * MODEL, bytes_accessed=4 << 20, transcendentals=0

time: 95.7 us -> 92.2 us (0.963)
  Pallas kernels: 9.46 us -> 6.67 us
    pallas_call x5, Pallas kernels: 7.22 us -> 4.42 us  [the longest x4 3.66 us: call_with(): pl.pallas_call(body, out_shape=shapes, scratch_shapes=scratch, compiler_p...]
where the time goes in v7:
time: 92.2 us; the launch traced here: 91.8 us
  blocking collectives  58.7 us (64%)
  starting transfers between devices  17.6 us (19%)
  Pallas kernels  6.67 us (7%)
  waiting for transfers between devices  5.05 us (5%)
  matrix products  2.01 us (2%)
    all_to_all x3, blocking collectives, exchange(): lax.all_to_all(pieces, axes, 0, 0, tiled=True, axis_index_groups=groups)  58.7 us
    all_to_all x1, starting transfers between devices, exchange(): lax.all_to_all(pieces, axes, 0, 0, tiled=True, axis_index_groups=groups)  9.25 us
    ppermute x2, starting transfers between devices, shifted(): lax.ppermute(value, axis, [(source, source + steps) for source in range(f...  6.45 us
    ppermute x2, waiting for transfers between devices, shifted(): lax.ppermute(value, axis, [(source, source + steps) for source in range(f...  5.04 us
    pallas_call x4, Pallas kernels, call_with(): pl.pallas_call(body, out_shape=shapes, scratch_shapes=scratch, compiler_p...  3.66 us
    pallas_call x4, Pallas kernels, call(): pl.pallas_call(body, out_shape=shapes, compiler_params=pltpu.CompilerPara...  2.24 us
    dot_general x1, matrix products, shards(): lax.dot_general(out_cotangent, out_weight, (((1,), (1,)), ((), ())), pref...  2.01 us
    ppermute x1, starting transfers between devices, shards(): other = lax.ppermute(other, 'c', [(0, 1), (1, 0)])  1.92 us
  transfers between devices with their start and end apart: 4, of which 1 were waited for; matrix products, arithmetic and copies ran while one was open for 2% of the time, Pallas kernels for 3%

profile of v7, /device:TPU:7, one launch (start us, length us, event | category | flops | bytes accessed | tf_op | source)
XLA Modules:
  0.0 91.8 jit_solution(10498629115756960098)
XLA Ops:
  0.6 0.0 copy-start
  0.6 0.0 copy-start.2
  0.7 0.0 copy-start.3
  0.7 0.0 copy-start.5
  0.7 0.0 copy-start.4
  0.7 0.0 copy-start.6
  0.7 0.0 copy-start.7
  0.7 0.9 multiply_convert_fusion
  1.6 0.0 copy-start.1
  1.6 4.2 %collective-permute-start = (bf16[32,256]{1,0:T(8,128)(2,1)S(1)}, bf16[32,256]{1,0:T(8,128)(2,1)S(1)}, u32[]{:S(2)}, u32[]{:S(2)}) collective-permute-start(bf16[32,256]{1,0:T(8,128)(2,1)S(1)} %multiply_convert_fusion), channel_id=1, source_target_pairs={{0,4},{4,8},{8,12},{12,16},{16,20},{20,24},{24,28},{28,32},{32,36}... | collective-permute-start | bytes 49160 | tf_op jit(solution)/shard_map/ppermute | solution.py:33
  5.7 0.0 copy-done
  5.7 2.0 %fusion.upstream = f32[384,256]{1,0:T(8,128)S(1)} fusion(bf16[384,2048]{1,0:T(8,128)(2,1)} %cotangent.1, bf16[256,2048]{1,0:T(8,128)(2,1)S(1)} %copy-done), kind=kOutput, calls=%fused_computation.1 | convolution fusion | flops 402653184 | bytes 3014656 | tf_op jit(solution)/shard_map/dot_general | solution.py:312
  7.8 0.0 copy-done.2
  7.8 0.0 copy-done.3
  7.8 0.0 copy-done.5
  7.8 0.0 copy-done.4
  7.8 0.0 copy-done.6
  7.8 0.0 copy-done.7
  7.8 1.3 %shard_map.119 = (bf16[384,256]{1,0:T(8,128)(2,1)S(1)}, f32[2,352,128]{2,1,0:T(8,128)S(1)}, f32[2,352,128]{2,1,0:T(8,128)S(1)}, bf16[352,256]{1,0:T(8,128)(2,1)S...) custom-call(bf16[384,256]{1,0:T(8,128)(2,1)S(1)} %copy-done.3, bf16[384,256]{1,0:T(8,128)(2,1)S(1)} %copy-done.2, ...), custom_call_target="tpu_custom_call" | custom-call | flops 9830400 | bytes 1916416 | tf_op jit(solution)/shard_map/pallas_call | solution.py:383
  9.1 0.0 collective-permute-done.halo
  9.1 0.2 shard_map.120
  9.3 0.0 copy-done.1
  9.3 0.8 weight_product.1
  10.1 1.9 %collective-permute-start.1 = (bf16[8,16,8,256]{3,2,1,0:T(8,128)(2,1)S(1)}, bf16[8,16,8,256]{3,2,1,0:T(8,128)(2,1)S(1)}, u32[]{:S(2)}, u32[]{:S(2)}) collective-permute-start(bf16[8,16,8,256]{3,2,1,0:T(8,128)(2,1)S(1)} %get-tuple-element.39), channel_id=1, source_target_pairs={{0,4},{4,0},{1,5},{5,1},{2,6},{6,2},{3,7},{7,3},{8,12},{12,8},{9,1... | collective-permute-start | bytes 1572872 | tf_op jit(solution)/shard_map/ppermute | solution.py:348
  12.0 8.2 %all_to_all.20.sums = f32[4,8,128]{2,1,0:T(8,128)S(1)} all-to-all(f32[4,8,128]{2,1,0:T(8,128)S(1)} %get-tuple-element.30), channel_id=1, replica_groups=mesh['zh'=16,'zl'=2,'x'=4,'c'=2,'tp'=4] {'tp'}, dimensions={0} | all-to-all | bytes 32768 | tf_op jit(solution)/shard_map/all_to_all | solution.py:38
  20.2 0.0 collective-permute-done.1.other
  20.2 1.3 %shard_map.121 = (bf16[8,136,256]{2,1,0:T(8,128)(2,1)S(1)}, f32[2,448,128]{2,1,0:T(8,128)S(1)}) custom-call(f32[4,8,128]{2,1,0:T(8,128)S(1)} %all_to_all.20.sums, f32[2,352,128]{2,1,0:T(8,128)S(1)} %get-tuple-element.31.scaled, f32[2,352,128]{2,1,0:T(8,128)S(1)} %get-tuple-element.32.spread, f32[2,32,128]{2,1,0:T(8,128)S(1)} %get-tuple-element.33.first_scaled, ...), custom_call_target="tpu_custom_call" | custom-call | flops 9830400 | bytes 3614208 | tf_op jit(solution)/shard_map/pallas_call | solution.py:383
  21.6 19.0 %all_to_all.21.arrived = bf16[8,136,256]{2,1,0:T(8,128)(2,1)S(1)} all-to-all(bf16[8,136,256]{2,1,0:T(8,128)(2,1)S(1)} %get-tuple-element.45), channel_id=1, replica_groups=mesh['zh'=16,'zl'=2,'x'=4,'c'=2,'tp'=4] {'zl','x'}, dimensions={0} | all-to-all | bytes 1114112 | tf_op jit(solution)/shard_map/all_to_all | solution.py:38
  40.6 0.1 shard_map.124
  40.7 31.5 %all_to_all.22.arrived.weights = bf16[16,8,384]{2,1,0:T(8,128)(2,1)S(1)} all-to-all(bf16[16,8,384]{2,1,0:T(8,128)(2,1)S(1)} %shard_map.124), channel_id=1, replica_groups={{640,704,768,832,896,960,0,64,128,192,256,320,384,448,512,576},{641,705..., dimensions={0} | all-to-all | bytes 196608 | tf_op jit(solution)/shard_map/all_to_all | solution.py:38
  72.2 0.6 shard_map.125
  72.8 9.3 %all-to-all-start.3 = ((f32[16,8,128]{2,1,0:T(8,128)}), f32[16,8,128]{2,1,0:T(8,128)S(1)}, u32[]{:S(2)}, u32[]{:S(2)}) async-start(f32[16,8,128]{2,1,0:T(8,128)} %shard_map.125), calls=%async_computation.3 | async-start | bytes 131072 | tf_op jit(solution)/shard_map/all_to_all | solution.py:38
  82.1 0.9 shard_map.122
  82.9 2.3 %collective-permute-start.2 = (f32[2,32,128]{2,1,0:T(8,128)S(1)}, f32[2,32,128]{2,1,0:T(8,128)S(1)}, u32[]{:S(2)}, u32[]{:S(2)}) collective-permute-start(f32[2,32,128]{2,1,0:T(8,128)S(1)} %get-tuple-element.42), channel_id=1, source_target_pairs={{4,0},{8,4},{12,8},{16,12},{20,16},{24,20},{28,24},{32,28},{36,32}... | collective-permute-start | bytes 98312 | tf_op jit(solution)/shard_map/ppermute | solution.py:33
  85.2 5.0 %collective-permute-done.2.arrived = f32[2,32,128]{2,1,0:T(8,128)S(1)} collective-permute-done((f32[2,32,128]{2,1,0:T(8,128)S(1)}, f32[2,32,128]{2,1,0:T(8,128)S(1)}, u32[]{:S(2)}, u32[]{:S(2)}) %collective-permute-start.2) | collective-permute-done | bytes 32800 | tf_op jit(solution)/shard_map/ppermute | solution.py:33
  90.3 0.9 shard_map.123
  91.2 0.0 all-to-all-done.3.arrived
  91.2 0.6 shard_map.126
Async XLA Ops:
  0.6 5.1 %copy-start = (bf16[256,2048]{1,0:T(8,128)(2,1)S(1)}, bf16[256,2048]{1,0:T(8,128)(2,1)}, u32[]{:S(2)}) copy-start(bf16[256,2048]{1,0:T(8,128)(2,1)} %param.11) | copy-start | bytes 3145732
  0.6 7.1 %copy-start.2 = (bf16[384,256]{1,0:T(8,128)(2,1)S(1)}, bf16[384,256]{1,0:T(8,128)(2,1)}, u32[]{:S(2)}) copy-start(bf16[384,256]{1,0:T(8,128)(2,1)} %gate.3) | copy-start | bytes 589828
  0.7 7.1 %copy-start.3 = (bf16[384,256]{1,0:T(8,128)(2,1)S(1)}, bf16[384,256]{1,0:T(8,128)(2,1)}, u32[]{:S(2)}) copy-start(bf16[384,256]{1,0:T(8,128)(2,1)} %value.3) | copy-start | bytes 589828
  0.7 7.1 %copy-start.5 = (f32[384]{0:T(512)S(1)}, f32[384]{0:T(512)}, u32[]{:S(2)}) copy-start(f32[384]{0:T(512)} %scale.5) | copy-start | bytes 4612
  0.7 7.1 %copy-start.4 = (bf16[31,256]{1,0:T(8,128)(2,1)S(1)}, bf16[31,256]{1,0:T(8,128)(2,1)}, u32[]{:S(2)}) copy-start(bf16[31,256]{1,0:T(8,128)(2,1)} %taps.5) | copy-start | bytes 47620
  0.7 7.1 %copy-start.6 = (f32[384]{0:T(512)S(1)}, f32[384]{0:T(512)}, u32[]{:S(2)}) copy-start(f32[384]{0:T(512)} %mean.3) | copy-start | bytes 4612
  0.7 7.1 %copy-start.7 = (f32[256]{0:T(256)S(1)}, f32[256]{0:T(256)}, u32[]{:S(2)}) copy-start(f32[256]{0:T(256)} %param.13) | copy-start | bytes 3076
  1.6 7.8 %copy-start.1 = (bf16[384,2048]{1,0:T(8,128)(2,1)S(1)}, bf16[384,2048]{1,0:T(8,128)(2,1)}, u32[]{:S(2)}) copy-start(bf16[384,2048]{1,0:T(8,128)(2,1)} %cotangent.1) | copy-start | bytes 4718596
  1.6 7.5 %collective-permute-start = (bf16[32,256]{1,0:T(8,128)(2,1)S(1)}, bf16[32,256]{1,0:T(8,128)(2,1)S(1)}, u32[]{:S(2)}, u32[]{:S(2)}) collective-permute-start(bf16[32,256]{1,0:T(8,128)(2,1)S(1)} %multiply_convert_fusion), channel_id=1, source_target_pairs={{0,4},{4,8},{8,12},{12,16},{16,20},{20,24},{24,28},{28,32},{32,36}... | collective-permute-start | bytes 49160 | tf_op jit(solution)/shard_map/ppermute | solution.py:33
  10.1 10.1 %collective-permute-start.1 = (bf16[8,16,8,256]{3,2,1,0:T(8,128)(2,1)S(1)}, bf16[8,16,8,256]{3,2,1,0:T(8,128)(2,1)S(1)}, u32[]{:S(2)}, u32[]{:S(2)}) collective-permute-start(bf16[8,16,8,256]{3,2,1,0:T(8,128)(2,1)S(1)} %get-tuple-element.39), channel_id=1, source_target_pairs={{0,4},{4,0},{1,5},{5,1},{2,6},{6,2},{3,7},{7,3},{8,12},{12,8},{9,1... | collective-permute-start | bytes 1572872 | tf_op jit(solution)/shard_map/ppermute | solution.py:348
  72.8 18.3 %all-to-all-start.3 = ((f32[16,8,128]{2,1,0:T(8,128)}), f32[16,8,128]{2,1,0:T(8,128)S(1)}, u32[]{:S(2)}, u32[]{:S(2)}) async-start(f32[16,8,128]{2,1,0:T(8,128)} %shard_map.125), calls=%async_computation.3 | async-start | bytes 131072 | tf_op jit(solution)/shard_map/all_to_all | solution.py:38
  82.9 7.3 %collective-permute-start.2 = (f32[2,32,128]{2,1,0:T(8,128)S(1)}, f32[2,32,128]{2,1,0:T(8,128)S(1)}, u32[]{:S(2)}, u32[]{:S(2)}) collective-permute-start(f32[2,32,128]{2,1,0:T(8,128)S(1)} %get-tuple-element.42), channel_id=1, source_target_pairs={{4,0},{8,4},{12,8},{16,12},{20,16},{24,20},{28,24},{32,28},{36,32}... | collective-permute-start | bytes 98312 | tf_op jit(solution)/shard_map/ppermute | solution.py:33

commit v8 on v7

--- a/solution.py
+++ b/solution.py
@@ -12,8 +12,9 @@
 FAR = 16
 CLOSE = 8
 AXES = (("zh", FAR), ("zl", 2), ("x", 4), ("c", 2))
-FAR_ORDER = [(place + 10) % FAR for place in range(FAR)]
 TP = 4
+BLOCK = CLOSE * 8
+GATHER_ORDER = [(place + 1) % (2 * CLOSE) for place in range(2 * CLOSE)]
 TAPS = 31
 ROWS = 384
 EDGE = 32
@@ -161,28 +162,24 @@
         message[peer] = total
 
 
-def weight_product(core, cotangent, hidden, first_hidden, mine, other, whole):
+def weight_product(place, cotangent, hidden, first_hidden, mine, other, whole):
     whole[0:EDGE] = first_hidden[...]
     whole[EDGE:] = hidden[...]
-    first = core[0] == 0
+    first = place[0] % 2 == 0
     for far in range(FAR):
         part = lax.dot_general(
             cotangent[:, lanes(far)], whole[...], (((0,), (0,)), ((), ())),
             preferred_element_type=WIDE,
         )
         part = part.reshape(CLOSE, 2, OWN, WIDTH)
-        low, high = part[:, 0], part[:, 1]
-        mine[:, far] = jnp.where(first, low, high)
-        other[:, far] = jnp.where(first, high, low).astype(NARROW)
-
-
-def halves(value):
-    high = value.astype(NARROW)
-    return high, (value - high.astype(WIDE)).astype(NARROW)
+        low = part[:, 0].reshape(CLOSE * OWN, WIDTH)
+        high = part[:, 1].reshape(CLOSE * OWN, WIDTH)
+        mine[far] = jnp.where(first, low, high)
+        other[far] = jnp.where(first, high, low).astype(NARROW)
 
 
 def backward(
-    sums, scaled, spread, first_scaled, first_spread, halo, gated, scale, gain_part, mine, other,
+    place, sums, scaled, spread, first_scaled, first_spread, halo, gated, scale, gain_part, mine, other,
     pieces, extended,
     small, padded,
 ):
@@ -229,11 +226,12 @@
                 small[tap : tap + 1, lanes(half)] = jnp.sum(found[half, q], 0, keepdims=True)
     for half in range(HALVES):
         small[TAPS : TAPS + 1, lanes(half)] = jnp.sum(gain_part[half], 0, keepdims=True)
+    taps_rows = small[...].astype(NARROW)
     for near in range(CLOSE):
-        chip = mine[near] + other[near].astype(WIDE)
-        pieces[near, 0 : FAR * OWN] = chip.reshape(FAR * OWN, WIDTH).astype(NARROW)
-        high, low = halves(small[near * 4 : near * 4 + 4])
-        pieces[near, FAR * OWN :] = jnp.concatenate([high.astype(WIDE), low.astype(WIDE)], 0).astype(NARROW)
+        for turn, rows in ((0, slice(0, BLOCK)), (CLOSE, slice(BLOCK, 2 * BLOCK))):
+            far = lax.rem(place[0] // (2 * CLOSE) + near + turn, FAR)
+            pieces[near, rows] = (mine[far] + other[far].astype(WIDE)).astype(NARROW)
+        pieces[near, 2 * BLOCK :] = taps_rows
 
 
 def gated_gradient(extended, taps, d_gated, margin, taps_wide):
@@ -250,56 +248,75 @@
                 d_gated[half, start - EDGE : start] = found
 
 
-def outputs(d_gated, arrived, value, gate, value_grad, gate_grad):
+def fold_near(arrived, to_first, to_second):
+    for start in range(0, 2 * BLOCK + 32, 32):
+        rows = slice(start, start + 32)
+        total = arrived[0, rows].astype(WIDE)
+        for near in range(1, CLOSE):
+            total = total + arrived[near, rows].astype(WIDE)
+        total = total.astype(NARROW)
+        if start < BLOCK:
+            to_first[rows] = total
+        elif start < 2 * BLOCK:
+            to_second[start - BLOCK : start - BLOCK + 32] = total
+        else:
+            to_first[BLOCK:] = total
+            to_second[BLOCK:] = total
+
+
+def fold_far(place, kept, first, second, message):
+    own = place[0] // 2 % CLOSE == 0
+    for start in range(BLOCK, -1, -8):
+        size = 32 if start == BLOCK else 8
+        rows = slice(start, start + size)
+        here = jnp.where(own, kept[rows].astype(WIDE), first[rows].astype(WIDE))
+        total = (here + second[rows].astype(WIDE)).astype(NARROW)
+        if start == BLOCK:
+            for position in range(2 * CLOSE):
+                message[position, OWN:] = total
+        else:
+            for position in range(2 * CLOSE):
+                if GATHER_ORDER[position] // 2 == start // 8:
+                    message[position, 0:OWN] = total
+
+
+def finish(
+    place, arrived, d_gated, late, value, gate,
+    value_grad, gate_grad, weight_grad, taps_grad, gain_grad,
+):
     for half in range(HALVES):
         for start in range(0, ROWS, EDGE):
             rows = slice(start, start + EDGE)
             grad = d_gated[half, rows]
             if start == ROWS - EDGE:
-                grad = grad + arrived[half]
+                grad = grad + late[half]
             sig = jax.nn.sigmoid(gate[rows, lanes(half)].astype(WIDE))
             wide = value[rows, lanes(half)].astype(WIDE)
             value_grad[rows, lanes(half)] = (grad * sig).astype(NARROW)
             gate_grad[rows, lanes(half)] = (grad * wide * sig * (1.0 - sig)).astype(NARROW)
-
-
-def fold_near(arrived, pieces):
+    by_core = []
+    for side in range(2):
+        positions = [p for p in range(2 * CLOSE) if GATHER_ORDER[p] % 2 == side]
+        total = arrived[positions[0], 0:OWN].astype(WIDE)
+        for position in positions[1:]:
+            total = total + arrived[position, 0:OWN].astype(WIDE)
+        by_core.append(total)
+    weight_grad[...] = jnp.where(place[0] % 2 == 0, by_core[0], by_core[1])
+    total = arrived[0, OWN:].astype(WIDE)
+    for position in range(1, 2 * CLOSE):
+        total = total + arrived[position, OWN:].astype(WIDE)
+    taps_grad[...] = total[0:TAPS]
+    gain_grad[...] = total[TAPS : TAPS + 1]
+
+
+def to_block(value, turn):
+    pairs = []
     for far in range(FAR):
-        rows = slice(far * OWN, (far + 1) * OWN)
-        total = arrived[0, rows].astype(WIDE)
-        for near in range(1, CLOSE):
-            total = total + arrived[near, rows].astype(WIDE)
-        pieces[FAR_ORDER.index(far), :, 0:WIDTH] = total.astype(NARROW)
-    both = arrived[0, FAR * OWN :].astype(WIDE)
-    for near in range(1, CLOSE):
-        both = both + arrived[near, FAR * OWN :].astype(WIDE)
-    small = both[0:4] + both[4:8]
-    small = jnp.concatenate([small[:, lanes(0)], small[:, lanes(1)]], 0).astype(NARROW)
-    for far in range(FAR):
-        pieces[far, :, WIDTH:] = small
-
-
-def fold_far(arrived, message):
-    total = arrived[0, :, WIDTH:].astype(WIDE)
-    for far in range(1, FAR):
-        total = total + arrived[far, :, WIDTH:].astype(WIDE)
-    for peer in range(CLOSE * 2):
-        message[peer] = total
-
-
-def finish(arrived, weights, taps_grad, gain_grad, weight_grad):
-    total = weights[0, :, 0:WIDTH].astype(WIDE)
-    for far in range(1, FAR):
-        total = total + weights[far, :, 0:WIDTH].astype(WIDE)
-    weight_grad[...] = total
-    for near in range(CLOSE):
-        total = arrived[2 * near] + arrived[2 * near + 1]
-        total = jnp.concatenate([total[0:4], total[4:8]], 1)
-        if near < CLOSE - 1:
-            taps_grad[near * 4 : near * 4 + 4] = total
-        else:
-            taps_grad[near * 4 : near * 4 + 3] = total[0:3]
-            gain_grad[...] = total[3:4]
+        for near in range(CLOSE):
+            step = (near + turn) % FAR
+            if step:
+                pairs.append((far * CLOSE + near, (far + step) % FAR * CLOSE + near))
+    return lax.ppermute(value, ("zh", *NEAR), pairs)
 
 
 def shards(
@@ -342,37 +359,41 @@
         flops=10 * ROWS * WIDTH,
     )
     sums = exchange(message, "tp")
-    core = lax.axis_index("c").reshape(1)
-    grouped = (CLOSE, FAR, OWN, WIDTH)
-    mine, other = weight_call(core, out_cotangent, hidden, first_hidden, [(grouped, WIDE), (grouped, NARROW)])
+    place = lax.axis_index(SP).reshape(1)
+    grouped = (FAR, CLOSE * OWN, WIDTH)
+    mine, other = scalar_call(
+        weight_product, [(grouped, WIDE), (grouped, NARROW)],
+        place, out_cotangent, hidden, first_hidden,
+        scratch=[pltpu.VMEM((ROWS, WIDTH), NARROW)], flops=2 * ROWS * WIDTH * MODEL,
+    )
     other = lax.ppermute(other, "c", [(0, 1), (1, 0)])
-    pieces, extended = call_with(
+    pieces, extended = scalar_call(
         backward,
-        [((CLOSE, FAR * OWN + 8, WIDTH), NARROW), ((HALVES, ROWS + 2 * EDGE, LANES), WIDE)],
-        [taps_scratch, sides],
-        sums, scaled, spread, first_scaled, first_spread, halo, gated, row_scale, gain_part,
-        mine, other,
+        [((CLOSE, 2 * BLOCK + TAPS + 1, WIDTH), NARROW), ((HALVES, ROWS + 2 * EDGE, LANES), WIDE)],
+        place, sums, scaled, spread, first_scaled, first_spread, halo, gated, row_scale,
+        gain_part, mine, other, scratch=[taps_scratch, sides],
         flops=100 * ROWS * WIDTH,
     )
-    (pieces,) = call(
-        fold_near, [((FAR, OWN, WIDTH + LANES), NARROW)], exchange(pieces, NEAR), flops=1 << 20
-    )
-    arrived = exchange(pieces, "zh", FAR_ORDER)
+    arrived = exchange(pieces, NEAR)
+    payload = ((BLOCK + TAPS + 1, WIDTH), NARROW)
+    to_first, to_second = call(fold_near, [payload, payload], arrived, flops=1 << 20)
+    first = to_block(to_first, 0)
+    second = to_block(to_second, CLOSE)
     d_gated, margin = call_with(
         gated_gradient, [(split, WIDE), ((HALVES, EDGE, LANES), WIDE)], [taps_scratch],
         extended, conv_taps, flops=100 * ROWS * WIDTH,
     )
     late = shifted(margin, SP, -1)
-    value_grad, gate_grad = call(
-        outputs, [((ROWS, WIDTH), NARROW), ((ROWS, WIDTH), NARROW)],
-        d_gated, late, proj_value, proj_gate, flops=10 * ROWS * WIDTH,
-    )
-    (message,) = call(
-        fold_far, [((CLOSE * 2, 8, LANES), WIDE)], arrived, flops=1 << 16
-    )
-    taps_grad, gain_grad, weight_grad = call(
-        finish, [((TAPS, WIDTH), WIDE), ((1, WIDTH), WIDE), ((OWN, WIDTH), WIDE)],
-        exchange(message, (*NEAR, "c")), arrived, flops=1 << 16,
+    (message,) = scalar_call(
+        fold_far, [((2 * CLOSE, OWN + TAPS + 1, WIDTH), NARROW)],
+        place, to_first, first, second,
+    )
+    arrived = exchange(message, (*NEAR, "c"), GATHER_ORDER)
+    narrow = ((ROWS, WIDTH), NARROW)
+    value_grad, gate_grad, weight_grad, taps_grad, gain_grad = scalar_call(
+        finish,
+        [narrow, narrow, ((OWN, WIDTH), WIDE), ((TAPS, WIDTH), WIDE), ((1, WIDTH), WIDE)],
+        place, arrived, d_gated, late, proj_value, proj_gate,
     )
     return (value_grad, gate_grad, weight_grad, taps_grad, gain_grad.reshape(WIDTH))
 
@@ -389,20 +410,19 @@
     )(*args)
 
 
-def weight_call(core, cotangent, hidden, first_hidden, outs):
+def scalar_call(body, outs, scalar, *args, scratch=(), flops=1 << 20, limit=6):
+    shapes = [jax.ShapeDtypeStruct(shape, dtype) for shape, dtype in outs]
+    size = sum(a.size * a.dtype.itemsize for a in (*args, *shapes))
     whole = pl.BlockSpec(memory_space=pltpu.VMEM)
     return pl.pallas_call(
-        weight_product,
-        out_shape=[jax.ShapeDtypeStruct(shape, dtype) for shape, dtype in outs],
-        in_specs=[pl.BlockSpec(memory_space=pltpu.SMEM), whole, whole, whole],
-        out_specs=[whole, whole],
-        scratch_shapes=[pltpu.VMEM((ROWS, WIDTH), NARROW)],
-        compiler_params=pltpu.CompilerParams(vmem_limit_bytes=6 << 20),
-        cost_estimate=pl.CostEstimate(
-            flops=2 * ROWS * WIDTH * MODEL, bytes_accessed=4 << 20, transcendentals=0
-        ),
-        name="weight_product",
-    )(core, cotangent, hidden, first_hidden)
+        body,
+        out_shape=shapes,
+        in_specs=[pl.BlockSpec(memory_space=pltpu.SMEM), *([whole] * len(args))],
+        out_specs=[whole] * len(shapes),
+        scratch_shapes=scratch,
+        compiler_params=pltpu.CompilerParams(vmem_limit_bytes=limit << 20),
+        cost_estimate=pl.CostEstimate(flops=flops, bytes_accessed=size, transcendentals=0),
+    )(scalar, *args)
 
 
 def solution(mesh):

time: 92.2 us -> 94.1 us (1.021)
  blocking collectives: 58.7 us -> 27.8 us
  starting transfers between devices: 17.6 us -> 42.8 us
  waiting for transfers between devices: 5.05 us -> 13 us
    all_to_all x3 -> x2, blocking collectives: 58.7 us -> 27.8 us  [exchange(): lax.all_to_all(pieces, axes, 0, 0, tiled=True, axis_index_groups=groups)]
    ppermute x0 -> x2, starting transfers between devices: none -> 20.5 us  [to_block(): return lax.ppermute(value, ('zh', *NEAR), pairs)]
    ppermute x0 -> x2, waiting for transfers between devices: none -> 7.97 us  [to_block(): return lax.ppermute(value, ('zh', *NEAR), pairs)]
    all_to_all x1, starting transfers between devices: 9.25 us -> 13.9 us  [exchange(): lax.all_to_all(pieces, axes, 0, 0, tiled=True, axis_index_groups=groups)]
    pallas_call x1 -> x4, Pallas kernels: 0.76 us -> 3.65 us  [scalar_call(): pl.pallas_call(body, out_shape=shapes, in_specs=[pl.BlockSpec(memory_spac...]
    pallas_call x4 -> x1, Pallas kernels: 2.24 us -> 0.09 us  [call(): pl.pallas_call(body, out_shape=shapes, compiler_params=pltpu.CompilerPara...]
    pallas_call x4 -> x3, Pallas kernels: 3.66 us -> 2.33 us  [call_with(): pl.pallas_call(body, out_shape=shapes, scratch_shapes=scratch, compiler_p...]
  transfers between devices with their start and end apart: 4 -> 6, of which waited for: 1 -> 2; matrix products, arithmetic and copies ran while one was open for 2% -> 2% of each run, Pallas kernels for 3% -> 2%
where the time goes in v8:
time: 94.1 us; the launch traced here: 93.5 us
  starting transfers between devices  42.8 us (45%)
  blocking collectives  27.8 us (30%)
  waiting for transfers between devices  13 us (14%)
  Pallas kernels  6.07 us (6%)
  matrix products  2.01 us (2%)
    all_to_all x2, blocking collectives, exchange(): lax.all_to_all(pieces, axes, 0, 0, tiled=True, axis_index_groups=groups)  27.8 us
    ppermute x2, starting transfers between devices, to_block(): return lax.ppermute(value, ('zh', *NEAR), pairs)  20.5 us
    all_to_all x1, starting transfers between devices, exchange(): lax.all_to_all(pieces, axes, 0, 0, tiled=True, axis_index_groups=groups)  13.9 us
    ppermute x2, waiting for transfers between devices, to_block(): return lax.ppermute(value, ('zh', *NEAR), pairs)  7.97 us
    ppermute x2, starting transfers between devices, shifted(): lax.ppermute(value, axis, [(source, source + steps) for source in range(f...  6.46 us
    ppermute x2, waiting for transfers between devices, shifted(): lax.ppermute(value, axis, [(source, source + steps) for source in range(f...  5.04 us
    pallas_call x4, Pallas kernels, scalar_call(): pl.pallas_call(body, out_shape=shapes, in_specs=[pl.BlockSpec(memory_spac...  3.65 us
    pallas_call x3, Pallas kernels, call_with(): pl.pallas_call(body, out_shape=shapes, scratch_shapes=scratch, compiler_p...  2.33 us
  transfers between devices with their start and end apart: 6, of which 2 were waited for; matrix products, arithmetic and copies ran while one was open for 2% of the time, Pallas kernels for 2%

profile of v8, /device:TPU:7, one launch (start us, length us, event | category | flops | bytes accessed | tf_op | source)
XLA Modules:
  0.0 93.5 jit_solution(18157657949404703406)
XLA Ops:
  0.6 0.0 copy-start
  0.6 0.0 copy-start.2
  0.7 0.0 copy-start.3
  0.7 0.0 copy-start.5
  0.7 0.0 copy-start.4
  0.7 0.0 copy-start.6
  0.7 0.0 copy-start.7
  0.7 0.9 multiply_convert_fusion
  1.6 0.0 copy-start.1
  1.6 4.2 %collective-permute-start = (bf16[32,256]{1,0:T(8,128)(2,1)S(1)}, bf16[32,256]{1,0:T(8,128)(2,1)S(1)}, u32[]{:S(2)}, u32[]{:S(2)}) collective-permute-start(bf16[32,256]{1,0:T(8,128)(2,1)S(1)} %multiply_convert_fusion), channel_id=1, source_target_pairs={{0,4},{4,8},{8,12},{12,16},{16,20},{20,24},{24,28},{28,32},{32,36}... | collective-permute-start | bytes 49160 | tf_op jit(solution)/shard_map/ppermute | solution.py:34
  5.7 0.0 copy-done
  5.7 2.0 %fusion.upstream = f32[384,256]{1,0:T(8,128)S(1)} fusion(bf16[384,2048]{1,0:T(8,128)(2,1)} %cotangent.1, bf16[256,2048]{1,0:T(8,128)(2,1)S(1)} %copy-done), kind=kOutput, calls=%fused_computation.1 | convolution fusion | flops 402653184 | bytes 3014656 | tf_op jit(solution)/shard_map/dot_general | solution.py:329
  7.8 0.0 copy-done.2
  7.8 0.0 copy-done.3
  7.8 0.0 copy-done.5
  7.8 0.0 copy-done.4
  7.8 0.0 copy-done.6
  7.8 0.0 copy-done.7
  7.8 1.3 %shard_map.119 = (bf16[384,256]{1,0:T(8,128)(2,1)S(1)}, f32[2,352,128]{2,1,0:T(8,128)S(1)}, f32[2,352,128]{2,1,0:T(8,128)S(1)}, bf16[352,256]{1,0:T(8,128)(2,1)S...) custom-call(bf16[384,256]{1,0:T(8,128)(2,1)S(1)} %copy-done.3, bf16[384,256]{1,0:T(8,128)(2,1)S(1)} %copy-done.2, ...), custom_call_target="tpu_custom_call" | custom-call | flops 9830400 | bytes 1916416 | tf_op jit(solution)/shard_map/pallas_call | solution.py:404
  9.1 0.0 collective-permute-done.halo
  9.1 0.2 shard_map.120
  9.3 0.0 copy-done.1
  9.3 0.8 shard_map.121
  10.1 1.9 %collective-permute-start.1 = (bf16[16,64,256]{2,1,0:T(8,128)(2,1)S(1)}, bf16[16,64,256]{2,1,0:T(8,128)(2,1)S(1)}, u32[]{:S(2)}, u32[]{:S(2)}) collective-permute-start(bf16[16,64,256]{2,1,0:T(8,128)(2,1)S(1)} %get-tuple-element.41), channel_id=1, source_target_pairs={{0,4},{4,0},{1,5},{5,1},{2,6},{6,2},{3,7},{7,3},{8,12},{12,8},{9,1... | collective-permute-start | bytes 1572872 | tf_op jit(solution)/shard_map/ppermute | solution.py:369
  12.0 8.2 %all_to_all.15.sums = f32[4,8,128]{2,1,0:T(8,128)S(1)} all-to-all(f32[4,8,128]{2,1,0:T(8,128)S(1)} %get-tuple-element.32), channel_id=1, replica_groups=mesh['zh'=16,'zl'=2,'x'=4,'c'=2,'tp'=4] {'tp'}, dimensions={0} | all-to-all | bytes 32768 | tf_op jit(solution)/shard_map/all_to_all | solution.py:39
  20.2 0.0 collective-permute-done.1.other
  20.2 1.3 %shard_map.122 = (bf16[8,160,256]{2,1,0:T(8,128)(2,1)S(1)}, f32[2,448,128]{2,1,0:T(8,128)S(1)}) custom-call(s32[1]{0:T(128)} %bitcast.place, f32[4,8,128]{2,1,0:T(8,128)S(1)} %all_to_all.15.sums, f32[2,352,128]{2,1,0:T(8,128)S(1)} %get-tuple-element.33.scaled, f32[2,352,128]{2,1,0:T(8,128)S(1)} %get-tuple-element.34.spread, ...), custom_call_target="tpu_custom_call" | custom-call | flops 9830400 | bytes 3712512 | tf_op jit(solution)/shard_map/pallas_call | solution.py:417
  21.5 19.6 %all_to_all.16.arrived = bf16[8,160,256]{2,1,0:T(8,128)(2,1)S(1)} all-to-all(bf16[8,160,256]{2,1,0:T(8,128)(2,1)S(1)} %get-tuple-element.42), channel_id=1, replica_groups=mesh['zh'=16,'zl'=2,'x'=4,'c'=2,'tp'=4] {'zl','x'}, dimensions={0} | all-to-all | bytes 1310720 | tf_op jit(solution)/shard_map/all_to_all | solution.py:39
  41.1 0.1 shard_map.123
  41.2 16.2 %collective-permute-start.3 = (bf16[96,256]{1,0:T(8,128)(2,1)S(1)}, bf16[96,256]{1,0:T(8,128)(2,1)S(1)}, u32[]{:S(2)}, u32[]{:S(2)}) collective-permute-start(bf16[96,256]{1,0:T(8,128)(2,1)S(1)} %get-tuple-element.44), channel_id=1, source_target_pairs={{0,512},{8,584},{16,656},{24,728},{32,800},{40,872},{48,944},{56,1... | collective-permute-start | bytes 147464 | tf_op jit(solution)/shard_map/ppermute | solution.py:319
  57.4 4.3 %collective-permute-start.2 = (bf16[96,256]{1,0:T(8,128)(2,1)S(1)}, bf16[96,256]{1,0:T(8,128)(2,1)S(1)}, u32[]{:S(2)}, u32[]{:S(2)}) collective-permute-start(bf16[96,256]{1,0:T(8,128)(2,1)S(1)} %get-tuple-element.43.kept), channel_id=1, source_target_pairs={{8,72},{16,144},{24,216},{32,288},{40,360},{48,432},{56,504},{72,1... | collective-permute-start | bytes 147464 | tf_op jit(solution)/shard_map/ppermute | solution.py:319
  61.7 0.0 collective-permute-done.3.second
  61.7 8.0 %collective-permute-done.2.first = bf16[96,256]{1,0:T(8,128)(2,1)S(1)} collective-permute-done((bf16[96,256]{1,0:T(8,128)(2,1)S(1)}, bf16[96,256]{1,0:T(8,128)(2,1)S(1)}, u32[]{:S(2)}, u32[]{:S(2)}) %collective-permute-start.2) | collective-permute-done | bytes 49184 | tf_op jit(solution)/shard_map/ppermute | solution.py:319
  69.7 0.8 shard_map.124
  70.5 13.9 %all-to-all-start.2 = ((bf16[16,40,256]{2,1,0:T(8,128)(2,1)}), bf16[16,40,256]{2,1,0:T(8,128)(2,1)S(1)}, u32[]{:S(2)}, u32[]{:S(2)}) async-start(bf16[16,40,256]{2,1,0:T(8,128)(2,1)} %shard_map.124), calls=%async_computation.2 | async-start | bytes 655360 | tf_op jit(solution)/shard_map/all_to_all | solution.py:39
  84.4 0.9 shard_map.125
  85.2 2.3 %collective-permute-start.4 = (f32[2,32,128]{2,1,0:T(8,128)S(1)}, f32[2,32,128]{2,1,0:T(8,128)S(1)}, u32[]{:S(2)}, u32[]{:S(2)}) collective-permute-start(f32[2,32,128]{2,1,0:T(8,128)S(1)} %get-tuple-element.47), channel_id=1, source_target_pairs={{4,0},{8,4},{12,8},{16,12},{20,16},{24,20},{28,24},{32,28},{36,32}... | collective-permute-start | bytes 98312 | tf_op jit(solution)/shard_map/ppermute | solution.py:34
  87.6 5.0 %collective-permute-done.4.late = f32[2,32,128]{2,1,0:T(8,128)S(1)} collective-permute-done((f32[2,32,128]{2,1,0:T(8,128)S(1)}, f32[2,32,128]{2,1,0:T(8,128)S(1)}, u32[]{:S(2)}, u32[]{:S(2)}) %collective-permute-start.4) | collective-permute-done | bytes 32800 | tf_op jit(solution)/shard_map/ppermute | solution.py:34
  92.6 0.0 all-to-all-done.2.arrived
  92.6 0.9 shard_map.126
Async XLA Ops:
  0.6 5.1 %copy-start = (bf16[256,2048]{1,0:T(8,128)(2,1)S(1)}, bf16[256,2048]{1,0:T(8,128)(2,1)}, u32[]{:S(2)}) copy-start(bf16[256,2048]{1,0:T(8,128)(2,1)} %param.11) | copy-start | bytes 3145732
  0.6 7.1 %copy-start.2 = (bf16[384,256]{1,0:T(8,128)(2,1)S(1)}, bf16[384,256]{1,0:T(8,128)(2,1)}, u32[]{:S(2)}) copy-start(bf16[384,256]{1,0:T(8,128)(2,1)} %gate.3) | copy-start | bytes 589828
  0.7 7.1 %copy-start.3 = (bf16[384,256]{1,0:T(8,128)(2,1)S(1)}, bf16[384,256]{1,0:T(8,128)(2,1)}, u32[]{:S(2)}) copy-start(bf16[384,256]{1,0:T(8,128)(2,1)} %value.3) | copy-start | bytes 589828
  0.7 7.1 %copy-start.5 = (f32[384]{0:T(512)S(1)}, f32[384]{0:T(512)}, u32[]{:S(2)}) copy-start(f32[384]{0:T(512)} %scale.5) | copy-start | bytes 4612
  0.7 7.1 %copy-start.4 = (bf16[31,256]{1,0:T(8,128)(2,1)S(1)}, bf16[31,256]{1,0:T(8,128)(2,1)}, u32[]{:S(2)}) copy-start(bf16[31,256]{1,0:T(8,128)(2,1)} %taps.5) | copy-start | bytes 47620
  0.7 7.1 %copy-start.6 = (f32[384]{0:T(512)S(1)}, f32[384]{0:T(512)}, u32[]{:S(2)}) copy-start(f32[384]{0:T(512)} %mean.3) | copy-start | bytes 4612
  0.7 7.1 %copy-start.7 = (f32[256]{0:T(256)S(1)}, f32[256]{0:T(256)}, u32[]{:S(2)}) copy-start(f32[256]{0:T(256)} %param.13) | copy-start | bytes 3076
  1.6 7.8 %copy-start.1 = (bf16[384,2048]{1,0:T(8,128)(2,1)S(1)}, bf16[384,2048]{1,0:T(8,128)(2,1)}, u32[]{:S(2)}) copy-start(bf16[384,2048]{1,0:T(8,128)(2,1)} %cotangent.1) | copy-start | bytes 4718596
  1.6 7.5 %collective-permute-start = (bf16[32,256]{1,0:T(8,128)(2,1)S(1)}, bf16[32,256]{1,0:T(8,128)(2,1)S(1)}, u32[]{:S(2)}, u32[]{:S(2)}) collective-permute-start(bf16[32,256]{1,0:T(8,128)(2,1)S(1)} %multiply_convert_fusion), channel_id=1, source_target_pairs={{0,4},{4,8},{8,12},{12,16},{16,20},{20,24},{24,28},{28,32},{32,36}... | collective-permute-start | bytes 49160 | tf_op jit(solution)/shard_map/ppermute | solution.py:34
  10.1 10.1 %collective-permute-start.1 = (bf16[16,64,256]{2,1,0:T(8,128)(2,1)S(1)}, bf16[16,64,256]{2,1,0:T(8,128)(2,1)S(1)}, u32[]{:S(2)}, u32[]{:S(2)}) collective-permute-start(bf16[16,64,256]{2,1,0:T(8,128)(2,1)S(1)} %get-tuple-element.41), channel_id=1, source_target_pairs={{0,4},{4,0},{1,5},{5,1},{2,6},{6,2},{3,7},{7,3},{8,12},{12,8},{9,1... | collective-permute-start | bytes 1572872 | tf_op jit(solution)/shard_map/ppermute | solution.py:369
  41.2 20.5 %collective-permute-start.3 = (bf16[96,256]{1,0:T(8,128)(2,1)S(1)}, bf16[96,256]{1,0:T(8,128)(2,1)S(1)}, u32[]{:S(2)}, u32[]{:S(2)}) collective-permute-start(bf16[96,256]{1,0:T(8,128)(2,1)S(1)} %get-tuple-element.44), channel_id=1, source_target_pairs={{0,512},{8,584},{16,656},{24,728},{32,800},{40,872},{48,944},{56,1... | collective-permute-start | bytes 147464 | tf_op jit(solution)/shard_map/ppermute | solution.py:319
  57.4 12.3 %collective-permute-start.2 = (bf16[96,256]{1,0:T(8,128)(2,1)S(1)}, bf16[96,256]{1,0:T(8,128)(2,1)S(1)}, u32[]{:S(2)}, u32[]{:S(2)}) collective-permute-start(bf16[96,256]{1,0:T(8,128)(2,1)S(1)} %get-tuple-element.43.kept), channel_id=1, source_target_pairs={{8,72},{16,144},{24,216},{32,288},{40,360},{48,432},{56,504},{72,1... | collective-permute-start | bytes 147464 | tf_op jit(solution)/shard_map/ppermute | solution.py:319
  70.5 22.1 %all-to-all-start.2 = ((bf16[16,40,256]{2,1,0:T(8,128)(2,1)}), bf16[16,40,256]{2,1,0:T(8,128)(2,1)S(1)}, u32[]{:S(2)}, u32[]{:S(2)}) async-start(bf16[16,40,256]{2,1,0:T(8,128)(2,1)} %shard_map.124), calls=%async_computation.2 | async-start | bytes 655360 | tf_op jit(solution)/shard_map/all_to_all | solution.py:39
  85.2 7.3 %collective-permute-start.4 = (f32[2,32,128]{2,1,0:T(8,128)S(1)}, f32[2,32,128]{2,1,0:T(8,128)S(1)}, u32[]{:S(2)}, u32[]{:S(2)}) collective-permute-start(f32[2,32,128]{2,1,0:T(8,128)S(1)} %get-tuple-element.47), channel_id=1, source_target_pairs={{4,0},{8,4},{12,8},{16,12},{20,16},{24,20},{28,24},{32,28},{36,32}... | collective-permute-start | bytes 98312 | tf_op jit(solution)/shard_map/ppermute | solution.py:34

commit v9 on v8

--- a/solution.py
+++ b/solution.py
@@ -13,9 +13,11 @@
 CLOSE = 8
 AXES = (("zh", FAR), ("zl", 2), ("x", 4), ("c", 2))
 TP = 4
-BLOCK = CLOSE * 8
+OFFSETS = ((0, -1, -2, -3, 1, 2, 3, -4), (8, 7, 6, 5, -7, -6, -5, 4))
+BLOCK = CLOSE * 2 * 8
 GATHER_ORDER = [(place + 1) % (2 * CLOSE) for place in range(2 * CLOSE)]
 TAPS = 31
+SMALL = TAPS + 1
 ROWS = 384
 EDGE = 32
 LANES = 128
@@ -129,7 +131,7 @@
 
 
 def head(
-    halo, gated, upstream, taps, gain, mean, scale, sums, gain_part,
+    _, halo, gated, upstream, taps, gain, mean, scale, sums, gain_part,
     scaled, spread, hidden, message, gain_total,
     padded, taps_wide, turned,
 ):
@@ -162,27 +164,22 @@
         message[peer] = total
 
 
-def weight_product(place, cotangent, hidden, first_hidden, mine, other, whole):
+def block_rows(cotangent, hidden, far):
+    columns = pl.ds(pl.multiple_of(far * BLOCK, BLOCK), BLOCK)
+    return lax.dot_general(
+        cotangent[:, columns], hidden[...], (((0,), (0,)), ((), ())), preferred_element_type=WIDE
+    )
+
+
+def backward(
+    place, sums, scaled, spread, first_scaled, first_spread, halo, gated, scale, gain_part,
+    cotangent, hidden, first_hidden,
+    mine, other, small, extended,
+    padded, whole,
+):
+    far, core = place[0] // (2 * CLOSE), place[0] % 2
     whole[0:EDGE] = first_hidden[...]
     whole[EDGE:] = hidden[...]
-    first = place[0] % 2 == 0
-    for far in range(FAR):
-        part = lax.dot_general(
-            cotangent[:, lanes(far)], whole[...], (((0,), (0,)), ((), ())),
-            preferred_element_type=WIDE,
-        )
-        part = part.reshape(CLOSE, 2, OWN, WIDTH)
-        low = part[:, 0].reshape(CLOSE * OWN, WIDTH)
-        high = part[:, 1].reshape(CLOSE * OWN, WIDTH)
-        mine[far] = jnp.where(first, low, high)
-        other[far] = jnp.where(first, high, low).astype(NARROW)
-
-
-def backward(
-    place, sums, scaled, spread, first_scaled, first_spread, halo, gated, scale, gain_part, mine, other,
-    pieces, extended,
-    small, padded,
-):
     for half in range(HALVES):
         padded[half, 0:EDGE] = halo[:, lanes(half)].astype(WIDE)
         padded[half, EDGE:] = gated[:, lanes(half)].astype(WIDE)
@@ -224,14 +221,31 @@
             for q in steps:
                 tap = 8 * q + offset - lead
                 small[tap : tap + 1, lanes(half)] = jnp.sum(found[half, q], 0, keepdims=True)
-    for half in range(HALVES):
-        small[TAPS : TAPS + 1, lanes(half)] = jnp.sum(gain_part[half], 0, keepdims=True)
-    taps_rows = small[...].astype(NARROW)
+        near = offset
+        low, high = OFFSETS[0][near], OFFSETS[1][near]
+        own = lax.rem(far + jnp.where(core == 0, low, high) + FAR, FAR)
+        theirs = lax.rem(far + jnp.where(core == 0, high, low) + FAR, FAR)
+        mine[near] = block_rows(cotangent, whole, own)
+        other[near * BLOCK : (near + 1) * BLOCK] = block_rows(cotangent, whole, theirs).astype(NARROW)
+    for half in range(HALVES):
+        small[TAPS:SMALL, lanes(half)] = jnp.sum(gain_part[half], 0, keepdims=True)
+    value = small[...]
+    top = value.astype(NARROW)
+    other[CLOSE * BLOCK : CLOSE * BLOCK + SMALL] = top
+    other[CLOSE * BLOCK + SMALL :] = (value - top.astype(WIDE)).astype(NARROW)
+
+
+def pack(mine, small, other, pieces):
+    end = CLOSE * BLOCK
+    top = other[end : end + SMALL].astype(WIDE)
+    both = small[...] + (top + other[end + SMALL :].astype(WIDE))
+    both = both.astype(NARROW)
     for near in range(CLOSE):
-        for turn, rows in ((0, slice(0, BLOCK)), (CLOSE, slice(BLOCK, 2 * BLOCK))):
-            far = lax.rem(place[0] // (2 * CLOSE) + near + turn, FAR)
-            pieces[near, rows] = (mine[far] + other[far].astype(WIDE)).astype(NARROW)
-        pieces[near, 2 * BLOCK :] = taps_rows
+        for start in range(0, BLOCK, 32):
+            rows = slice(start, start + 32)
+            there = other[near * BLOCK + start : near * BLOCK + start + 32].astype(WIDE)
+            pieces[near, rows] = (mine[near, rows] + there).astype(NARROW)
+        pieces[near, BLOCK:] = both
 
 
 def gated_gradient(extended, taps, d_gated, margin, taps_wide):
@@ -248,40 +262,23 @@
                 d_gated[half, start - EDGE : start] = found
 
 
-def fold_near(arrived, to_first, to_second):
-    for start in range(0, 2 * BLOCK + 32, 32):
+def fold_near(arrived, payload):
+    for start in range(0, BLOCK + SMALL, 32):
         rows = slice(start, start + 32)
         total = arrived[0, rows].astype(WIDE)
         for near in range(1, CLOSE):
             total = total + arrived[near, rows].astype(WIDE)
-        total = total.astype(NARROW)
-        if start < BLOCK:
-            to_first[rows] = total
-        elif start < 2 * BLOCK:
-            to_second[start - BLOCK : start - BLOCK + 32] = total
-        else:
-            to_first[BLOCK:] = total
-            to_second[BLOCK:] = total
-
-
-def fold_far(place, kept, first, second, message):
-    own = place[0] // 2 % CLOSE == 0
-    for start in range(BLOCK, -1, -8):
-        size = 32 if start == BLOCK else 8
-        rows = slice(start, start + size)
-        here = jnp.where(own, kept[rows].astype(WIDE), first[rows].astype(WIDE))
-        total = (here + second[rows].astype(WIDE)).astype(NARROW)
-        if start == BLOCK:
-            for position in range(2 * CLOSE):
-                message[position, OWN:] = total
-        else:
-            for position in range(2 * CLOSE):
-                if GATHER_ORDER[position] // 2 == start // 8:
-                    message[position, 0:OWN] = total
+        payload[rows] = total.astype(NARROW)
+
+
+def hand_out(payload, message):
+    for position, member in enumerate(GATHER_ORDER):
+        message[position, 0:OWN] = payload[member * OWN : (member + 1) * OWN]
+        message[position, OWN:] = payload[BLOCK:]
 
 
 def finish(
-    place, arrived, d_gated, late, value, gate,
+    arrived, d_gated, late, value, gate,
     value_grad, gate_grad, weight_grad, taps_grad, gain_grad,
 ):
     for half in range(HALVES):
@@ -294,29 +291,22 @@
             wide = value[rows, lanes(half)].astype(WIDE)
             value_grad[rows, lanes(half)] = (grad * sig).astype(NARROW)
             gate_grad[rows, lanes(half)] = (grad * wide * sig * (1.0 - sig)).astype(NARROW)
-    by_core = []
-    for side in range(2):
-        positions = [p for p in range(2 * CLOSE) if GATHER_ORDER[p] % 2 == side]
-        total = arrived[positions[0], 0:OWN].astype(WIDE)
-        for position in positions[1:]:
-            total = total + arrived[position, 0:OWN].astype(WIDE)
-        by_core.append(total)
-    weight_grad[...] = jnp.where(place[0] % 2 == 0, by_core[0], by_core[1])
-    total = arrived[0, OWN:].astype(WIDE)
+    total = arrived[0].astype(WIDE)
     for position in range(1, 2 * CLOSE):
-        total = total + arrived[position, OWN:].astype(WIDE)
-    taps_grad[...] = total[0:TAPS]
-    gain_grad[...] = total[TAPS : TAPS + 1]
-
-
-def to_block(value, turn):
+        total = total + arrived[position].astype(WIDE)
+    weight_grad[...] = total[0:OWN]
+    taps_grad[...] = total[OWN : OWN + TAPS]
+    gain_grad[...] = total[OWN + TAPS :]
+
+
+def to_block(value):
     pairs = []
     for far in range(FAR):
         for near in range(CLOSE):
-            step = (near + turn) % FAR
-            if step:
-                pairs.append((far * CLOSE + near, (far + step) % FAR * CLOSE + near))
-    return lax.ppermute(value, ("zh", *NEAR), pairs)
+            for core in range(2):
+                target = (far + OFFSETS[core][near]) % FAR
+                pairs.append(((far * CLOSE + near) * 2 + core, (target * CLOSE + near) * 2 + core))
+    return lax.ppermute(value, SP, pairs)
 
 
 def shards(
@@ -344,56 +334,53 @@
         flops=100 * ROWS * WIDTH,
     )
     edge = (HALVES, EDGE, LANES)
-    first_scaled, first_spread, first_hidden, message, gain_part = call_with(
+    place = lax.axis_index(SP).reshape(1)
+    first_scaled, first_spread, first_hidden, message, gain_part = scalar_call(
         head,
         [
             (edge, WIDE), (edge, WIDE), ((EDGE, WIDTH), NARROW),
             ((TP, 8, LANES), WIDE), ((HALVES, 8, LANES), WIDE),
         ],
-        [
+        place, halo, gated, upstream, conv_taps, row_gain, row_mean, row_scale, sums,
+        gain_part,
+        scratch=[
             pltpu.VMEM((HALVES, 2 * EDGE, LANES), WIDE),
             taps_scratch,
             pltpu.VMEM((2, LANES, LANES), WIDE),
         ],
-        halo, gated, upstream, conv_taps, row_gain, row_mean, row_scale, sums, gain_part,
         flops=10 * ROWS * WIDTH,
     )
     sums = exchange(message, "tp")
-    place = lax.axis_index(SP).reshape(1)
-    grouped = (FAR, CLOSE * OWN, WIDTH)
-    mine, other = scalar_call(
-        weight_product, [(grouped, WIDE), (grouped, NARROW)],
-        place, out_cotangent, hidden, first_hidden,
-        scratch=[pltpu.VMEM((ROWS, WIDTH), NARROW)], flops=2 * ROWS * WIDTH * MODEL,
+    rows = CLOSE * BLOCK + 2 * SMALL
+    mine, other, small, extended = scalar_call(
+        backward,
+        [
+            ((CLOSE, BLOCK, WIDTH), WIDE), ((rows, WIDTH), NARROW), ((SMALL, WIDTH), WIDE),
+            ((HALVES, ROWS + 2 * EDGE, LANES), WIDE),
+        ],
+        place, sums, scaled, spread, first_scaled, first_spread, halo, gated, row_scale, gain_part,
+        out_cotangent, hidden, first_hidden,
+        scratch=[sides, pltpu.VMEM((ROWS, WIDTH), NARROW)], flops=2 * ROWS * WIDTH * MODEL,
     )
     other = lax.ppermute(other, "c", [(0, 1), (1, 0)])
-    pieces, extended = scalar_call(
-        backward,
-        [((CLOSE, 2 * BLOCK + TAPS + 1, WIDTH), NARROW), ((HALVES, ROWS + 2 * EDGE, LANES), WIDE)],
-        place, sums, scaled, spread, first_scaled, first_spread, halo, gated, row_scale,
-        gain_part, mine, other, scratch=[taps_scratch, sides],
-        flops=100 * ROWS * WIDTH,
-    )
-    arrived = exchange(pieces, NEAR)
-    payload = ((BLOCK + TAPS + 1, WIDTH), NARROW)
-    to_first, to_second = call(fold_near, [payload, payload], arrived, flops=1 << 20)
-    first = to_block(to_first, 0)
-    second = to_block(to_second, CLOSE)
     d_gated, margin = call_with(
         gated_gradient, [(split, WIDE), ((HALVES, EDGE, LANES), WIDE)], [taps_scratch],
         extended, conv_taps, flops=100 * ROWS * WIDTH,
     )
+    (pieces,) = call(
+        pack, [((CLOSE, BLOCK + SMALL, WIDTH), NARROW)], mine, small, other, flops=1 << 20
+    )
+    arrived = exchange(pieces, NEAR)
+    (payload,) = call(fold_near, [((BLOCK + SMALL, WIDTH), NARROW)], arrived, flops=1 << 20)
+    payload = to_block(payload)
     late = shifted(margin, SP, -1)
-    (message,) = scalar_call(
-        fold_far, [((2 * CLOSE, OWN + TAPS + 1, WIDTH), NARROW)],
-        place, to_first, first, second,
-    )
+    (message,) = call(hand_out, [((2 * CLOSE, OWN + SMALL, WIDTH), NARROW)], payload, flops=1 << 16)
     arrived = exchange(message, (*NEAR, "c"), GATHER_ORDER)
     narrow = ((ROWS, WIDTH), NARROW)
-    value_grad, gate_grad, weight_grad, taps_grad, gain_grad = scalar_call(
+    value_grad, gate_grad, weight_grad, taps_grad, gain_grad = call(
         finish,
         [narrow, narrow, ((OWN, WIDTH), WIDE), ((TAPS, WIDTH), WIDE), ((1, WIDTH), WIDE)],
-        place, arrived, d_gated, late, proj_value, proj_gate,
+        arrived, d_gated, late, proj_value, proj_gate, flops=10 * ROWS * WIDTH,
     )
     return (value_grad, gate_grad, weight_grad, taps_grad, gain_grad.reshape(WIDTH))
 

time: 94.1 us -> 85 us (0.903)
  starting transfers between devices: 42.8 us -> 31.1 us
  blocking collectives: 27.8 us -> 29.3 us
  local copies, waits for them, and re-layouts: 0.04 us -> 1.06 us
    ppermute x2 -> x1, starting transfers between devices: 20.5 us -> 12.1 us  [to_block(): return lax.ppermute(value, SP, pairs)]
    all_to_all x1, starting transfers between devices: 13.9 us -> 10.6 us  [exchange(): lax.all_to_all(pieces, axes, 0, 0, tiled=True, axis_index_groups=groups)]
    ppermute x1, waiting for transfers between devices: 0.01 us -> 1.92 us  [shards(): other = lax.ppermute(other, 'c', [(0, 1), (1, 0)])]
    pallas_call x1 -> x4, Pallas kernels: 0.09 us -> 1.8 us  [call(): pl.pallas_call(body, out_shape=shapes, compiler_params=pltpu.CompilerPara...]
    pallas_call x4 -> x2, Pallas kernels: 3.65 us -> 2.06 us  [scalar_call(): pl.pallas_call(body, out_shape=shapes, in_specs=[pl.BlockSpec(memory_spac...]
    ppermute x2 -> x1, waiting for transfers between devices: 7.97 us -> 6.38 us  [to_block(): return lax.ppermute(value, SP, pairs)]
    all_to_all x2, blocking collectives: 27.8 us -> 29.3 us  [exchange(): lax.all_to_all(pieces, axes, 0, 0, tiled=True, axis_index_groups=groups)]
    unnamed x16 -> x20, local copies, waits for them, and re-layouts: 0.04 us -> 1.06 us
  transfers between devices with their start and end apart: 6 -> 5, of which waited for: 2 -> 3; matrix products, arithmetic and copies ran while one was open for 2% -> 2% of each run, Pallas kernels for 2% -> 3%
where the time goes in v9:
time: 85 us; the launch traced here: 84.5 us
  starting transfers between devices  31.1 us (37%)
  blocking collectives  29.3 us (34%)
  waiting for transfers between devices  13.3 us (16%)
  Pallas kernels  5.98 us (7%)
  matrix products  2.01 us (2%)
  local copies, waits for them, and re-layouts  1.06 us (1%)
  other arithmetic  0.85 us (1%)
  between operations  0.85 us (1%)
    all_to_all x2, blocking collectives, exchange(): lax.all_to_all(pieces, axes, 0, 0, tiled=True, axis_index_groups=groups)  29.3 us
    ppermute x1, starting transfers between devices, to_block(): return lax.ppermute(value, SP, pairs)  12.1 us
    all_to_all x1, starting transfers between devices, exchange(): lax.all_to_all(pieces, axes, 0, 0, tiled=True, axis_index_groups=groups)  10.6 us
    ppermute x2, starting transfers between devices, shifted(): lax.ppermute(value, axis, [(source, source + steps) for source in range(f...  6.45 us
    ppermute x1, waiting for transfers between devices, to_block(): return lax.ppermute(value, SP, pairs)  6.38 us
    ppermute x2, waiting for transfers between devices, shifted(): lax.ppermute(value, axis, [(source, source + steps) for source in range(f...  5.04 us
    pallas_call x2, Pallas kernels, call_with(): pl.pallas_call(body, out_shape=shapes, scratch_shapes=scratch, compiler_p...  2.12 us
    pallas_call x2, Pallas kernels, scalar_call(): pl.pallas_call(body, out_shape=shapes, in_specs=[pl.BlockSpec(memory_spac...  2.06 us
  transfers between devices with their start and end apart: 5, of which 3 were waited for; matrix products, arithmetic and copies ran while one was open for 2% of the time, Pallas kernels for 3%

profile of v9, /device:TPU:7, one launch (start us, length us, event | category | flops | bytes accessed | tf_op | source)
XLA Modules:
  0.0 84.5 jit_solution(16614770539180303485)
XLA Ops:
  0.6 0.0 copy-start
  0.6 0.0 copy-start.2
  0.7 0.0 copy-start.3
  0.7 0.0 copy-start.7
  0.7 0.0 copy-start.6
  0.7 0.0 copy-start.8
  0.7 0.0 copy-start.9
  0.7 0.9 %multiply_convert_fusion = bf16[32,256]{1,0:T(8,128)(2,1)S(1)} fusion(bf16[384,256]{1,0:T(8,128)(2,1)} %gate.3, bf16[384,256]{1,0:T(8,128)(2,1)} %value.3), kind=kLoop, calls=%fused_computation | loop fusion | flops 57344 | bytes 49152 | tf_op jit(solution)/shard_map/convert_element_type | solution.py:316
  1.6 0.0 copy-start.1
  1.6 4.2 %collective-permute-start = (bf16[32,256]{1,0:T(8,128)(2,1)S(1)}, bf16[32,256]{1,0:T(8,128)(2,1)S(1)}, u32[]{:S(2)}, u32[]{:S(2)}) collective-permute-start(bf16[32,256]{1,0:T(8,128)(2,1)S(1)} %multiply_convert_fusion), channel_id=1, source_target_pairs={{0,4},{4,8},{8,12},{12,16},{16,20},{20,24},{24,28},{28,32},{32,36}... | collective-permute-start | bytes 49160 | tf_op jit(solution)/shard_map/ppermute | solution.py:36
  5.7 0.0 copy-done
  5.7 2.0 %fusion.upstream = f32[384,256]{1,0:T(8,128)S(1)} fusion(bf16[384,2048]{1,0:T(8,128)(2,1)} %cotangent.1, bf16[256,2048]{1,0:T(8,128)(2,1)S(1)} %copy-done), kind=kOutput, calls=%fused_computation.1 | convolution fusion | flops 402653184 | bytes 3014656 | tf_op jit(solution)/shard_map/dot_general | solution.py:319
  7.8 0.0 copy-done.2
  7.8 0.0 copy-done.3
  7.8 0.0 copy-done.7
  7.8 0.0 copy-done.6
  7.8 0.0 copy-done.8
  7.8 0.0 copy-done.9
  7.8 1.3 %shard_map.119 = (bf16[384,256]{1,0:T(8,128)(2,1)S(1)}, f32[2,352,128]{2,1,0:T(8,128)S(1)}, f32[2,352,128]{2,1,0:T(8,128)S(1)}, bf16[352,256]{1,0:T(8,128)(2,1)S...) custom-call(bf16[384,256]{1,0:T(8,128)(2,1)S(1)} %copy-done.3, bf16[384,256]{1,0:T(8,128)(2,1)S(1)} %copy-done.2, ...), custom_call_target="tpu_custom_call" | custom-call | flops 9830400 | bytes 1916416 | tf_op jit(solution)/shard_map/pallas_call | solution.py:391
  9.1 0.0 collective-permute-done.halo
  9.1 0.2 shard_map.120
  9.3 8.2 %all_to_all.15.sums = f32[4,8,128]{2,1,0:T(8,128)S(1)} all-to-all(f32[4,8,128]{2,1,0:T(8,128)S(1)} %get-tuple-element.30), channel_id=1, replica_groups=mesh['zh'=16,'zl'=2,'x'=4,'c'=2,'tp'=4] {'tp'}, dimensions={0} | all-to-all | bytes 32768 | tf_op jit(solution)/shard_map/all_to_all | solution.py:41
  17.5 0.0 copy-done.1
  17.5 1.8 %shard_map.121 = (f32[8,128,256]{2,1,0:T(8,128)S(1)}, bf16[1088,256]{1,0:T(8,128)(2,1)S(1)}, f32[32,256]{1,0:T(8,128)S(1)}, f32[2,448,128]{2,1,0:T(8,128)S(1)}) custom-call(s32[1]{0:T(128)} %bitcast._.place, f32[4,8,128]{2,1,0:T(8,128)S(1)} %all_to_all.15.sums, f32[2,352,128]{2,1,0:T(8,128)S(1)} %get-tuple-element.31.scaled, ...), custom_call_target="tpu_custom_call" | custom-call | flops 402653184 | bytes 4892160 | tf_op jit(solution)/shard_map/pallas_call | solution.py:404
  19.4 0.0 copy-start.4
  19.4 1.9 %collective-permute-start.1 = (bf16[1088,256]{1,0:T(8,128)(2,1)S(1)}, bf16[1088,256]{1,0:T(8,128)(2,1)S(1)}, u32[]{:S(2)}, u32[]{:S(2)}) collective-permute-start(bf16[1088,256]{1,0:T(8,128)(2,1)S(1)} %get-tuple-element.40), channel_id=1, source_target_pairs={{0,4},{4,0},{1,5},{5,1},{2,6},{6,2},{3,7},{7,3},{8,12},{12,8},{9,1... | collective-permute-start | bytes 1671176 | tf_op jit(solution)/shard_map/ppermute | solution.py:365
  21.3 1.9 %collective-permute-done.1.other = bf16[1088,256]{1,0:T(8,128)(2,1)S(1)} collective-permute-done((bf16[1088,256]{1,0:T(8,128)(2,1)S(1)}, bf16[1088,256]{1,0:T(8,128)(2,1)S(1)}, u32[]{:S(2)}, u32[]{:S(2)}) %collective-permute-start.1) | collective-permute-done | bytes 557088 | tf_op jit(solution)/shard_map/ppermute | solution.py:365
  23.2 0.1 shard_map.122
  23.3 21.1 %all_to_all.16.arrived = bf16[8,160,256]{2,1,0:T(8,128)(2,1)S(1)} all-to-all(bf16[8,160,256]{2,1,0:T(8,128)(2,1)S(1)} %shard_map.122), channel_id=1, replica_groups=mesh['zh'=16,'zl'=2,'x'=4,'c'=2,'tp'=4] {'zl','x'}, dimensions={0} | all-to-all | bytes 1310720 | tf_op jit(solution)/shard_map/all_to_all | solution.py:41
  44.5 0.0 copy-done.4
  44.5 0.1 shard_map.123
  44.6 12.1 %collective-permute-start.2 = (bf16[160,256]{1,0:T(8,128)(2,1)S(1)}, bf16[160,256]{1,0:T(8,128)(2,1)S(1)}, u32[]{:S(2)}, u32[]{:S(2)}) collective-permute-start(bf16[160,256]{1,0:T(8,128)(2,1)S(1)} %shard_map.123), channel_id=1, source_target_pairs={{0,0},{4,516},{8,968},{12,460},{16,912},{20,404},{24,856},{28,348}... | collective-permute-start | bytes 245768 | tf_op jit(solution)/shard_map/ppermute | solution.py:309
  56.7 6.4 %collective-permute-done.2.payload = bf16[160,256]{1,0:T(8,128)(2,1)S(1)} collective-permute-done((bf16[160,256]{1,0:T(8,128)(2,1)S(1)}, bf16[160,256]{1,0:T(8,128)(2,1)S(1)}, u32[]{:S(2)}, u32[]{:S(2)}) %collective-permute-start.2) | collective-permute-done | bytes 81952 | tf_op jit(solution)/shard_map/ppermute | solution.py:309
  63.1 0.7 shard_map.124
  63.8 10.6 %all-to-all-start.2 = ((bf16[16,40,256]{2,1,0:T(8,128)(2,1)}), bf16[16,40,256]{2,1,0:T(8,128)(2,1)S(1)}, u32[]{:S(2)}, u32[]{:S(2)}) async-start(bf16[16,40,256]{2,1,0:T(8,128)(2,1)} %shard_map.124), calls=%async_computation.2 | async-start | bytes 655360 | tf_op jit(solution)/shard_map/all_to_all | solution.py:41
  74.4 0.0 copy-start.5
  74.4 1.0 %copy-done.5 = f32[2,448,128]{2,1,0:T(8,128)S(1)} copy-done((f32[2,448,128]{2,1,0:T(8,128)S(1)}, f32[2,448,128]{2,1,0:T(8,128)}, u32[]{:S(2)}) %copy-start.5) | copy-done | bytes 458776
  75.4 0.9 %shard_map.125 = (f32[2,384,128]{2,1,0:T(8,128)S(1)}, f32[2,32,128]{2,1,0:T(8,128)S(1)}) custom-call(f32[2,448,128]{2,1,0:T(8,128)S(1)} %copy-done.5, bf16[31,256]{1,0:T(8,128)(2,1)S(1)} %copy-done.6), custom_call_target="tpu_custom_call" | custom-call | flops 9830400 | bytes 900608 | tf_op jit(solution)/shard_map/pallas_call | solution.py:391
  76.3 2.3 %collective-permute-start.3 = (f32[2,32,128]{2,1,0:T(8,128)S(1)}, f32[2,32,128]{2,1,0:T(8,128)S(1)}, u32[]{:S(2)}, u32[]{:S(2)}) collective-permute-start(f32[2,32,128]{2,1,0:T(8,128)S(1)} %get-tuple-element.43), channel_id=1, source_target_pairs={{4,0},{8,4},{12,8},{16,12},{20,16},{24,20},{28,24},{32,28},{36,32}... | collective-permute-start | bytes 98312 | tf_op jit(solution)/shard_map/ppermute | solution.py:36
  78.6 5.0 %collective-permute-done.3.late = f32[2,32,128]{2,1,0:T(8,128)S(1)} collective-permute-done((f32[2,32,128]{2,1,0:T(8,128)S(1)}, f32[2,32,128]{2,1,0:T(8,128)S(1)}, u32[]{:S(2)}, u32[]{:S(2)}) %collective-permute-start.3) | collective-permute-done | bytes 32800 | tf_op jit(solution)/shard_map/ppermute | solution.py:36
  83.6 0.0 all-to-all-done.2.arrived
  83.6 0.9 %shard_map.126 = (bf16[384,256]{1,0:T(8,128)(2,1)}, bf16[384,256]{1,0:T(8,128)(2,1)}, f32[8,256]{1,0:T(8,128)}, f32[31,256]{1,0:T(8,128)}, f32[1,256]{1,0:T(1,128)}) custom-call(bf16[16,40,256]{2,1,0:T(8,128)(2,1)S(1)} %all-to-all-done.2.arrived, f32[2,384,128]{2,1,0:T(8,128)S(1)} %get-tuple-element.42.d_gated, ...), custom_call_target="tpu_custom_call" | custom-call | flops 983040 | bytes 1581056 | tf_op jit(solution)/shard_map/pallas_call | solution.py:55
Async XLA Ops:
  0.6 5.1 %copy-start = (bf16[256,2048]{1,0:T(8,128)(2,1)S(1)}, bf16[256,2048]{1,0:T(8,128)(2,1)}, u32[]{:S(2)}) copy-start(bf16[256,2048]{1,0:T(8,128)(2,1)} %param.11) | copy-start | bytes 3145732
  0.6 7.1 %copy-start.2 = (bf16[384,256]{1,0:T(8,128)(2,1)S(1)}, bf16[384,256]{1,0:T(8,128)(2,1)}, u32[]{:S(2)}) copy-start(bf16[384,256]{1,0:T(8,128)(2,1)} %gate.3) | copy-start | bytes 589828
  0.7 7.1 %copy-start.3 = (bf16[384,256]{1,0:T(8,128)(2,1)S(1)}, bf16[384,256]{1,0:T(8,128)(2,1)}, u32[]{:S(2)}) copy-start(bf16[384,256]{1,0:T(8,128)(2,1)} %value.3) | copy-start | bytes 589828
  0.7 7.1 %copy-start.7 = (f32[384]{0:T(512)S(1)}, f32[384]{0:T(512)}, u32[]{:S(2)}) copy-start(f32[384]{0:T(512)} %scale.5) | copy-start | bytes 4612
  0.7 7.1 %copy-start.6 = (bf16[31,256]{1,0:T(8,128)(2,1)S(1)}, bf16[31,256]{1,0:T(8,128)(2,1)}, u32[]{:S(2)}) copy-start(bf16[31,256]{1,0:T(8,128)(2,1)} %taps.5) | copy-start | bytes 47620
  0.7 7.1 %copy-start.8 = (f32[384]{0:T(512)S(1)}, f32[384]{0:T(512)}, u32[]{:S(2)}) copy-start(f32[384]{0:T(512)} %mean.3) | copy-start | bytes 4612
  0.7 7.1 %copy-start.9 = (f32[256]{0:T(256)S(1)}, f32[256]{0:T(256)}, u32[]{:S(2)}) copy-start(f32[256]{0:T(256)} %param.13) | copy-start | bytes 3076
  1.6 16.0 %copy-start.1 = (bf16[384,2048]{1,0:T(8,128)(2,1)S(1)}, bf16[384,2048]{1,0:T(8,128)(2,1)}, u32[]{:S(2)}) copy-start(bf16[384,2048]{1,0:T(8,128)(2,1)} %cotangent.1) | copy-start | bytes 4718596
  1.6 7.5 %collective-permute-start = (bf16[32,256]{1,0:T(8,128)(2,1)S(1)}, bf16[32,256]{1,0:T(8,128)(2,1)S(1)}, u32[]{:S(2)}, u32[]{:S(2)}) collective-permute-start(bf16[32,256]{1,0:T(8,128)(2,1)S(1)} %multiply_convert_fusion), channel_id=1, source_target_pairs={{0,4},{4,8},{8,12},{12,16},{16,20},{20,24},{24,28},{28,32},{32,36}... | collective-permute-start | bytes 49160 | tf_op jit(solution)/shard_map/ppermute | solution.py:36
  19.4 25.1 %copy-start.4 = (f32[2,448,128]{2,1,0:T(8,128)}, f32[2,448,128]{2,1,0:T(8,128)S(1)}, u32[]{:S(2)}) copy-start(f32[2,448,128]{2,1,0:T(8,128)S(1)} %get-tuple-element.41.extended) | copy-start | bytes 1376260
  19.4 3.9 %collective-permute-start.1 = (bf16[1088,256]{1,0:T(8,128)(2,1)S(1)}, bf16[1088,256]{1,0:T(8,128)(2,1)S(1)}, u32[]{:S(2)}, u32[]{:S(2)}) collective-permute-start(bf16[1088,256]{1,0:T(8,128)(2,1)S(1)} %get-tuple-element.40), channel_id=1, source_target_pairs={{0,4},{4,0},{1,5},{5,1},{2,6},{6,2},{3,7},{7,3},{8,12},{12,8},{9,1... | collective-permute-start | bytes 1671176 | tf_op jit(solution)/shard_map/ppermute | solution.py:365
  44.6 18.5 %collective-permute-start.2 = (bf16[160,256]{1,0:T(8,128)(2,1)S(1)}, bf16[160,256]{1,0:T(8,128)(2,1)S(1)}, u32[]{:S(2)}, u32[]{:S(2)}) collective-permute-start(bf16[160,256]{1,0:T(8,128)(2,1)S(1)} %shard_map.123), channel_id=1, source_target_pairs={{0,0},{4,516},{8,968},{12,460},{16,912},{20,404},{24,856},{28,348}... | collective-permute-start | bytes 245768 | tf_op jit(solution)/shard_map/ppermute | solution.py:309
  63.8 19.8 %all-to-all-start.2 = ((bf16[16,40,256]{2,1,0:T(8,128)(2,1)}), bf16[16,40,256]{2,1,0:T(8,128)(2,1)S(1)}, u32[]{:S(2)}, u32[]{:S(2)}) async-start(bf16[16,40,256]{2,1,0:T(8,128)(2,1)} %shard_map.124), calls=%async_computation.2 | async-start | bytes 655360 | tf_op jit(solution)/shard_map/all_to_all | solution.py:41
  74.4 1.0 %copy-start.5 = (f32[2,448,128]{2,1,0:T(8,128)S(1)}, f32[2,448,128]{2,1,0:T(8,128)}, u32[]{:S(2)}) copy-start(f32[2,448,128]{2,1,0:T(8,128)} %copy-done.4) | copy-start | bytes 1376260
  76.3 7.3 %collective-permute-start.3 = (f32[2,32,128]{2,1,0:T(8,128)S(1)}, f32[2,32,128]{2,1,0:T(8,128)S(1)}, u32[]{:S(2)}, u32[]{:S(2)}) collective-permute-start(f32[2,32,128]{2,1,0:T(8,128)S(1)} %get-tuple-element.43), channel_id=1, source_target_pairs={{4,0},{8,4},{12,8},{16,12},{20,16},{24,20},{28,24},{32,28},{36,32}... | collective-permute-start | bytes 98312 | tf_op jit(solution)/shard_map/ppermute | solution.py:36

commit v10 on v9

--- a/solution.py
+++ b/solution.py
@@ -13,6 +13,7 @@
 CLOSE = 8
 AXES = (("zh", FAR), ("zl", 2), ("x", 4), ("c", 2))
 TP = 4
+SUMS_ORDER = [1, 2, 3, 0]
 OFFSETS = ((0, -1, -2, -3, 1, 2, 3, -4), (8, 7, 6, 5, -7, -6, -5, 4))
 BLOCK = CLOSE * 2 * 8
 GATHER_ORDER = [(place + 1) % (2 * CLOSE) for place in range(2 * CLOSE)]
@@ -277,8 +278,17 @@
         message[position, OWN:] = payload[BLOCK:]
 
 
+def totals(arrived, total):
+    for start in range(0, OWN + SMALL, 8):
+        rows = slice(start, start + 8)
+        found = arrived[0, rows].astype(WIDE)
+        for position in range(1, 2 * CLOSE):
+            found = found + arrived[position, rows].astype(WIDE)
+        total[rows] = found
+
+
 def finish(
-    arrived, d_gated, late, value, gate,
+    total, d_gated, late, value, gate,
     value_grad, gate_grad, weight_grad, taps_grad, gain_grad,
 ):
     for half in range(HALVES):
@@ -291,9 +301,6 @@
             wide = value[rows, lanes(half)].astype(WIDE)
             value_grad[rows, lanes(half)] = (grad * sig).astype(NARROW)
             gate_grad[rows, lanes(half)] = (grad * wide * sig * (1.0 - sig)).astype(NARROW)
-    total = arrived[0].astype(WIDE)
-    for position in range(1, 2 * CLOSE):
-        total = total + arrived[position].astype(WIDE)
     weight_grad[...] = total[0:OWN]
     taps_grad[...] = total[OWN : OWN + TAPS]
     gain_grad[...] = total[OWN + TAPS :]
@@ -350,7 +357,7 @@
         ],
         flops=10 * ROWS * WIDTH,
     )
-    sums = exchange(message, "tp")
+    sums = exchange(message, "tp", SUMS_ORDER)
     rows = CLOSE * BLOCK + 2 * SMALL
     mine, other, small, extended = scalar_call(
         backward,
@@ -376,11 +383,12 @@
     late = shifted(margin, SP, -1)
     (message,) = call(hand_out, [((2 * CLOSE, OWN + SMALL, WIDTH), NARROW)], payload, flops=1 << 16)
     arrived = exchange(message, (*NEAR, "c"), GATHER_ORDER)
+    (total,) = call(totals, [((OWN + SMALL, WIDTH), WIDE)], arrived, flops=1 << 20)
     narrow = ((ROWS, WIDTH), NARROW)
     value_grad, gate_grad, weight_grad, taps_grad, gain_grad = call(
         finish,
         [narrow, narrow, ((OWN, WIDTH), WIDE), ((TAPS, WIDTH), WIDE), ((1, WIDTH), WIDE)],
-        arrived, d_gated, late, proj_value, proj_gate, flops=10 * ROWS * WIDTH,
+        total, d_gated, late, proj_value, proj_gate, flops=10 * ROWS * WIDTH,
     )
     return (value_grad, gate_grad, weight_grad, taps_grad, gain_grad.reshape(WIDTH))
 

time: 85 us -> 84.8 us (level)
    ppermute x2, waiting for transfers between devices: 5.04 us -> 2.4 us  [shifted(): lax.ppermute(value, axis, [(source, source + steps) for source in range(f...]
    all_to_all x1, waiting for transfers between devices: 0.01 us -> 2.59 us  [exchange(): lax.all_to_all(pieces, axes, 0, 0, tiled=True, axis_index_groups=groups)]
    pallas_call x4 -> x5, Pallas kernels: 1.8 us -> 1.85 us  [call(): pl.pallas_call(body, out_shape=shapes, compiler_params=pltpu.CompilerPara...]
  transfers between devices with their start and end apart: 5 -> 5, of which waited for: 3 -> 4; matrix products, arithmetic and copies ran while one was open for 2% -> 2% of each run, Pallas kernels for 3% -> 3%
where the time goes in v10:
time: 84.8 us; the launch traced here: 84.3 us
  starting transfers between devices  31.1 us (37%)
  blocking collectives  29.2 us (34%)
  waiting for transfers between devices  13.3 us (16%)
  Pallas kernels  6.02 us (7%)
  matrix products  2.01 us (2%)
  local copies, waits for them, and re-layouts  1.06 us (1%)
  other arithmetic  0.85 us (1%)
  between operations  0.85 us (1%)
    all_to_all x2, blocking collectives, exchange(): lax.all_to_all(pieces, axes, 0, 0, tiled=True, axis_index_groups=groups)  29.2 us
    ppermute x1, starting transfers between devices, to_block(): return lax.ppermute(value, SP, pairs)  12 us
    all_to_all x1, starting transfers between devices, exchange(): lax.all_to_all(pieces, axes, 0, 0, tiled=True, axis_index_groups=groups)  10.7 us
    ppermute x2, starting transfers between devices, shifted(): lax.ppermute(value, axis, [(source, source + steps) for source in range(f...  6.45 us
    ppermute x1, waiting for transfers between devices, to_block(): return lax.ppermute(value, SP, pairs)  6.38 us
    all_to_all x1, waiting for transfers between devices, exchange(): lax.all_to_all(pieces, axes, 0, 0, tiled=True, axis_index_groups=groups)  2.59 us
    ppermute x2, waiting for transfers between devices, shifted(): lax.ppermute(value, axis, [(source, source + steps) for source in range(f...  2.4 us
    pallas_call x2, Pallas kernels, call_with(): pl.pallas_call(body, out_shape=shapes, scratch_shapes=scratch, compiler_p...  2.12 us
  transfers between devices with their start and end apart: 5, of which 4 were waited for; matrix products, arithmetic and copies ran while one was open for 2% of the time, Pallas kernels for 3%

profile of v10, /device:TPU:7, one launch (start us, length us, event | category | flops | bytes accessed | tf_op | source)
XLA Modules:
  0.0 84.3 jit_solution(16390946093939387374)
XLA Ops:
  0.6 0.0 copy-start
  0.6 0.0 copy-start.2
  0.7 0.0 copy-start.3
  0.7 0.0 copy-start.7
  0.7 0.0 copy-start.6
  0.7 0.0 copy-start.8
  0.7 0.0 copy-start.9
  0.7 0.9 %multiply_convert_fusion = bf16[32,256]{1,0:T(8,128)(2,1)S(1)} fusion(bf16[384,256]{1,0:T(8,128)(2,1)} %gate.3, bf16[384,256]{1,0:T(8,128)(2,1)} %value.3), kind=kLoop, calls=%fused_computation | loop fusion | flops 57344 | bytes 49152 | tf_op jit(solution)/shard_map/convert_element_type | solution.py:323
  1.6 0.0 copy-start.1
  1.6 4.2 %collective-permute-start = (bf16[32,256]{1,0:T(8,128)(2,1)S(1)}, bf16[32,256]{1,0:T(8,128)(2,1)S(1)}, u32[]{:S(2)}, u32[]{:S(2)}) collective-permute-start(bf16[32,256]{1,0:T(8,128)(2,1)S(1)} %multiply_convert_fusion), channel_id=1, source_target_pairs={{0,4},{4,8},{8,12},{12,16},{16,20},{20,24},{24,28},{28,32},{32,36}... | collective-permute-start | bytes 49160 | tf_op jit(solution)/shard_map/ppermute | solution.py:37
  5.7 0.0 copy-done
  5.7 2.0 %fusion.upstream = f32[384,256]{1,0:T(8,128)S(1)} fusion(bf16[384,2048]{1,0:T(8,128)(2,1)} %cotangent.1, bf16[256,2048]{1,0:T(8,128)(2,1)S(1)} %copy-done), kind=kOutput, calls=%fused_computation.1 | convolution fusion | flops 402653184 | bytes 3014656 | tf_op jit(solution)/shard_map/dot_general | solution.py:326
  7.8 0.0 copy-done.2
  7.8 0.0 copy-done.3
  7.8 0.0 copy-done.7
  7.8 0.0 copy-done.6
  7.8 0.0 copy-done.8
  7.8 0.0 copy-done.9
  7.8 1.3 %shard_map.119 = (bf16[384,256]{1,0:T(8,128)(2,1)S(1)}, f32[2,352,128]{2,1,0:T(8,128)S(1)}, f32[2,352,128]{2,1,0:T(8,128)S(1)}, bf16[352,256]{1,0:T(8,128)(2,1)S...) custom-call(bf16[384,256]{1,0:T(8,128)(2,1)S(1)} %copy-done.3, bf16[384,256]{1,0:T(8,128)(2,1)S(1)} %copy-done.2, ...), custom_call_target="tpu_custom_call" | custom-call | flops 9830400 | bytes 1916416 | tf_op jit(solution)/shard_map/pallas_call | solution.py:399
  9.1 0.0 collective-permute-done.halo
  9.1 0.2 shard_map.120
  9.3 8.0 %all_to_all.15.sums = f32[4,8,128]{2,1,0:T(8,128)S(1)} all-to-all(f32[4,8,128]{2,1,0:T(8,128)S(1)} %get-tuple-element.30), channel_id=1, replica_groups={{1,2,3,0},{5,6,7,4},{9,10,11,8},{13,14,15,12},{17,18,19,16},{21,22,23,2..., dimensions={0} | all-to-all | bytes 32768 | tf_op jit(solution)/shard_map/all_to_all | solution.py:42
  17.3 0.0 copy-done.1
  17.3 1.8 %shard_map.121 = (f32[8,128,256]{2,1,0:T(8,128)S(1)}, bf16[1088,256]{1,0:T(8,128)(2,1)S(1)}, f32[32,256]{1,0:T(8,128)S(1)}, f32[2,448,128]{2,1,0:T(8,128)S(1)}) custom-call(s32[1]{0:T(128)} %bitcast._.place, f32[4,8,128]{2,1,0:T(8,128)S(1)} %all_to_all.15.sums, f32[2,352,128]{2,1,0:T(8,128)S(1)} %get-tuple-element.31.scaled, ...), custom_call_target="tpu_custom_call" | custom-call | flops 402653184 | bytes 4892160 | tf_op jit(solution)/shard_map/pallas_call | solution.py:412
  19.1 0.0 copy-start.4
  19.2 1.9 %collective-permute-start.1 = (bf16[1088,256]{1,0:T(8,128)(2,1)S(1)}, bf16[1088,256]{1,0:T(8,128)(2,1)S(1)}, u32[]{:S(2)}, u32[]{:S(2)}) collective-permute-start(bf16[1088,256]{1,0:T(8,128)(2,1)S(1)} %get-tuple-element.40), channel_id=1, source_target_pairs={{0,4},{4,0},{1,5},{5,1},{2,6},{6,2},{3,7},{7,3},{8,12},{12,8},{9,1... | collective-permute-start | bytes 1671176 | tf_op jit(solution)/shard_map/ppermute | solution.py:372
  21.1 1.9 %collective-permute-done.1.other = bf16[1088,256]{1,0:T(8,128)(2,1)S(1)} collective-permute-done((bf16[1088,256]{1,0:T(8,128)(2,1)S(1)}, bf16[1088,256]{1,0:T(8,128)(2,1)S(1)}, u32[]{:S(2)}, u32[]{:S(2)}) %collective-permute-start.1) | collective-permute-done | bytes 557088 | tf_op jit(solution)/shard_map/ppermute | solution.py:372
  23.0 0.1 shard_map.122
  23.1 21.2 %all_to_all.16.arrived = bf16[8,160,256]{2,1,0:T(8,128)(2,1)S(1)} all-to-all(bf16[8,160,256]{2,1,0:T(8,128)(2,1)S(1)} %shard_map.122), channel_id=1, replica_groups=mesh['zh'=16,'zl'=2,'x'=4,'c'=2,'tp'=4] {'zl','x'}, dimensions={0} | all-to-all | bytes 1310720 | tf_op jit(solution)/shard_map/all_to_all | solution.py:42
  44.3 0.0 copy-done.4
  44.3 0.1 shard_map.123
  44.4 12.0 %collective-permute-start.2 = (bf16[160,256]{1,0:T(8,128)(2,1)S(1)}, bf16[160,256]{1,0:T(8,128)(2,1)S(1)}, u32[]{:S(2)}, u32[]{:S(2)}) collective-permute-start(bf16[160,256]{1,0:T(8,128)(2,1)S(1)} %shard_map.123), channel_id=1, source_target_pairs={{0,0},{4,516},{8,968},{12,460},{16,912},{20,404},{24,856},{28,348}... | collective-permute-start | bytes 245768 | tf_op jit(solution)/shard_map/ppermute | solution.py:316
  56.5 6.4 %collective-permute-done.2.payload = bf16[160,256]{1,0:T(8,128)(2,1)S(1)} collective-permute-done((bf16[160,256]{1,0:T(8,128)(2,1)S(1)}, bf16[160,256]{1,0:T(8,128)(2,1)S(1)}, u32[]{:S(2)}, u32[]{:S(2)}) %collective-permute-start.2) | collective-permute-done | bytes 81952 | tf_op jit(solution)/shard_map/ppermute | solution.py:316
  62.8 0.7 shard_map.124
  63.6 10.7 %all-to-all-start.2 = ((bf16[16,40,256]{2,1,0:T(8,128)(2,1)}), bf16[16,40,256]{2,1,0:T(8,128)(2,1)S(1)}, u32[]{:S(2)}, u32[]{:S(2)}) async-start(bf16[16,40,256]{2,1,0:T(8,128)(2,1)} %shard_map.124), calls=%async_computation.2 | async-start | bytes 655360 | tf_op jit(solution)/shard_map/all_to_all | solution.py:42
  74.2 0.0 copy-start.5
  74.2 1.0 %copy-done.5 = f32[2,448,128]{2,1,0:T(8,128)S(1)} copy-done((f32[2,448,128]{2,1,0:T(8,128)S(1)}, f32[2,448,128]{2,1,0:T(8,128)}, u32[]{:S(2)}) %copy-start.5) | copy-done | bytes 458776
  75.3 0.9 %shard_map.126 = (f32[2,384,128]{2,1,0:T(8,128)S(1)}, f32[2,32,128]{2,1,0:T(8,128)S(1)}) custom-call(f32[2,448,128]{2,1,0:T(8,128)S(1)} %copy-done.5, bf16[31,256]{1,0:T(8,128)(2,1)S(1)} %copy-done.6), custom_call_target="tpu_custom_call" | custom-call | flops 9830400 | bytes 900608 | tf_op jit(solution)/shard_map/pallas_call | solution.py:399
  76.1 2.3 %collective-permute-start.3 = (f32[2,32,128]{2,1,0:T(8,128)S(1)}, f32[2,32,128]{2,1,0:T(8,128)S(1)}, u32[]{:S(2)}, u32[]{:S(2)}) collective-permute-start(f32[2,32,128]{2,1,0:T(8,128)S(1)} %get-tuple-element.43), channel_id=1, source_target_pairs={{4,0},{8,4},{12,8},{16,12},{20,16},{24,20},{28,24},{32,28},{36,32}... | collective-permute-start | bytes 98312 | tf_op jit(solution)/shard_map/ppermute | solution.py:37
  78.4 2.6 %all-to-all-done.2.arrived = bf16[16,40,256]{2,1,0:T(8,128)(2,1)S(1)} async-done(((bf16[16,40,256]{2,1,0:T(8,128)(2,1)}), bf16[16,40,256]{2,1,0:T(8,128)(2,1)S(1)}, u32[]{:S(2)}, u32[]{:S(2)}) %all-to-all-start.2) | async-done | bytes 327712 | tf_op jit(solution)/shard_map/all_to_all | solution.py:42
  81.1 2.4 %collective-permute-done.3.late = f32[2,32,128]{2,1,0:T(8,128)S(1)} collective-permute-done((f32[2,32,128]{2,1,0:T(8,128)S(1)}, f32[2,32,128]{2,1,0:T(8,128)S(1)}, u32[]{:S(2)}, u32[]{:S(2)}) %collective-permute-start.3) | collective-permute-done | bytes 32800 | tf_op jit(solution)/shard_map/ppermute | solution.py:37
  83.5 0.9 %shard_map.127 = (bf16[384,256]{1,0:T(8,128)(2,1)}, bf16[384,256]{1,0:T(8,128)(2,1)}, f32[8,256]{1,0:T(8,128)}, f32[31,256]{1,0:T(8,128)}, f32[1,256]{1,0:T(1,128)}) custom-call(f32[40,256]{1,0:T(8,128)S(1)} %shard_map.125.total, f32[2,384,128]{2,1,0:T(8,128)S(1)} %get-tuple-element.42.d_gated, f32[2,32,128]{2,1,0:T(8,128)S(1)} %collective-permute-done.3.late, ...), custom_call_target="tpu_custom_call" | custom-call | flops 983040 | bytes 1294336 | tf_op jit(solution)/shard_map/pallas_call | solution.py:56
  (1 shorter events, 0.0 us)
Async XLA Ops:
  0.6 5.1 %copy-start = (bf16[256,2048]{1,0:T(8,128)(2,1)S(1)}, bf16[256,2048]{1,0:T(8,128)(2,1)}, u32[]{:S(2)}) copy-start(bf16[256,2048]{1,0:T(8,128)(2,1)} %param.11) | copy-start | bytes 3145732
  0.6 7.1 %copy-start.2 = (bf16[384,256]{1,0:T(8,128)(2,1)S(1)}, bf16[384,256]{1,0:T(8,128)(2,1)}, u32[]{:S(2)}) copy-start(bf16[384,256]{1,0:T(8,128)(2,1)} %gate.3) | copy-start | bytes 589828
  0.7 7.1 %copy-start.3 = (bf16[384,256]{1,0:T(8,128)(2,1)S(1)}, bf16[384,256]{1,0:T(8,128)(2,1)}, u32[]{:S(2)}) copy-start(bf16[384,256]{1,0:T(8,128)(2,1)} %value.3) | copy-start | bytes 589828
  0.7 7.1 %copy-start.7 = (f32[384]{0:T(512)S(1)}, f32[384]{0:T(512)}, u32[]{:S(2)}) copy-start(f32[384]{0:T(512)} %scale.5) | copy-start | bytes 4612
  0.7 7.1 %copy-start.6 = (bf16[31,256]{1,0:T(8,128)(2,1)S(1)}, bf16[31,256]{1,0:T(8,128)(2,1)}, u32[]{:S(2)}) copy-start(bf16[31,256]{1,0:T(8,128)(2,1)} %taps.5) | copy-start | bytes 47620
  0.7 7.1 %copy-start.8 = (f32[384]{0:T(512)S(1)}, f32[384]{0:T(512)}, u32[]{:S(2)}) copy-start(f32[384]{0:T(512)} %mean.3) | copy-start | bytes 4612
  0.7 7.1 %copy-start.9 = (f32[256]{0:T(256)S(1)}, f32[256]{0:T(256)}, u32[]{:S(2)}) copy-start(f32[256]{0:T(256)} %param.13) | copy-start | bytes 3076
  1.6 15.7 %copy-start.1 = (bf16[384,2048]{1,0:T(8,128)(2,1)S(1)}, bf16[384,2048]{1,0:T(8,128)(2,1)}, u32[]{:S(2)}) copy-start(bf16[384,2048]{1,0:T(8,128)(2,1)} %cotangent.1) | copy-start | bytes 4718596
  1.6 7.5 %collective-permute-start = (bf16[32,256]{1,0:T(8,128)(2,1)S(1)}, bf16[32,256]{1,0:T(8,128)(2,1)S(1)}, u32[]{:S(2)}, u32[]{:S(2)}) collective-permute-start(bf16[32,256]{1,0:T(8,128)(2,1)S(1)} %multiply_convert_fusion), channel_id=1, source_target_pairs={{0,4},{4,8},{8,12},{12,16},{16,20},{20,24},{24,28},{28,32},{32,36}... | collective-permute-start | bytes 49160 | tf_op jit(solution)/shard_map/ppermute | solution.py:37
  19.1 25.2 %copy-start.4 = (f32[2,448,128]{2,1,0:T(8,128)}, f32[2,448,128]{2,1,0:T(8,128)S(1)}, u32[]{:S(2)}) copy-start(f32[2,448,128]{2,1,0:T(8,128)S(1)} %get-tuple-element.41.extended) | copy-start | bytes 1376260
  19.2 3.9 %collective-permute-start.1 = (bf16[1088,256]{1,0:T(8,128)(2,1)S(1)}, bf16[1088,256]{1,0:T(8,128)(2,1)S(1)}, u32[]{:S(2)}, u32[]{:S(2)}) collective-permute-start(bf16[1088,256]{1,0:T(8,128)(2,1)S(1)} %get-tuple-element.40), channel_id=1, source_target_pairs={{0,4},{4,0},{1,5},{5,1},{2,6},{6,2},{3,7},{7,3},{8,12},{12,8},{9,1... | collective-permute-start | bytes 1671176 | tf_op jit(solution)/shard_map/ppermute | solution.py:372
  44.4 18.4 %collective-permute-start.2 = (bf16[160,256]{1,0:T(8,128)(2,1)S(1)}, bf16[160,256]{1,0:T(8,128)(2,1)S(1)}, u32[]{:S(2)}, u32[]{:S(2)}) collective-permute-start(bf16[160,256]{1,0:T(8,128)(2,1)S(1)} %shard_map.123), channel_id=1, source_target_pairs={{0,0},{4,516},{8,968},{12,460},{16,912},{20,404},{24,856},{28,348}... | collective-permute-start | bytes 245768 | tf_op jit(solution)/shard_map/ppermute | solution.py:316
  63.6 17.4 %all-to-all-start.2 = ((bf16[16,40,256]{2,1,0:T(8,128)(2,1)}), bf16[16,40,256]{2,1,0:T(8,128)(2,1)S(1)}, u32[]{:S(2)}, u32[]{:S(2)}) async-start(bf16[16,40,256]{2,1,0:T(8,128)(2,1)} %shard_map.124), calls=%async_computation.2 | async-start | bytes 655360 | tf_op jit(solution)/shard_map/all_to_all | solution.py:42
  74.2 1.0 %copy-start.5 = (f32[2,448,128]{2,1,0:T(8,128)S(1)}, f32[2,448,128]{2,1,0:T(8,128)}, u32[]{:S(2)}) copy-start(f32[2,448,128]{2,1,0:T(8,128)} %copy-done.4) | copy-start | bytes 1376260
  76.1 7.3 %collective-permute-start.3 = (f32[2,32,128]{2,1,0:T(8,128)S(1)}, f32[2,32,128]{2,1,0:T(8,128)S(1)}, u32[]{:S(2)}, u32[]{:S(2)}) collective-permute-start(f32[2,32,128]{2,1,0:T(8,128)S(1)} %get-tuple-element.43), channel_id=1, source_target_pairs={{4,0},{8,4},{12,8},{16,12},{20,16},{24,20},{28,24},{32,28},{36,32}... | collective-permute-start | bytes 98312 | tf_op jit(solution)/shard_map/ppermute | solution.py:37
